TPU v7x, 256 devices: a whole 4x4x8 slice. The times are simulated.
256 devices in a mesh: sp: 64 (over z, x, core), tp: 4 (over y).
Axes of the slice: x: 4, y: 4, z: 8, core: 2. Of those that a mesh axis runs over, the one named last changes fastest.
Arguments:
- stream: bfloat16 [8192, 2048], P(('sp', 'tp')), may hold values from -2.5 to 2.5
- recurrence_input: bfloat16 [8192, 2, 1024], P('sp', None, 'tp'), may hold values from -6 to 6
- output_gate_input: bfloat16 [8192, 2, 1024], P('sp', None, 'tp'), may hold values from -6 to 6
- convolution_taps: bfloat16 [4, 2, 1024], P(None, None, 'tp'), may hold values from -4 to 4
- first_group_gates: bfloat16 [2, 16, 64, 64], P(None, 'tp'), may hold values from -0.75 to 0.75
- second_group_gates: bfloat16 [2, 8, 128, 128], P(None, 'tp'), may hold values from -0.5 to 0.5
- channel_decay: float32 [2, 1024], P(None, 'tp'), may hold values from 4.7 to 13.6
- position_log_extra: float32 [8192, 2, 1024], P('sp', None, 'tp'), may hold values from -1.4 to 0, as said below
- recurrence_output_weight: bfloat16 [2, 1024, 2048], P(None, 'tp'), may hold values from -0.125 to 0.125
- first_norm_gain: float32 [2048], replicated, may hold values from 0.1 to 1.9
- first_norm_bias: float32 [2048], replicated, may hold values from -1.75 to 1.75
- routed_expert_index: int32 [8192, 4], P('sp'), may hold values from 0 to 63, all different within a row; in each aligned block of 32 rows (0 to 31, 32 to 63, ...) at most 2 rows name the same one
- routed_expert_weight: float32 [8192, 4], P('sp'), may hold values from 0.25 to 1
- routed_gate_weight: bfloat16 [64, 2048, 512], P('sp', None, 'tp'), may hold values from -0.125 to 0.125
- routed_up_weight: bfloat16 [64, 2048, 512], P('sp', None, 'tp'), may hold values from -0.125 to 0.125
- routed_down_weight: bfloat16 [64, 512, 2048], P('sp', 'tp'), may hold values from -0.25 to 0.25
- shared_gate_weight: bfloat16 [2048, 512], replicated, may hold values from -0.125 to 0.125
- shared_up_weight: bfloat16 [2048, 512], replicated, may hold values from -0.125 to 0.125
- shared_down_weight: bfloat16 [512, 2048], replicated, may hold values from -0.25 to 0.25
- second_norm_gain: float32 [2048], replicated, may hold values from 0.1 to 1.9
- second_norm_bias: float32 [2048], replicated, may hold values from -1.75 to 1.75
Outputs:
- result: bfloat16 [8192, 2048], P(('sp', 'tp'))
Inputs may be any that keep to these rules, and one draw needn't show every extreme that they name: `routed_expert_index`: each row names 4 different experts. In each aligned block of 32 rows no expert is named more than 2 times, and in some block an expert is named exactly 2 times. `position_log_extra`: every entry is negative.
All inputs are finite; a program needn't handle non-finite values.
Results may differ from a plain program's by a relative error of at most 0.015.
Values may be sent and summed in bfloat16 or wider, within the bound.
No kernel may reach another device: no remote copies, remote signals or barrier semaphores. Data moves between devices by JAX's collectives and lax.ppermute only.
A program may use at most 64 MiB of HBM per device.

v0:
```python
import jax
import jax.numpy as jnp
from jax import lax
from jax.sharding import PartitionSpec as P

RESIDUAL_SCALE = 8.0**0.25
NORM_EPSILON = 1e-05


def copy_for_each(shard, axis):
    count = lax.axis_size(axis)
    return lax.all_to_all(
        jnp.broadcast_to(shard[None], (count, *shard.shape)), axis, 0, 0, tiled=True
    )


def all_in_one(shard, axis):
    leaves = jax.tree.leaves(shard)
    sequence = sorted(range(len(leaves)), key=lambda k: -leaves[k].size)
    width = (1, *leaves[sequence[0]].shape)[-1]
    lines = [
        jnp.pad(leaves[k].reshape(-1), (0, -leaves[k].size % width)).reshape(-1, width)
        for k in sequence
    ]
    both, at, found = (copy_for_each(jnp.concatenate(lines), axis), 0, {})
    for k, line in zip(sequence, lines):
        slab = both[:, at : at + len(line)].reshape(len(both), -1)
        found[k] = slab[:, : leaves[k].size].reshape(-1, *leaves[k].shape)
        at += len(line)
    numbers = iter(range(len(leaves)))
    return jax.tree.map(lambda _: found[next(numbers)], shard)


def joined_by_halves(pieces, combine):
    while len(jax.tree.leaves(pieces)[0]) > 1:
        pieces = jax.vmap(combine)(
            *(jax.tree.map(lambda part: part[side::2], pieces) for side in (0, 1))
        )
    return jax.tree.map(lambda part: part[0], pieces)


def entering(shard, axis, combine, identity):
    count, mine = (lax.axis_size(axis), lax.axis_index(axis))
    passed = jnp.arange(count) < mine

    def kept(part, zero, own):
        part = jnp.where(
            passed.reshape(-1, *(1 for _ in own.shape)), part, jnp.asarray(zero, own.dtype)
        )
        return part

    pieces = all_in_one(shard, axis)
    return joined_by_halves(jax.tree.map(kept, pieces, identity, shard), combine)


def shifted(shard, axis, by):
    count = lax.axis_size(axis)
    pairs = [(i, i + by) for i in range(count) if 0 <= i + by < count]
    return lax.ppermute(shard, axis, pairs)


def cut_along(shard, dim, count):
    dims = shard.shape
    pieces = shard.reshape(*dims[:dim], count, dims[dim] // count, *dims[dim + 1 :])
    return jnp.moveaxis(pieces, dim, 0)


def summed_on_arrival(shard, axis, dim):
    count = lax.axis_size(axis)
    pieces = lax.all_to_all(cut_along(shard, dim, count), axis, 0, 0, tiled=True)
    return jnp.sum(pieces.astype(jnp.float32), axis=0)


def layer_norm(values, gain_vec, bias_vec):
    row_mean = jnp.mean(values, axis=-1, keepdims=True)
    spread = jnp.mean(jnp.square(values - row_mean), axis=-1, keepdims=True)
    return (values - row_mean) * lax.rsqrt(spread + NORM_EPSILON) * gain_vec + bias_vec


def block_gates(conv_rows, weights, head_size):
    length = conv_rows.shape[0]
    head_rows = conv_rows.reshape(length, -1, head_size)
    pre_act = jnp.einsum("thc,ghcd->gthd", head_rows, weights, preferred_element_type=jnp.float32)
    gate_pair = jax.nn.sigmoid(pre_act).reshape(2, length, -1)
    return (gate_pair[0], gate_pair[1])


def chain_link(first_part, second_part):
    return (first_part[0] * second_part[0], second_part[0] * first_part[1] + second_part[1])


def carried(totals):
    unity = jnp.ones_like(totals[0])
    nought = jnp.zeros_like(totals[1])
    return entering(totals, "sp", chain_link, (unity, nought))[1]


def expert_terms(picked, letters, gate_w, up_w, down_w):
    gate_form = letters + "d,ldf->" + letters + "f"
    down_form = letters + "f,lfd->" + letters + "d"
    gated = jnp.einsum(gate_form, picked, gate_w, preferred_element_type=jnp.float32)
    lifted = jnp.einsum(gate_form, picked, up_w, preferred_element_type=jnp.float32)
    hidden = (jax.nn.silu(gated) * lifted).astype(jnp.bfloat16)
    return jnp.einsum(down_form, hidden, down_w, preferred_element_type=jnp.float32)


def shards(
    stream,
    recurrence_input,
    output_gate_input,
    convolution_taps,
    first_group_gates,
    second_group_gates,
    channel_decay,
    position_log_extra,
    recurrence_output_weight,
    first_norm_gain,
    first_norm_bias,
    routed_expert_index,
    routed_expert_weight,
    routed_gate_weight,
    routed_up_weight,
    routed_down_weight,
    shared_gate_weight,
    shared_up_weight,
    shared_down_weight,
    second_norm_gain,
    second_norm_bias,
):
    length = recurrence_input.shape[0]
    tap_count = convolution_taps.shape[0]
    border = shifted(recurrence_input[length - (tap_count - 1) :], "sp", 1)
    padded = jnp.concatenate([border, recurrence_input], axis=0).astype(jnp.float32)
    tap_weights = convolution_taps.astype(jnp.float32)
    summed = tap_weights[0] * padded[0:length]
    for offset in range(1, tap_count):
        summed = summed + tap_weights[offset] * padded[offset : offset + length]
    conv_rows = summed.astype(jnp.bfloat16)
    recur_a, input_a = block_gates(conv_rows[:, 0], first_group_gates, first_group_gates.shape[-1])
    recur_b, input_b = block_gates(
        conv_rows[:, 1], second_group_gates, second_group_gates.shape[-1]
    )
    recurrence_gate = jnp.stack([recur_a, recur_b], axis=1)
    input_gate = jnp.stack([input_a, input_b], axis=1)
    decay_logarithm = -8.0 * recurrence_gate * jax.nn.softplus(-channel_decay) + position_log_extra
    decay_rate = jnp.exp(decay_logarithm)
    driving = (
        jnp.sqrt(-jnp.expm1(2.0 * decay_logarithm)) * input_gate * conv_rows.astype(jnp.float32)
    )
    running = jnp.cumsum(decay_logarithm, axis=0)
    tail_sum = jnp.sum(jnp.exp(running[-1] - running) * driving, axis=0)
    incoming = carried((jnp.exp(running[-1]), tail_sum))
    opening = driving[:1] + decay_rate[:1] * incoming
    started = jnp.concatenate([opening, driving[1:]], axis=0)
    states = lax.associative_scan(chain_link, (decay_rate, started), axis=0)[1]
    branch_output = (jax.nn.gelu(output_gate_input.astype(jnp.float32)) * states).astype(
        jnp.bfloat16
    )
    tp_count = lax.axis_size("tp")
    quarter = length // tp_count
    mixed = summed_on_arrival(
        jnp.einsum(
            "tgc,gcd->td",
            branch_output,
            recurrence_output_weight,
            preferred_element_type=jnp.float32,
        ).astype(jnp.bfloat16),
        "tp",
        0,
    )
    normed = layer_norm(
        RESIDUAL_SCALE * stream.astype(jnp.float32) + mixed, first_norm_gain, first_norm_bias
    ).astype(jnp.bfloat16)
    width = normed.shape[1]
    top_count = routed_expert_index.shape[1]
    local_count = routed_gate_weight.shape[0]
    expert_count = local_count * lax.axis_size("sp")
    capacity = max(2, 5 * quarter * top_count // (4 * expert_count))
    block_ids = routed_expert_index.reshape(tp_count, quarter * top_count)
    onehot = (
        block_ids[:, :, None] == jnp.arange(expert_count, dtype=jnp.int32)[None, None, :]
    ).astype(jnp.int32)
    slot_ranks = jnp.sum((jnp.cumsum(onehot, axis=1) - onehot) * onehot, axis=2)
    own_index = lax.axis_index("tp")
    own_ids = lax.dynamic_index_in_dim(block_ids, own_index, 0, keepdims=False)
    own_ranks = lax.dynamic_index_in_dim(slot_ranks, own_index, 0, keepdims=False)
    blank_row = jnp.zeros((1, width), jnp.bfloat16)
    padded_rows = jnp.concatenate([normed, blank_row], axis=0)
    targets = own_ids * capacity + own_ranks
    sources = jnp.arange(quarter * top_count, dtype=jnp.int32) // top_count
    table = jnp.full((expert_count * capacity,), quarter, jnp.int32).at[targets].set(sources)
    outgoing = jnp.take(padded_rows, table, axis=0).reshape(expert_count, capacity, width)
    arrived = lax.all_to_all(outgoing, "sp", split_axis=0, concat_axis=0, tiled=True)
    slots = arrived.shape[1]
    fanned = lax.all_gather(arrived[None], "tp", axis=0, tiled=True)
    shaped = fanned.reshape(tp_count, -1, local_count, slots, width)
    partial_value = expert_terms(
        shaped, "xslc", routed_gate_weight, routed_up_weight, routed_down_weight
    )
    summed_rows = summed_on_arrival(partial_value.astype(jnp.bfloat16), "tp", 0)
    leaving = summed_rows.astype(jnp.bfloat16).reshape(-1, slots, width)
    returned = lax.all_to_all(leaving, "sp", split_axis=0, concat_axis=0, tiled=True)
    picked_rows = returned.reshape(expert_count * capacity, width)[own_ids * capacity + own_ranks]
    own_weights = lax.dynamic_slice_in_dim(routed_expert_weight, own_index * quarter, quarter, 0)
    routed = jnp.sum(
        own_weights[:, :, None]
        * picked_rows.reshape(quarter, top_count, width).astype(jnp.float32),
        axis=1,
    )
    shared_hidden = (
        jax.nn.silu(jnp.dot(normed, shared_gate_weight, preferred_element_type=jnp.float32))
        * jnp.dot(normed, shared_up_weight, preferred_element_type=jnp.float32)
    ).astype(jnp.bfloat16)
    shared_out = jnp.dot(shared_hidden, shared_down_weight, preferred_element_type=jnp.float32)
    final = layer_norm(
        RESIDUAL_SCALE * normed.astype(jnp.float32) + (shared_out + routed),
        second_norm_gain,
        second_norm_bias,
    )
    return final.astype(jnp.bfloat16)


def solution(mesh):
    in_specs = (
        P(("sp", "tp"), None),
        P("sp", None, "tp"),
        P("sp", None, "tp"),
        P(None, None, "tp"),
        P(None, "tp", None, None),
        P(None, "tp", None, None),
        P(None, "tp"),
        P("sp", None, "tp"),
        P(None, "tp", None),
        P(),
        P(),
        P("sp", None),
        P("sp", None),
        P("sp", None, "tp"),
        P("sp", None, "tp"),
        P("sp", "tp", None),
        P(),
        P(),
        P(),
        P(),
        P(),
    )
    out_specs = P(("sp", "tp"), None)
    return jax.shard_map(shards, mesh=mesh, in_specs=in_specs, out_specs=out_specs, check_vma=False)
```

profile of v0, /device:TPU:1, one launch (start us, length us, event | category | flops | bytes accessed | tf_op | source)
XLA Modules:
  0.0 205.7 jit_solution(793034132163294517)
XLA Ops:
  6.5 1.1 copy.130
  7.6 4.5 %collective-permute-start = (bf16[3,2,256]{2,0,1:T(4,128)(2,1)S(1)}, bf16[3,2,256]{2,0,1:T(4,128)(2,1)S(1)}, u32[]{:S(2)}, u32[]{:S(2)}) collective-permute-start(bf16[3,2,256]{2,0,1:T(4,128)(2,1)S(1)} %slice.395), channel_id=1, source_target_pairs={{0,4},{4,8},{8,12},{12,16},{16,20},{20,24},{24,28},{28,32},{32,36}... | collective-permute-start | bytes 9224 | tf_op jit(solution)/shard_map/ppermute | solution.py:59
  12.1 0.7 convert_element_type.67
  12.9 0.7 fusion.84
  13.6 0.8 copy.147
  14.4 0.7 reshape.136
  15.1 0.1 fusion.45
  15.2 0.1 copy.132
  15.4 0.3 fusion.20
  15.7 0.1 copy.138
  15.8 0.1 copy.134
  16.0 0.3 fusion.16
  16.3 0.1 copy.165
  16.4 1.0 fusion.101
  17.4 0.2 fusion.53
  17.6 0.6 slice_bitcast_fusion
  18.1 0.6 fusion.99
  18.7 0.1 copy.141
  18.8 0.8 copy.166
  19.6 1.2 fusion.52
  20.9 0.7 broadcast_in_dim.61
  21.6 11.3 %all-to-all-start = ((f32[64,4,256]{2,1,0:T(4,128)}), f32[64,4,256]{2,1,0:T(4,128)S(1)}, u32[]{:S(2)}, u32[]{:S(2)}) async-start(f32[64,4,256]{2,1,0:T(4,128)} %broadcast_in_dim.61), calls=%async_computation | async-start | bytes 524288 | tf_op jit(solution)/shard_map/all_to_all | solution.py:12
  32.9 0.8 fusion.60
  33.7 0.3 reduce_window_sum.23
  34.0 0.9 select_reduce_fusion
  34.9 0.7 fusion.90
  35.6 1.5 scatter_custom_fusion
  37.1 0.7 slice.345
  37.9 0.7 slice.343
  38.7 7.3 %all-to-all-done = f32[64,4,256]{2,1,0:T(4,128)S(1)} async-done(((f32[64,4,256]{2,1,0:T(4,128)}), f32[64,4,256]{2,1,0:T(4,128)S(1)}, u32[]{:S(2)}, u32[]{:S(2)}) %all-to-all-start) | async-done | bytes 262176 | tf_op jit(solution)/shard_map/all_to_all | solution.py:12
  46.0 0.1 fusion.103
  46.2 0.6 slice.315
  46.8 0.6 slice.316
  47.5 0.9 fusion.109
  49.0 1.0 fusion.106
  51.7 1.3 fusion.1
  53.0 4.3 %all-to-all-start.1 = ((bf16[4,32,2048]{2,1,0:T(8,128)(2,1)}), bf16[4,32,2048]{2,1,0:T(8,128)(2,1)S(1)}, u32[]{:S(2)}, u32[]{:S(2)}) async-start(bf16[4,32,2048]{2,1,0:T(8,128)(2,1)} %bitcast.17), calls=%async_computation.1 | async-start | bytes 1048576 | tf_op jit(solution)/shard_map/all_to_all | solution.py:70
  57.3 0.1 broadcast_in_dim.65
  57.5 8.8 %all-to-all-done.1 = bf16[4,32,2048]{2,1,0:T(8,128)(2,1)S(1)} async-done(((bf16[4,32,2048]{2,1,0:T(8,128)(2,1)}), bf16[4,32,2048]{2,1,0:T(8,128)(2,1)S(1)}, u32[]{:S(2)}, u32[]{:S(2)}) %all-to-all-start.1) | async-done | bytes 524320 | tf_op jit(solution)/shard_map/all_to_all | solution.py:70
  66.4 0.2 fusion.71
  66.6 0.2 multiply_reduce_fusion.2
  66.8 0.1 add_convert_fusion.1
  67.0 0.9 gather_fusion
  67.9 1.1 gather.10
  69.0 1.6 broadcast_select_fusion
  70.6 23.1 %all_to_all.25 = bf16[64,2,2048]{2,1,0:T(2,128)(2,1)S(1)} all-to-all(bf16[64,2,2048]{2,1,0:T(2,128)(2,1)S(1)} %broadcast_select_fusion), channel_id=1, replica_groups=mesh['sp'=64,'tp'=4] {'sp'}, dimensions={0} | all-to-all | bytes 1048576 | tf_op jit(solution)/shard_map/all_to_all | solution.py:193
  93.8 1.0 copy.148
  94.8 27.8 %all-gather.3.cloned.1.call-done = bf16[256,2,2048]{2,0,1:T(8,128)(2,1)} async-done(((bf16[64,2,2048]{2,0,1:T(8,128)(2,1)}), bf16[256,2,2048]{2,0,1:T(8,128)(2,1)}) %all-gather.3.cloned.1.call-update) | async-done | bytes 2097168 | tf_op jit(solution)/shard_map/all_gather | solution.py:195
  122.6 2.4 %fusion.7 = f32[4,64,1,2,128]{4,1,3,0,2:T(8,128)S(1)} fusion(bf16[4,64,2,2048]{3,1,0,2:T(8,128)(2,1)} %bitcast.118, bf16[1,2048,128]{2,1,0:T(8,128)(2,1)} %param.34), kind=kOutput, calls=%fused_computation.14 | convolution fusion | flops 268435456 | bytes 2883584 | tf_op jit(solution)/shard_map/xslcd,ldf->xslcf/dot_general | solution.py:101
  125.0 5.2 %fusion = bf16[4,1,64,1,2,2048]{5,2,4,3,1,0:T(8,128)(2,1)} fusion(bf16[4,64,2,2048]{3,1,0,2:T(8,128)(2,1)} %bitcast.119, bf16[1,128,2048]{2,1,0:T(8,128)(2,1)S(1)} %copy-done.2, bf16[1,2048,128]{2,1,0:T(8,128)(2,1)S(1)} %copy-done.3, f32[4,64,1,2,128]{4,1,3,0,2:T(8,128)S(1)} %fusion.7), kind=kOutput, calls=%fused_computation.4 | convolution fusion | flops 538312704 | bytes 5505024 | tf_op jit(solution)/shard_map/xslcf,lfd->xslcd/dot_general | solution.py:104
  130.2 28.9 %all_to_all.26 = bf16[4,1,64,1,2,2048]{5,2,4,3,1,0:T(8,128)(2,1)S(1)} all-to-all(bf16[4,1,64,1,2,2048]{5,2,4,3,1,0:T(8,128)(2,1)} %fusion), channel_id=1, replica_groups=mesh['sp'=64,'tp'=4] {'tp'}, dimensions={0} | all-to-all | bytes 4194304 | tf_op jit(solution)/shard_map/all_to_all | solution.py:70
  159.2 0.4 bitcast_reduce_fusion
  159.5 1.3 copy.153
  160.9 11.9 %all-to-all-start.4 = ((bf16[64,2,2048]{2,1,0:T(2,128)(2,1)}), bf16[64,2,2048]{2,1,0:T(2,128)(2,1)S(1)}, u32[]{:S(2)}, u32[]{:S(2)}) async-start(bf16[64,2,2048]{2,1,0:T(2,128)(2,1)} %copy.153), calls=%async_computation.4 | async-start | bytes 1048576 | tf_op jit(solution)/shard_map/all_to_all | solution.py:202
  172.9 0.1 copy.146
  173.0 2.7 %fusion.118 = f32[32,512]{1,0:T(8,128)} fusion(bf16[32,2048]{1,0:T(8,128)(2,1)S(1)} %add_convert_fusion.1, bf16[2048,512]{1,0:T(8,128)(2,1)} %param.37), kind=kOutput, calls=%fused_computation.192 | convolution fusion | flops 67108864 | bytes 2293760 | tf_op jit(solution)/shard_map/dot_general | solution.py:211
  175.6 14.8 %all-to-all-done.4 = bf16[64,2,2048]{2,1,0:T(2,128)(2,1)S(1)} async-done(((bf16[64,2,2048]{2,1,0:T(2,128)(2,1)}), bf16[64,2,2048]{2,1,0:T(2,128)(2,1)S(1)}, u32[]{:S(2)}, u32[]{:S(2)}) %all-to-all-start.4) | async-done | bytes 524320 | tf_op jit(solution)/shard_map/all_to_all | solution.py:202
  190.5 0.2 reshape.142
  190.7 1.7 gather_fusion.1
  192.4 1.4 reshape.143
  193.8 0.7 multiply_reduce_fusion
  194.5 3.3 %fusion.117 = (f32[32]{0:T(128)S(1)}, f32[32,2048]{1,0:T(8,128)S(1)}) fusion(f32[32,2048]{1,0:T(8,128)S(1)} %multiply_reduce_fusion, bf16[512,2048]{1,0:T(8,128)(2,1)} %param.39, bf16[32,2048]{1,0:T(8,128)(2,1)S(1)} %add_convert_fusion.1, bf16[2048,512]{1,0:T(8,128)(2,1)} %param.38, f32[32,512]{1,0:T(8,128)} %fusion.118), kind=kOutput, calls=%fused_computation.191 | convolution fusion | flops 134643680 | bytes 4915328 | tf_op jit(solution)/shard_map/dot_general | solution.py:214
  197.8 0.2 multiply_reduce_fusion.1
  198.0 0.8 add_convert_fusion
  (165 shorter events, 2.6 us)
Async XLA Ops:
  6.5 45.1 %copy-start = (bf16[2,256,2048]{2,1,0:T(8,128)(2,1)S(1)}, bf16[2,256,2048]{2,1,0:T(8,128)(2,1)}, u32[]{:S(2)}) copy-start(bf16[2,256,2048]{2,1,0:T(8,128)(2,1)} %param.29) | copy-start | bytes 6291460
  6.5 8.9 %copy-start.19 = (bf16[2,4,64,64]{3,2,1,0:T(8,128)(2,1)S(1)}, bf16[2,4,64,64]{3,2,1,0:T(8,128)(2,1)}, u32[]{:S(2)}) copy-start(bf16[2,4,64,64]{3,2,1,0:T(8,128)(2,1)} %param.25) | copy-start | bytes 196612
  7.6 7.4 %collective-permute-start = (bf16[3,2,256]{2,0,1:T(4,128)(2,1)S(1)}, bf16[3,2,256]{2,0,1:T(4,128)(2,1)S(1)}, u32[]{:S(2)}, u32[]{:S(2)}) collective-permute-start(bf16[3,2,256]{2,0,1:T(4,128)(2,1)S(1)} %slice.395), channel_id=1, source_target_pairs={{0,4},{4,8},{8,12},{12,16},{16,20},{20,24},{24,28},{28,32},{32,36}... | collective-permute-start | bytes 9224 | tf_op jit(solution)/shard_map/ppermute | solution.py:59
  12.8 2.5 %copy-start.7 = (f32[2,256]{1,0:T(2,128)}, f32[2,256]{1,0:T(2,128)S(1)}, u32[]{:S(2)}) copy-start(f32[2,256]{1,0:T(2,128)S(1)} %get-tuple-element.37) | copy-start | bytes 6148
  12.8 2.5 %copy-start.8 = (f32[2,256]{1,0:T(2,128)}, f32[2,256]{1,0:T(2,128)S(1)}, u32[]{:S(2)}) copy-start(f32[2,256]{1,0:T(2,128)S(1)} %get-tuple-element.38) | copy-start | bytes 6148
  12.8 2.5 %copy-start.9 = (f32[2,256]{1,0:T(2,128)}, f32[2,256]{1,0:T(2,128)S(1)}, u32[]{:S(2)}) copy-start(f32[2,256]{1,0:T(2,128)S(1)} %get-tuple-element.39) | copy-start | bytes 6148
  12.9 2.5 %copy-start.10 = (f32[2,256]{1,0:T(2,128)}, f32[2,256]{1,0:T(2,128)S(1)}, u32[]{:S(2)}) copy-start(f32[2,256]{1,0:T(2,128)S(1)} %get-tuple-element.40) | copy-start | bytes 6148
  15.0 0.9 copy-start.20
  19.6 1.2 copy-start.15
  21.6 24.4 %all-to-all-start = ((f32[64,4,256]{2,1,0:T(4,128)}), f32[64,4,256]{2,1,0:T(4,128)S(1)}, u32[]{:S(2)}, u32[]{:S(2)}) async-start(f32[64,4,256]{2,1,0:T(4,128)} %broadcast_in_dim.61), calls=%async_computation | async-start | bytes 524288 | tf_op jit(solution)/shard_map/all_to_all | solution.py:12
  35.6 12.9 %copy-start.17 = (s32[128]{0:T(128)}, s32[128]{0:T(128)S(1)}, u32[]{:S(2)}) copy-start(s32[128]{0:T(128)S(1)} %fusion.90) | copy-start | bytes 1540
  48.9 1.2 copy-start.5
  50.3 1.2 copy-start.6
  50.8 0.9 copy-start.4
  51.7 5.6 %copy-start.21 = (s32[128]{0:T(128)S(1)}, s32[128]{0:T(128)}, u32[]{:S(2)}) copy-start(s32[128]{0:T(128)} %scatter_custom_fusion) | copy-start | bytes 1540
  51.7 14.7 %copy-start.1 = (bf16[32,2048]{1,0:T(8,128)(2,1)S(1)}, bf16[32,2048]{1,0:T(8,128)(2,1)}, u32[]{:S(2)}) copy-start(bf16[32,2048]{1,0:T(8,128)(2,1)} %param.21) | copy-start | bytes 393220
  53.0 13.8 %copy-start.11 = (f32[2048]{0:T(1024)S(1)}, f32[2048]{0:T(1024)}, u32[]{:S(2)}) copy-start(f32[2048]{0:T(1024)} %param.31) | copy-start | bytes 24580
  53.0 13.8 %copy-start.12 = (f32[2048]{0:T(1024)S(1)}, f32[2048]{0:T(1024)}, u32[]{:S(2)}) copy-start(f32[2048]{0:T(1024)} %param.30) | copy-start | bytes 24580
  53.0 13.3 %all-to-all-start.1 = ((bf16[4,32,2048]{2,1,0:T(8,128)(2,1)}), bf16[4,32,2048]{2,1,0:T(8,128)(2,1)S(1)}, u32[]{:S(2)}, u32[]{:S(2)}) async-start(bf16[4,32,2048]{2,1,0:T(8,128)(2,1)} %bitcast.17), calls=%async_computation.1 | async-start | bytes 1048576 | tf_op jit(solution)/shard_map/all_to_all | solution.py:70
  57.3 65.3 %all-gather.3.cloned.1.call-start = ((), (), s32[]{:S(2)}) async-start(), calls=%async_computation.5 | async-start | bytes 2621440 | tf_op jit(solution)/shard_map/all_gather | solution.py:195
  94.7 30.2 %copy-start.2 = (bf16[1,128,2048]{2,1,0:T(8,128)(2,1)S(1)}, bf16[1,128,2048]{2,1,0:T(8,128)(2,1)}, u32[]{:S(2)}) copy-start(bf16[1,128,2048]{2,1,0:T(8,128)(2,1)} %param.36) | copy-start | bytes 1572868
  94.7 30.2 %copy-start.3 = (bf16[1,2048,128]{2,1,0:T(8,128)(2,1)S(1)}, bf16[1,2048,128]{2,1,0:T(8,128)(2,1)}, u32[]{:S(2)}) copy-start(bf16[1,2048,128]{2,1,0:T(8,128)(2,1)} %param.35) | copy-start | bytes 1572868
  159.2 13.6 %copy-start.16 = (f32[128,4]{0,1:T(4,128)S(1)}, f32[128,4]{0,1:T(4,128)}, u32[]{:S(2)}) copy-start(f32[128,4]{0,1:T(4,128)} %param.33) | copy-start | bytes 6148
  159.2 13.8 %copy-start.18 = (s32[128]{0:T(128)S(1)}, s32[128]{0:T(128)}, u32[]{:S(2)}) copy-start(s32[128]{0:T(128)} %copy-done.17) | copy-start | bytes 1540
  160.9 29.6 %all-to-all-start.4 = ((bf16[64,2,2048]{2,1,0:T(2,128)(2,1)}), bf16[64,2,2048]{2,1,0:T(2,128)(2,1)S(1)}, u32[]{:S(2)}, u32[]{:S(2)}) async-start(bf16[64,2,2048]{2,1,0:T(2,128)(2,1)} %copy.153), calls=%async_computation.4 | async-start | bytes 1048576 | tf_op jit(solution)/shard_map/all_to_all | solution.py:202
  194.5 3.5 %copy-start.13 = (f32[2048]{0:T(1024)S(1)}, f32[2048]{0:T(1024)}, u32[]{:S(2)}) copy-start(f32[2048]{0:T(1024)} %param.41) | copy-start | bytes 24580
  194.5 3.5 %copy-start.14 = (f32[2048]{0:T(1024)S(1)}, f32[2048]{0:T(1024)}, u32[]{:S(2)}) copy-start(f32[2048]{0:T(1024)} %param.40) | copy-start | bytes 24580
Sparse Core Ops, SparseCore 0:
  94.9 27.6 all-gather.2
where the time goes:
time: 207 us; the launch traced here: 206 us
  waiting for transfers between devices  58.8 us (28%)
  blocking collectives  52.1 us (25%)
  starting transfers between devices  32 us (15%)
  local copies, waits for them, and re-layouts  19.8 us (10%)
  matrix products  15.4 us (7%)
  between operations  14.3 us (7%)
  other arithmetic  13.3 us (6%)
    all_to_all x1, blocking collectives, summed_on_arrival(): lax.all_to_all(cut_along(shard, dim, count), axis, 0, 0, tiled=True)  28.9 us
    all_gather x1, waiting for transfers between devices, shards(): fanned = lax.all_gather(arrived[None], 'tp', axis=0, tiled=True)  27.8 us
    all_to_all x1, blocking collectives, shards(): lax.all_to_all(outgoing, 'sp', split_axis=0, concat_axis=0, tiled=True)  23.1 us
    all_to_all x1, waiting for transfers between devices, shards(): lax.all_to_all(leaving, 'sp', split_axis=0, concat_axis=0, tiled=True)  14.8 us
    all_to_all x1, starting transfers between devices, shards(): lax.all_to_all(leaving, 'sp', split_axis=0, concat_axis=0, tiled=True)  11.9 us
    all_to_all x1, starting transfers between devices, copy_for_each(): lax.all_to_all(jnp.broadcast_to(shard[None], (count, *shard.shape)), axis...  11.3 us
    all_to_all x1, waiting for transfers between devices, summed_on_arrival(): lax.all_to_all(cut_along(shard, dim, count), axis, 0, 0, tiled=True)  8.83 us
    all_to_all x1, waiting for transfers between devices, copy_for_each(): lax.all_to_all(jnp.broadcast_to(shard[None], (count, *shard.shape)), axis...  7.34 us
  transfers between devices with their start and end apart: 5, of which 4 were waited for; matrix products, arithmetic and copies ran while one was open for 6% of the time, Pallas kernels for 0%

commit v1 on v0

v1 whole, which is shorter than its diff:
```python
import jax
import jax.numpy as jnp
from jax import lax
from jax.experimental import pallas as pl
from jax.experimental.pallas import tpu as pltpu
from jax.sharding import Mesh
from jax.sharding import PartitionSpec as P

RESIDUAL_SCALE = 8.0**0.25
NORM_EPSILON = 1e-05
LANES = 128
SLOTS = 2
BF16, F32 = jnp.bfloat16, jnp.float32
VMEM = pl.BlockSpec(memory_space=pltpu.VMEM)
SMEM = pl.BlockSpec(memory_space=pltpu.SMEM)


def kernel_call(body, out_shape, *operands, scalars=0, scratch=()):
    several = isinstance(out_shape, (list, tuple))
    return pl.pallas_call(
        body,
        out_shape=out_shape,
        in_specs=[SMEM] * scalars + [VMEM] * (len(operands) - scalars),
        out_specs=[VMEM] * len(out_shape) if several else VMEM,
        scratch_shapes=scratch,
    )(*operands)


def dot(a, b):
    return jnp.dot(a, b, preferred_element_type=F32)


def layer_norm(values, gain_vec, bias_vec):
    row_mean = jnp.mean(values, axis=-1, keepdims=True)
    spread = jnp.mean(jnp.square(values - row_mean), axis=-1, keepdims=True)
    return (values - row_mean) * lax.rsqrt(spread + NORM_EPSILON) * gain_vec + bias_vec


def softplus(x):
    u = jnp.exp(-jnp.abs(x))
    s = u / (2.0 + u)
    q = s * s
    series = 1.0 / 17.0
    for k in (15.0, 13.0, 11.0, 9.0, 7.0, 5.0, 3.0, 1.0):
        series = series * q + 1.0 / k
    return jnp.maximum(x, 0.0) + 2.0 * s * series


def expm1(z):
    series = 1.0 + z * (1.0 / 9.0)
    for k in (8.0, 7.0, 6.0, 5.0, 4.0, 3.0, 2.0):
        series = 1.0 + z * (1.0 / k) * series
    return jnp.where(jnp.abs(z) < 0.5, z * series, jnp.exp(z) - 1.0)


def shifted_rows(values, by, row, fill):
    if by < 8:
        return jnp.where(row >= by, pltpu.roll(values, by, 0), fill)
    head = jnp.full((by, values.shape[1]), fill, values.dtype)
    return jnp.concatenate([head, values[: values.shape[0] - by]], axis=0)


def chain_rows(decay, drive):
    row = lax.broadcasted_iota(jnp.int32, decay.shape, 0)
    by = 1
    while by < decay.shape[0]:
        drive = decay * shifted_rows(drive, by, row, 0.0) + drive
        decay = decay * shifted_rows(decay, by, row, 1.0)
        by *= 2
    return decay, drive


def local_kernel(rows, border, taps, small_maps, large_maps, decay_param, extra, decays, states, totals, padded, maps):
    length, half = rows.shape[1], rows.shape[2]
    tap_count = taps.shape[0]
    tap_weights = taps[...].astype(F32)
    rate = -8.0 * softplus(-decay_param[...])
    margin = border.shape[1]
    per_half = half // LANES
    for g, blocks in enumerate((small_maps, large_maps)):
        padded[0:margin] = border[g].astype(F32)
        padded[margin : margin + length] = rows[g].astype(F32)
        start = margin - (tap_count - 1)
        summed = tap_weights[0, g : g + 1] * padded[start : start + length]
        for k in range(1, tap_count):
            summed = summed + tap_weights[k, g : g + 1] * padded[start + k : start + k + length]
        conv_rows = summed.astype(BF16)
        maps[...] = jnp.zeros(maps.shape, BF16)
        head = blocks.shape[-1]
        for m in range(2):
            for h in range(blocks.shape[1]):
                maps[h * head : (h + 1) * head, m * half + h * head : m * half + (h + 1) * head] = blocks[m, h]
        gates = jax.nn.sigmoid(dot(conv_rows, maps[...]))
        log_decay = gates[:, :half] * rate[g : g + 1] + extra[g]
        drive = jnp.sqrt(-expm1(2.0 * log_decay)) * gates[:, half:] * conv_rows.astype(F32)
        decay = jnp.exp(log_decay)
        for c in range(per_half):
            at = slice(c * LANES, (c + 1) * LANES)
            run = g * per_half + c
            product, state = chain_rows(decay[:, at], drive[:, at])
            to = slice(run * LANES, (run + 1) * LANES)
            decays[:, to] = product
            states[:, to] = state
            for j in range(totals.shape[0]):
                totals[j, run : run + 1] = product[length - 1 :]
                totals[j, 2 * per_half + run : 2 * per_half + run + 1] = state[length - 1 :]


def joined(first, second):
    return first[0] * second[0], second[0] * first[1] + second[1]


def before_mine(spans, mine):
    half = spans.shape[1] // 2
    ahead = (jnp.ones((half, LANES), F32), jnp.zeros((half, LANES), F32))
    whole = ahead
    for j in range(spans.shape[0]):
        span = (spans[j, :half], spans[j, half:])
        whole = joined(whole, span)
        passed = j < mine
        ahead = tuple(jnp.where(passed, new, old) for new, old in zip(whole, ahead))
    return ahead, whole


def near_kernel(mine, spans, ahead, totals):
    half = spans.shape[1] // 2
    first, whole = before_mine(spans, mine[0])
    ahead[:half], ahead[half:] = first
    for j in range(totals.shape[0]):
        totals[j, :half], totals[j, half:] = whole


def project_kernel(mine, spans, ahead, decays, states, gate_rows, weight, out):
    half = spans.shape[1] // 2
    far, _ = before_mine(spans, mine[0])
    entering = joined(far, (ahead[:half], ahead[half:]))[1]
    width = gate_rows.shape[2]
    per_half = width // LANES
    acc = None
    for g in range(gate_rows.shape[0]):
        start = jnp.concatenate([entering[g * per_half + c : g * per_half + c + 1] for c in range(per_half)], axis=1)
        at = slice(g * width, (g + 1) * width)
        state = states[:, at] + decays[:, at] * start
        branch = (jax.nn.gelu(gate_rows[g].astype(F32), approximate=True) * state).astype(BF16)
        part = dot(branch, weight[g])
        acc = part if acc is None else acc + part
    out[...] = acc.astype(BF16).reshape(out.shape)


def route_kernel(ids, weights, select, merge):
    slot_count, rows = select.shape[0], ids.shape[1]
    slot = lax.broadcasted_iota(jnp.int32, (slot_count, rows), 0)
    names = jnp.zeros((slot_count, rows), F32)
    weight = jnp.zeros((slot_count, rows), F32)
    for k in range(ids.shape[0]):
        named = ids[k : k + 1] == slot // SLOTS
        names = jnp.where(named, 1.0, names)
        weight = jnp.where(named, weights[k : k + 1], weight)
    earlier = lax.broadcasted_iota(jnp.int32, (rows, rows), 0) < lax.broadcasted_iota(jnp.int32, (rows, rows), 1)
    rank = dot(names.astype(BF16), jnp.where(earlier, 1.0, 0.0).astype(BF16))
    taken = (names > 0.0) & (rank == (slot % SLOTS).astype(F32))
    select[...] = jnp.where(taken, 1.0, 0.0).astype(BF16)[:, : select.shape[1]]
    merge[...] = jnp.where(taken, weight, 0.0).T[: merge.shape[0]]


def mix_kernel(parts, stream, gain, bias, select, normed, outgoing):
    mixed = parts[0].astype(F32)
    for j in range(1, parts.shape[0]):
        mixed = mixed + parts[j].astype(F32)
    rows = layer_norm(RESIDUAL_SCALE * stream[...].astype(F32) + mixed, gain[...], bias[...]).astype(BF16)
    normed[...] = rows
    outgoing[...] = dot(select[...], rows).astype(BF16)


def shared_kernel(normed, gate_w, up_w, down_w, base):
    rows = normed[...]
    gated, lifted = dot(rows, gate_w[...]), dot(rows, up_w[...])
    hidden = (jax.nn.silu(gated) * lifted).astype(BF16)
    base[...] = RESIDUAL_SCALE * rows.astype(F32) + dot(hidden, down_w[...])


def expert_kernel(rows, g0, g1, g2, g3, u0, u1, u2, u3, d0, d1, d2, d3a, d3b, out):
    picked = rows[...]
    hidden = []
    for gate_w, up_w in ((g0, u0), (g1, u1), (g2, u2), (g3, u3)):
        pair = dot(picked, jnp.concatenate([gate_w[...], up_w[...]], axis=1))
        width = gate_w.shape[1]
        hidden.append((jax.nn.silu(pair[:, :width]) * pair[:, width:]).astype(BF16))
    down = jnp.concatenate([d3a[...], d3b[...]], axis=0)
    acc = dot(hidden[0], d0[...]) + dot(hidden[1], d1[...]) + dot(hidden[2], d2[...]) + dot(hidden[3], down)
    out[...] = acc.astype(BF16)


def merge_kernel(merge, returned, base, gain, bias, out):
    rest = merge[...]
    rows = returned[...]
    total = base[...]
    for _ in range(3):
        part = rest.astype(BF16)
        total = total + dot(part, rows)
        rest = rest - part.astype(F32)
    out[...] = layer_norm(total, gain[...], bias[...]).astype(BF16)


def turned(shard, by):
    count = lax.axis_size("tp")
    return lax.ppermute(shard, "tp", [(i, (i + by) % count) for i in range(count)])


def swapped(pieces, axis):
    return lax.all_to_all(pieces, axis, 0, 0, tiled=True)


def shards(
    stream,
    recurrence_input,
    output_gate_input,
    convolution_taps,
    first_group_gates,
    second_group_gates,
    channel_decay,
    position_log_extra,
    recurrence_output_weight,
    first_norm_gain,
    first_norm_bias,
    routed_expert_index,
    routed_expert_weight,
    routed_gate_weight,
    routed_up_weight,
    routed_down_weight,
    shared_gate_weight,
    shared_up_weight,
    shared_down_weight,
    second_norm_gain,
    second_norm_bias,
):
    length, groups, half = recurrence_input.shape
    width = stream.shape[1]
    tp_count, far_count, near_count = (lax.axis_size(a) for a in ("tp", "far", "near"))
    quarter = length // tp_count
    sp_axes = ("far", "near")
    expert_count = routed_gate_weight.shape[0] * far_count * near_count
    slot_count = expert_count * SLOTS
    channels = groups * half

    rows = jnp.transpose(recurrence_input, (1, 0, 2))
    margin = 8
    sp_count = far_count * near_count
    border = lax.ppermute(rows[:, length - margin :], sp_axes, [(i, i + 1) for i in range(sp_count - 1)])

    gate_w, up_w, down_w = routed_gate_weight[0], routed_up_weight[0], routed_down_weight[0]
    gate_left, up_right = turned(gate_w, 1), turned(up_w, -1)
    up_left, gate_right = turned(up_w, 1), turned(gate_w, -1)

    own_index = lax.axis_index("tp")
    own_ids = lax.dynamic_slice_in_dim(routed_expert_index.T, own_index * quarter, quarter, 1)
    own_weights = lax.dynamic_slice_in_dim(routed_expert_weight.T, own_index * quarter, quarter, 1)
    fill = ((0, 0), (0, LANES - quarter))
    select, merge = kernel_call(
        route_kernel,
        [jax.ShapeDtypeStruct((slot_count, quarter), BF16), jax.ShapeDtypeStruct((quarter, slot_count), F32)],
        jnp.pad(own_ids, fill, constant_values=-1),
        jnp.pad(own_weights, fill),
    )

    runs = channels // LANES
    span = jax.ShapeDtypeStruct((2 * runs, LANES), F32)
    decays, states, totals = kernel_call(
        local_kernel,
        [
            jax.ShapeDtypeStruct((length, channels), F32),
            jax.ShapeDtypeStruct((length, channels), F32),
            jax.ShapeDtypeStruct((near_count, 2 * runs, LANES), F32),
        ],
        rows,
        border,
        convolution_taps,
        first_group_gates,
        second_group_gates,
        channel_decay,
        jnp.transpose(position_log_extra, (1, 0, 2)),
        scratch=(pltpu.VMEM((margin + length, half), F32), pltpu.VMEM((half, 2 * half), BF16)),
    )
    near_spans = swapped(totals, "near")
    ahead, totals = kernel_call(
        near_kernel,
        [span, jax.ShapeDtypeStruct((far_count, 2 * runs, LANES), F32)],
        lax.axis_index("near").reshape(1),
        near_spans,
        scalars=1,
    )
    far_spans = swapped(totals, "far")
    parts = kernel_call(
        project_kernel,
        jax.ShapeDtypeStruct((tp_count, quarter, width), BF16),
        lax.axis_index("far").reshape(1),
        far_spans,
        ahead,
        decays,
        states,
        jnp.transpose(output_gate_input, (1, 0, 2)),
        recurrence_output_weight,
        scalars=1,
    )
    parts = swapped(parts, "tp")

    down_left, down_right = turned(down_w, 1), turned(down_w, -1)
    gate_far, up_far = turned(gate_left, 1), turned(up_right, -1)

    normed, outgoing = kernel_call(
        mix_kernel,
        [jax.ShapeDtypeStruct((quarter, width), BF16), jax.ShapeDtypeStruct((slot_count, width), BF16)],
        parts,
        stream,
        first_norm_gain.reshape(1, width),
        first_norm_bias.reshape(1, width),
        select,
    )
    arrived = swapped(outgoing.reshape(expert_count, SLOTS, width), sp_axes)

    cut = down_w.shape[0] // 2
    down_far = turned(down_left[:cut], 1), turned(down_right[cut:], -1)

    base = kernel_call(
        shared_kernel,
        jax.ShapeDtypeStruct((quarter, width), F32),
        normed,
        shared_gate_weight,
        shared_up_weight,
        shared_down_weight,
    )
    leaving = kernel_call(
        expert_kernel,
        jax.ShapeDtypeStruct((slot_count, width), BF16),
        arrived.reshape(slot_count, width),
        *(gate_w, gate_left, gate_right, gate_far),
        *(up_w, up_left, up_right, up_far),
        *(down_w, down_left, down_right, *down_far),
    )
    returned = swapped(leaving.reshape(expert_count, SLOTS, width), sp_axes)
    return kernel_call(
        merge_kernel,
        jax.ShapeDtypeStruct((quarter, width), BF16),
        merge,
        returned.reshape(slot_count, width),
        base,
        second_norm_gain.reshape(1, width),
        second_norm_bias.reshape(1, width),
    )


def solution(mesh):
    near = 8
    shape = (mesh.shape["sp"] // near, near, mesh.shape["tp"])
    fine = Mesh(mesh.devices.reshape(shape), ("far", "near", "tp"))
    sp = ("far", "near")
    in_specs = (
        P((*sp, "tp"), None),
        P(sp, None, "tp"),
        P(sp, None, "tp"),
        P(None, None, "tp"),
        P(None, "tp", None, None),
        P(None, "tp", None, None),
        P(None, "tp"),
        P(sp, None, "tp"),
        P(None, "tp", None),
        P(),
        P(),
        P(sp, None),
        P(sp, None),
        P(sp, None, "tp"),
        P(sp, None, "tp"),
        P(sp, "tp", None),
        P(),
        P(),
        P(),
        P(),
        P(),
    )

    return jax.shard_map(shards, mesh=fine, in_specs=in_specs, out_specs=P((*sp, "tp"), None), check_vma=False)
```

time: 207 us -> 152 us (0.73)
  blocking collectives: 52.1 us -> 0 us
  Pallas kernels: 0 us -> 23.8 us
  starting transfers between devices: 32 us -> 53.7 us
  matrix products: 15.4 us -> 0 us
  between operations: 14.3 us -> 0.12 us
  other arithmetic: 13.3 us -> 0 us
  local copies, waits for them, and re-layouts: 19.8 us -> 16 us
    all_to_all x2 -> x0, blocking collectives: 52.1 us -> none  [the longest x1 28.9 us: summed_on_arrival(): lax.all_to_all(cut_along(shard, dim, count), axis, 0, 0, tiled=True)]
    ppermute x1 -> x11, waiting for transfers between devices: 0.01 us -> 33.9 us  [the longest x10 33.9 us: turned(): lax.ppermute(shard, 'tp', [(i, (i + by) % count) for i in range(count)])]
    all_gather x1 -> x0, waiting for transfers between devices: 27.8 us -> none  [shards(): fanned = lax.all_gather(arrived[None], 'tp', axis=0, tiled=True)]
    pallas_call x0 -> x8, Pallas kernels: none -> 23.8 us  [kernel_call(): pl.pallas_call(body, out_shape=out_shape, in_specs=[SMEM] * scalars + [VM...]
    dot_general x7 -> x0, matrix products: 15.4 us -> none  [the longest x1 5.22 us: expert_terms(): jnp.einsum(down_form, hidden, down_w, preferred_element_type=jnp.float32)]
    all_to_all x3 -> x5, starting transfers between devices: 27.5 us -> 41 us  [swapped(): return lax.all_to_all(pieces, axis, 0, 0, tiled=True)]
    ppermute x1 -> x11, starting transfers between devices: 4.5 us -> 12.7 us  [the longest x10 8.22 us: turned(): lax.ppermute(shard, 'tp', [(i, (i + by) % count) for i in range(count)])]
    all_to_all x3 -> x5, waiting for transfers between devices: 31 us -> 24.1 us  [swapped(): return lax.all_to_all(pieces, axis, 0, 0, tiled=True)]
  transfers between devices with their start and end apart: 5 -> 16, of which waited for: 4 -> 9; matrix products, arithmetic and copies ran while one was open for 6% -> 5% of each run, Pallas kernels for 0% -> 6%
where the time goes in v1:
time: 152 us
  waiting for transfers between devices  58 us (38%)
  starting transfers between devices  53.7 us (35%)
  Pallas kernels  23.8 us (16%)
  local copies, waits for them, and re-layouts  16 us (11%)
    all_to_all x5, starting transfers between devices, swapped(): return lax.all_to_all(pieces, axis, 0, 0, tiled=True)  41 us
    ppermute x10, waiting for transfers between devices, turned(): lax.ppermute(shard, 'tp', [(i, (i + by) % count) for i in range(count)])  33.9 us
    all_to_all x5, waiting for transfers between devices, swapped(): return lax.all_to_all(pieces, axis, 0, 0, tiled=True)  24.1 us
    pallas_call x8, Pallas kernels, kernel_call(): pl.pallas_call(body, out_shape=out_shape, in_specs=[SMEM] * scalars + [VM...  23.8 us
    unnamed x33, local copies, waits for them, and re-layouts  8.26 us
    ppermute x10, starting transfers between devices, turned(): lax.ppermute(shard, 'tp', [(i, (i + by) % count) for i in range(count)])  8.22 us
    ppermute x1, starting transfers between devices, shards(): lax.ppermute(rows[:, length - margin:], sp_axes, [(i, i + 1) for i in ran...  4.5 us
  transfers between devices with their start and end apart: 16, of which 9 were waited for; matrix products, arithmetic and copies ran while one was open for 5% of the time, Pallas kernels for 6%

profile of v1, /device:TPU:1, one launch (start us, length us, event | category | flops | bytes accessed | tf_op | source)
XLA Modules:
  0.0 151.7 jit_solution(222024489136146834)
XLA Ops:
  0.0 0.9 copy.30
  0.9 0.0 copy-start.4
  1.0 4.5 %collective-permute-start = (bf16[2,8,256]{2,1,0:T(8,128)(2,1)S(1)}, bf16[2,8,256]{2,1,0:T(8,128)(2,1)S(1)}, u32[]{:S(2)}, u32[]{:S(2)}) collective-permute-start(bf16[2,8,256]{2,1,0:T(8,128)(2,1)S(1)} %slice.12), channel_id=1, source_target_pairs={{0,4},{4,8},{8,12},{12,16},{16,20},{20,24},{24,28},{28,32},{32,36}... | collective-permute-start | bytes 24584 | tf_op jit(solution)/shard_map/ppermute | solution.py:249
  5.5 1.7 %copy.28 = f32[128,2,256]{2,0,1:T(8,128)} copy(f32[128,2,256]{2,1,0:T(2,128)} %param.28) | data formatting | bytes 524288 | tf_op args[7]
  7.1 0.0 collective-permute-done.border
  7.1 0.6 copy-done.13
  7.7 3.1 %shard_map.200 = (f32[128,512]{1,0:T(8,128)}, f32[128,512]{1,0:T(8,128)}, f32[8,8,128]{2,1,0:T(8,128)}) custom-call(bf16[2,128,256]{2,1,0:T(8,128)(2,1)} %bitcast.24, bf16[2,8,256]{2,1,0:T(8,128)(2,1)} %copy-done.13, bf16[4,2,256]{2,1,0:T(2,128)(2,1)} %taps.1, bf16[2,4,64,64]{3,2,1,0:T(8,128)(2,1)} %small_maps.1, bf16[2,2,128,128]{3,2,1,0:T(8,128)(2,1)} %large_maps.1, ...), custom_call_target="tpu_custom_call" | custom-call | tf_op jit(solution)/shard_map/pallas_call | solution.py:20
  10.8 4.6 %all-to-all-start = ((f32[8,8,128]{2,1,0:T(8,128)}), f32[8,8,128]{2,1,0:T(8,128)S(1)}, u32[]{:S(2)}, u32[]{:S(2)}) async-start(f32[8,8,128]{2,1,0:T(8,128)} %get-tuple-element.15), calls=%async_computation | async-start | bytes 65536 | tf_op jit(solution)/shard_map/all_to_all | solution.py:211
  15.4 4.7 %all-to-all-done.spans = f32[8,8,128]{2,1,0:T(8,128)S(1)} async-done(((f32[8,8,128]{2,1,0:T(8,128)}), f32[8,8,128]{2,1,0:T(8,128)S(1)}, u32[]{:S(2)}, u32[]{:S(2)}) %all-to-all-start) | async-done | bytes 32800 | tf_op jit(solution)/shard_map/all_to_all | solution.py:211
  20.1 0.6 copy-done.12
  20.7 1.4 shard_map.201
  22.1 10.5 %all-to-all-start.1 = ((f32[8,8,128]{2,1,0:T(8,128)}), f32[8,8,128]{2,1,0:T(8,128)S(1)}, u32[]{:S(2)}, u32[]{:S(2)}) async-start(f32[8,8,128]{2,1,0:T(8,128)} %get-tuple-element.16), calls=%async_computation.1 | async-start | bytes 65536 | tf_op jit(solution)/shard_map/all_to_all | solution.py:211
  32.6 1.6 %copy.29 = bf16[128,2,256]{2,0,1:T(8,128)(2,1)} copy(bf16[128,2,256]{2,1,0:T(2,128)(2,1)} %param.23) | data formatting | bytes 262144 | tf_op args[2]
  34.2 5.3 %all-to-all-done.1.spans = f32[8,8,128]{2,1,0:T(8,128)S(1)} async-done(((f32[8,8,128]{2,1,0:T(8,128)}), f32[8,8,128]{2,1,0:T(8,128)S(1)}, u32[]{:S(2)}, u32[]{:S(2)}) %all-to-all-start.1) | async-done | bytes 32800 | tf_op jit(solution)/shard_map/all_to_all | solution.py:211
  39.5 0.6 copy-done.11
  40.1 3.2 %shard_map.202 = bf16[4,32,2048]{2,1,0:T(8,128)(2,1)} custom-call(s32[1]{0:T(128)} %bitcast.2.mine, f32[8,8,128]{2,1,0:T(8,128)} %copy-done.11, f32[8,128]{1,0:T(8,128)} %get-tuple-element.17.ahead, f32[128,512]{1,0:T(8,128)} %get-tuple-element.18.decays, f32[128,512]{1,0:T(8,128)} %get-tuple-element.19.states, bf16[2,128,256]{2,1,0:T(8,128)(2,1)} %bitcast.34, ...), custom_call_target="tpu_custom_call" | custom-call | tf_op jit(solution)/shard_map/pallas_call | solution.py:20
  43.3 4.2 %all-to-all-start.2 = ((bf16[4,32,2048]{2,1,0:T(8,128)(2,1)}), bf16[4,32,2048]{2,1,0:T(8,128)(2,1)S(1)}, u32[]{:S(2)}, u32[]{:S(2)}) async-start(bf16[4,32,2048]{2,1,0:T(8,128)(2,1)} %shard_map.202), calls=%async_computation.2 | async-start | bytes 1048576 | tf_op jit(solution)/shard_map/all_to_all | solution.py:211
  47.5 0.0 copy-done.5
  47.5 1.5 collective-permute-start.1
  48.9 1.3 collective-permute-start.5
  50.2 0.2 collective-permute-start.7
  50.4 0.0 copy-done
  50.4 0.1 dynamic-slice_bitcast_fusion.1
  50.5 0.0 copy-done.14
  50.5 0.1 dynamic-slice_bitcast_fusion
  50.5 0.6 pad.8.ids
  51.1 0.6 pad.9.weights
  51.7 1.5 shard_map.199
  53.2 1.3 all-to-all-done.2.parts
  54.5 0.8 copy-done.1
  55.3 2.5 %shard_map.203 = (bf16[32,2048]{1,0:T(8,128)(2,1)}, bf16[128,2048]{1,0:T(8,128)(2,1)}) custom-call(bf16[4,32,2048]{2,1,0:T(8,128)(2,1)} %copy-done.1, bf16[32,2048]{1,0:T(8,128)(2,1)} %stream.1, f32[1,2048]{1,0:T(1,128)} %bitcast.35, f32[1,2048]{1,0:T(1,128)} %bitcast.36, bf16[128,32]{1,0:T(8,128)(2,1)} %get-tuple-element.20.select), custom_call_target="tpu_custom_call" | custom-call | tf_op jit(solution)/shard_map/pallas_call | solution.py:20
  57.8 2.2 %reshape.34 = bf16[64,2,2048]{2,1,0:T(2,128)(2,1)} reshape(bf16[128,2048]{1,0:T(8,128)(2,1)} %get-tuple-element.21) | data formatting | bytes 1048576 | tf_op jit(solution)/shard_map/reshape | solution.py:319
  60.0 10.4 %all-to-all-start.3 = ((bf16[64,2,2048]{2,1,0:T(2,128)(2,1)}), bf16[64,2,2048]{2,1,0:T(2,128)(2,1)S(1)}, u32[]{:S(2)}, u32[]{:S(2)}) async-start(bf16[64,2,2048]{2,1,0:T(2,128)(2,1)} %reshape.34), calls=%async_computation.3 | async-start | bytes 1048576 | tf_op jit(solution)/shard_map/all_to_all | solution.py:211
  70.3 1.0 collective-permute-start.8
  71.3 0.1 collective-permute-start.2
  71.4 0.0 collective-permute-done.1.g1
  71.4 1.4 collective-permute-start.4
  72.8 0.0 collective-permute-done.5.u2
  72.8 0.6 collective-permute-start.3
  73.3 4.5 %collective-permute-done.7.d1 = bf16[128,2048]{1,0:T(8,128)(2,1)S(1)} collective-permute-done((bf16[128,2048]{1,0:T(8,128)(2,1)S(1)}, bf16[128,2048]{1,0:T(8,128)(2,1)S(1)}, u32[]{:S(2)}, u32[]{:S(2)}) %collective-permute-start.7) | collective-permute-done | bytes 524320 | tf_op jit(solution)/shard_map/ppermute | solution.py:207
  77.9 0.0 collective-permute-start.6
  77.9 5.5 %collective-permute-done.8.d2 = bf16[128,2048]{1,0:T(8,128)(2,1)S(1)} collective-permute-done((bf16[128,2048]{1,0:T(8,128)(2,1)S(1)}, bf16[128,2048]{1,0:T(8,128)(2,1)S(1)}, u32[]{:S(2)}, u32[]{:S(2)}) %collective-permute-start.8) | collective-permute-done | bytes 524320 | tf_op jit(solution)/shard_map/ppermute | solution.py:207
  83.4 0.3 collective-permute-start.9
  83.7 10.9 %collective-permute-done.2.g2 = bf16[2048,128]{1,0:T(8,128)(2,1)S(1)} collective-permute-done((bf16[2048,128]{1,0:T(8,128)(2,1)S(1)}, bf16[2048,128]{1,0:T(8,128)(2,1)S(1)}, u32[]{:S(2)}, u32[]{:S(2)}) %collective-permute-start.2) | collective-permute-done | bytes 524320 | tf_op jit(solution)/shard_map/ppermute | solution.py:207
  94.7 0.8 copy-done.8
  95.4 2.0 %collective-permute-start.10 = (bf16[64,2048]{1,0:T(8,128)(2,1)S(1)}, bf16[64,2048]{1,0:T(8,128)(2,1)S(1)}, u32[]{:S(2)}, u32[]{:S(2)}) collective-permute-start(bf16[64,2048]{1,0:T(8,128)(2,1)S(1)} %slice.14), channel_id=1, source_target_pairs={{0,3},{1,0},{2,1},{3,2},{4,7},{5,4},{6,5},{7,6},{8,11},{9,8},{10,9... | collective-permute-start | bytes 786440 | tf_op jit(solution)/shard_map/ppermute | solution.py:207
  97.4 0.0 all-to-all-done.3
  97.4 1.0 reshape.35.rows
  98.5 0.0 collective-permute-done.4.u1
  98.5 7.5 %collective-permute-done.9.d3a = bf16[64,2048]{1,0:T(8,128)(2,1)S(1)} collective-permute-done((bf16[64,2048]{1,0:T(8,128)(2,1)S(1)}, bf16[64,2048]{1,0:T(8,128)(2,1)S(1)}, u32[]{:S(2)}, u32[]{:S(2)}) %collective-permute-start.9) | collective-permute-done | bytes 262176 | tf_op jit(solution)/shard_map/ppermute | solution.py:207
  106.0 5.4 %collective-permute-done.10.d3b = bf16[64,2048]{1,0:T(8,128)(2,1)S(1)} collective-permute-done((bf16[64,2048]{1,0:T(8,128)(2,1)S(1)}, bf16[64,2048]{1,0:T(8,128)(2,1)S(1)}, u32[]{:S(2)}, u32[]{:S(2)}) %collective-permute-start.10) | collective-permute-done | bytes 262176 | tf_op jit(solution)/shard_map/ppermute | solution.py:207
  111.4 0.0 collective-permute-done.3.g3
  111.4 0.0 collective-permute-done.6.u3
  111.4 0.0 copy-done.2
  111.4 0.0 copy-done.3
  111.4 0.0 copy-done.9
  111.4 0.7 copy-done.10
  112.1 5.0 %shard_map.204 = bf16[128,2048]{1,0:T(8,128)(2,1)} custom-call(bf16[128,2048]{1,0:T(8,128)(2,1)} %reshape.35.rows, bf16[2048,128]{1,0:T(8,128)(2,1)} %bitcast.25, bf16[2048,128]{1,0:T(8,128)(2,1)} %collective-permute-done.1.g1, bf16[2048,128]{1,0:T(8,128)(2,1)} %copy-done.8, bf16[2048,128]{1,0:T(8,128)(2,1)} %collective-permute-done.3.g3, ...), custom_call_target="tpu_custom_call" | custom-call | tf_op jit(solution)/shard_map/pallas_call | solution.py:20
  117.1 2.2 %reshape.36 = bf16[64,2,2048]{2,1,0:T(2,128)(2,1)} reshape(bf16[128,2048]{1,0:T(8,128)(2,1)} %shard_map.204) | data formatting | bytes 1048576 | tf_op jit(solution)/shard_map/reshape | solution.py:340
  119.2 11.4 %all-to-all-start.4 = ((bf16[64,2,2048]{2,1,0:T(2,128)(2,1)}), bf16[64,2,2048]{2,1,0:T(2,128)(2,1)S(1)}, u32[]{:S(2)}, u32[]{:S(2)}) async-start(bf16[64,2,2048]{2,1,0:T(2,128)(2,1)} %reshape.36), calls=%async_computation.4 | async-start | bytes 1048576 | tf_op jit(solution)/shard_map/all_to_all | solution.py:211
  130.7 4.9 %shard_map.205.base = f32[32,2048]{1,0:T(8,128)} custom-call(bf16[32,2048]{1,0:T(8,128)(2,1)} %get-tuple-element.22.normed, bf16[2048,512]{1,0:T(8,128)(2,1)} %gate_w.1, bf16[2048,512]{1,0:T(8,128)(2,1)} %up_w.1, bf16[512,2048]{1,0:T(8,128)(2,1)} %down_w.1), custom_call_target="tpu_custom_call" | custom-call | tf_op jit(solution)/shard_map/pallas_call | solution.py:20
  135.5 12.8 %all-to-all-done.4 = bf16[64,2,2048]{2,1,0:T(2,128)(2,1)S(1)} async-done(((bf16[64,2,2048]{2,1,0:T(2,128)(2,1)}), bf16[64,2,2048]{2,1,0:T(2,128)(2,1)S(1)}, u32[]{:S(2)}, u32[]{:S(2)}) %all-to-all-start.4) | async-done | bytes 524320 | tf_op jit(solution)/shard_map/all_to_all | solution.py:211
  148.4 1.0 reshape.37.returned
  149.4 2.4 %shard_map.206 = bf16[32,2048]{1,0:T(8,128)(2,1)} custom-call(f32[32,128]{1,0:T(8,128)} %get-tuple-element.14.merge, bf16[128,2048]{1,0:T(8,128)(2,1)} %reshape.37.returned, f32[32,2048]{1,0:T(8,128)} %shard_map.205.base, f32[1,2048]{1,0:T(1,128)} %bitcast.37, f32[1,2048]{1,0:T(1,128)} %bitcast.38), custom_call_target="tpu_custom_call" | custom-call | tf_op jit(solution)/shard_map/pallas_call | solution.py:20
  (20 shorter events, 0.1 us)
Async XLA Ops:
  0.0 50.4 %copy-start = (s32[128,4]{0,1:T(4,128)S(1)}, s32[128,4]{0,1:T(4,128)}, u32[]{:S(2)}) copy-start(s32[128,4]{0,1:T(4,128)} %param.32) | copy-start | bytes 6148
  0.9 6.2 %copy-start.4 = (bf16[128,2,256]{2,0,1:T(8,128)(2,1)}, bf16[128,2,256]{2,0,1:T(8,128)(2,1)S(1)}, u32[]{:S(2)}) copy-start(bf16[128,2,256]{2,0,1:T(8,128)(2,1)S(1)} %copy.30) | copy-start | bytes 393220
  1.0 6.2 %collective-permute-start = (bf16[2,8,256]{2,1,0:T(8,128)(2,1)S(1)}, bf16[2,8,256]{2,1,0:T(8,128)(2,1)S(1)}, u32[]{:S(2)}, u32[]{:S(2)}) collective-permute-start(bf16[2,8,256]{2,1,0:T(8,128)(2,1)S(1)} %slice.12), channel_id=1, source_target_pairs={{0,4},{4,8},{8,12},{12,16},{16,20},{20,24},{24,28},{28,32},{32,36}... | collective-permute-start | bytes 24584 | tf_op jit(solution)/shard_map/ppermute | solution.py:249
  7.1 0.6 copy-start.13
  10.8 9.3 %all-to-all-start = ((f32[8,8,128]{2,1,0:T(8,128)}), f32[8,8,128]{2,1,0:T(8,128)S(1)}, u32[]{:S(2)}, u32[]{:S(2)}) async-start(f32[8,8,128]{2,1,0:T(8,128)} %get-tuple-element.15), calls=%async_computation | async-start | bytes 65536 | tf_op jit(solution)/shard_map/all_to_all | solution.py:211
  20.1 0.6 copy-start.12
  22.1 17.3 %all-to-all-start.1 = ((f32[8,8,128]{2,1,0:T(8,128)}), f32[8,8,128]{2,1,0:T(8,128)S(1)}, u32[]{:S(2)}, u32[]{:S(2)}) async-start(f32[8,8,128]{2,1,0:T(8,128)} %get-tuple-element.16), calls=%async_computation.1 | async-start | bytes 65536 | tf_op jit(solution)/shard_map/all_to_all | solution.py:211
  39.5 0.6 copy-start.11
  40.1 7.4 %copy-start.5 = (bf16[1,2048,128]{2,1,0:T(8,128)(2,1)S(1)}, bf16[1,2048,128]{2,1,0:T(8,128)(2,1)}, u32[]{:S(2)}) copy-start(bf16[1,2048,128]{2,1,0:T(8,128)(2,1)} %param.34) | copy-start | bytes 1572868
  40.1 8.9 %copy-start.6 = (bf16[1,2048,128]{2,1,0:T(8,128)(2,1)S(1)}, bf16[1,2048,128]{2,1,0:T(8,128)(2,1)}, u32[]{:S(2)}) copy-start(bf16[1,2048,128]{2,1,0:T(8,128)(2,1)} %param.35) | copy-start | bytes 1572868
  40.1 10.2 %copy-start.7 = (bf16[1,128,2048]{2,1,0:T(8,128)(2,1)S(1)}, bf16[1,128,2048]{2,1,0:T(8,128)(2,1)}, u32[]{:S(2)}) copy-start(bf16[1,128,2048]{2,1,0:T(8,128)(2,1)} %param.36) | copy-start | bytes 1572868
  40.1 10.4 %copy-start.14 = (f32[128,4]{0,1:T(4,128)S(1)}, f32[128,4]{0,1:T(4,128)}, u32[]{:S(2)}) copy-start(f32[128,4]{0,1:T(4,128)} %param.33) | copy-start | bytes 6148
  43.3 11.2 %all-to-all-start.2 = ((bf16[4,32,2048]{2,1,0:T(8,128)(2,1)}), bf16[4,32,2048]{2,1,0:T(8,128)(2,1)S(1)}, u32[]{:S(2)}, u32[]{:S(2)}) async-start(bf16[4,32,2048]{2,1,0:T(8,128)(2,1)} %shard_map.202), calls=%async_computation.2 | async-start | bytes 1048576 | tf_op jit(solution)/shard_map/all_to_all | solution.py:211
  47.5 23.9 %collective-permute-start.1 = (bf16[2048,128]{1,0:T(8,128)(2,1)S(1)}, bf16[2048,128]{1,0:T(8,128)(2,1)}, u32[]{:S(2)}, u32[]{:S(2)}) collective-permute-start(bf16[2048,128]{1,0:T(8,128)(2,1)S(1)} %bitcast.26), channel_id=1, source_target_pairs={{0,1},{1,2},{2,3},{3,0},{4,5},{5,6},{6,7},{7,4},{8,9},{9,10},{10,1... | collective-permute-start | bytes 1572872 | tf_op jit(solution)/shard_map/ppermute | solution.py:207
  48.9 23.8 %collective-permute-start.5 = (bf16[2048,128]{1,0:T(8,128)(2,1)S(1)}, bf16[2048,128]{1,0:T(8,128)(2,1)}, u32[]{:S(2)}, u32[]{:S(2)}) collective-permute-start(bf16[2048,128]{1,0:T(8,128)(2,1)S(1)} %bitcast.29), channel_id=1, source_target_pairs={{0,3},{1,0},{2,1},{3,2},{4,7},{5,4},{6,5},{7,6},{8,11},{9,8},{10,9... | collective-permute-start | bytes 1572872 | tf_op jit(solution)/shard_map/ppermute | solution.py:207
  50.2 27.6 %collective-permute-start.7 = (bf16[128,2048]{1,0:T(8,128)(2,1)S(1)}, bf16[128,2048]{1,0:T(8,128)(2,1)S(1)}, u32[]{:S(2)}, u32[]{:S(2)}) collective-permute-start(bf16[128,2048]{1,0:T(8,128)(2,1)S(1)} %bitcast.32), channel_id=1, source_target_pairs={{0,1},{1,2},{2,3},{3,0},{4,5},{5,6},{6,7},{7,4},{8,9},{9,10},{10,1... | collective-permute-start | bytes 1572872 | tf_op jit(solution)/shard_map/ppermute | solution.py:207
  54.5 0.8 copy-start.1
  60.0 37.5 %all-to-all-start.3 = ((bf16[64,2,2048]{2,1,0:T(2,128)(2,1)}), bf16[64,2,2048]{2,1,0:T(2,128)(2,1)S(1)}, u32[]{:S(2)}, u32[]{:S(2)}) async-start(bf16[64,2,2048]{2,1,0:T(2,128)(2,1)} %reshape.34), calls=%async_computation.3 | async-start | bytes 1048576 | tf_op jit(solution)/shard_map/all_to_all | solution.py:211
  70.3 13.1 %collective-permute-start.8 = (bf16[128,2048]{1,0:T(8,128)(2,1)S(1)}, bf16[128,2048]{1,0:T(8,128)(2,1)S(1)}, u32[]{:S(2)}, u32[]{:S(2)}) collective-permute-start(bf16[128,2048]{1,0:T(8,128)(2,1)S(1)} %bitcast.33), channel_id=1, source_target_pairs={{0,3},{1,0},{2,1},{3,2},{4,7},{5,4},{6,5},{7,6},{8,11},{9,8},{10,9... | collective-permute-start | bytes 1572872 | tf_op jit(solution)/shard_map/ppermute | solution.py:207
  71.3 23.4 %collective-permute-start.2 = (bf16[2048,128]{1,0:T(8,128)(2,1)S(1)}, bf16[2048,128]{1,0:T(8,128)(2,1)S(1)}, u32[]{:S(2)}, u32[]{:S(2)}) collective-permute-start(bf16[2048,128]{1,0:T(8,128)(2,1)S(1)} %bitcast.27), channel_id=1, source_target_pairs={{0,3},{1,0},{2,1},{3,2},{4,7},{5,4},{6,5},{7,6},{8,11},{9,8},{10,9... | collective-permute-start | bytes 1572872 | tf_op jit(solution)/shard_map/ppermute | solution.py:207
  71.4 27.1 %collective-permute-start.4 = (bf16[2048,128]{1,0:T(8,128)(2,1)S(1)}, bf16[2048,128]{1,0:T(8,128)(2,1)}, u32[]{:S(2)}, u32[]{:S(2)}) collective-permute-start(bf16[2048,128]{1,0:T(8,128)(2,1)S(1)} %bitcast.30), channel_id=1, source_target_pairs={{0,1},{1,2},{2,3},{3,0},{4,5},{5,6},{6,7},{7,4},{8,9},{9,10},{10,1... | collective-permute-start | bytes 1572872 | tf_op jit(solution)/shard_map/ppermute | solution.py:207
  72.8 38.6 %collective-permute-start.3 = (bf16[2048,128]{1,0:T(8,128)(2,1)}, bf16[2048,128]{1,0:T(8,128)(2,1)}, u32[]{:S(2)}, u32[]{:S(2)}) collective-permute-start(bf16[2048,128]{1,0:T(8,128)(2,1)} %collective-permute-done.1.g1), channel_id=1, source_target_pairs={{0,1},{1,2},{2,3},{3,0},{4,5},{5,6},{6,7},{7,4},{8,9},{9,10},{10,1... | collective-permute-start | bytes 1572872 | tf_op jit(solution)/shard_map/ppermute | solution.py:207
  77.9 33.5 %copy-start.2 = (bf16[128,2048]{1,0:T(8,128)(2,1)}, bf16[128,2048]{1,0:T(8,128)(2,1)S(1)}, u32[]{:S(2)}) copy-start(bf16[128,2048]{1,0:T(8,128)(2,1)S(1)} %collective-permute-done.7.d1) | copy-start | bytes 1572868
  77.9 33.5 %collective-permute-start.6 = (bf16[2048,128]{1,0:T(8,128)(2,1)}, bf16[2048,128]{1,0:T(8,128)(2,1)}, u32[]{:S(2)}, u32[]{:S(2)}) collective-permute-start(bf16[2048,128]{1,0:T(8,128)(2,1)} %collective-permute-done.5.u2), channel_id=1, source_target_pairs={{0,3},{1,0},{2,1},{3,2},{4,7},{5,4},{6,5},{7,6},{8,11},{9,8},{10,9... | collective-permute-start | bytes 1572872 | tf_op jit(solution)/shard_map/ppermute | solution.py:207
  83.4 28.0 %copy-start.3 = (bf16[128,2048]{1,0:T(8,128)(2,1)}, bf16[128,2048]{1,0:T(8,128)(2,1)S(1)}, u32[]{:S(2)}) copy-start(bf16[128,2048]{1,0:T(8,128)(2,1)S(1)} %collective-permute-done.8.d2) | copy-start | bytes 1572868
  83.4 22.5 %collective-permute-start.9 = (bf16[64,2048]{1,0:T(8,128)(2,1)S(1)}, bf16[64,2048]{1,0:T(8,128)(2,1)S(1)}, u32[]{:S(2)}, u32[]{:S(2)}) collective-permute-start(bf16[64,2048]{1,0:T(8,128)(2,1)S(1)} %slice.13), channel_id=1, source_target_pairs={{0,1},{1,2},{2,3},{3,0},{4,5},{5,6},{6,7},{7,4},{8,9},{9,10},{10,1... | collective-permute-start | bytes 786440 | tf_op jit(solution)/shard_map/ppermute | solution.py:207
  94.7 0.8 copy-start.8
  95.4 16.0 %collective-permute-start.10 = (bf16[64,2048]{1,0:T(8,128)(2,1)S(1)}, bf16[64,2048]{1,0:T(8,128)(2,1)S(1)}, u32[]{:S(2)}, u32[]{:S(2)}) collective-permute-start(bf16[64,2048]{1,0:T(8,128)(2,1)S(1)} %slice.14), channel_id=1, source_target_pairs={{0,3},{1,0},{2,1},{3,2},{4,7},{5,4},{6,5},{7,6},{8,11},{9,8},{10,9... | collective-permute-start | bytes 786440 | tf_op jit(solution)/shard_map/ppermute | solution.py:207
  106.0 5.5 %copy-start.9 = (bf16[64,2048]{1,0:T(8,128)(2,1)}, bf16[64,2048]{1,0:T(8,128)(2,1)S(1)}, u32[]{:S(2)}) copy-start(bf16[64,2048]{1,0:T(8,128)(2,1)S(1)} %collective-permute-done.9.d3a) | copy-start | bytes 786436
  111.4 0.7 copy-start.10
  119.2 29.1 %all-to-all-start.4 = ((bf16[64,2,2048]{2,1,0:T(2,128)(2,1)}), bf16[64,2,2048]{2,1,0:T(2,128)(2,1)S(1)}, u32[]{:S(2)}, u32[]{:S(2)}) async-start(bf16[64,2,2048]{2,1,0:T(2,128)(2,1)} %reshape.36), calls=%async_computation.4 | async-start | bytes 1048576 | tf_op jit(solution)/shard_map/all_to_all | solution.py:211

commit v2 on v1

v2 whole, which is shorter than its diff:
```python
import jax
import jax.numpy as jnp
from jax import lax
from jax.experimental import pallas as pl
from jax.experimental.pallas import tpu as pltpu
from jax.sharding import PartitionSpec as P

RESIDUAL_SCALE = 8.0**0.25
NORM_EPSILON = 1e-05
LANES = 128
SLOTS = 2
BF16, F32 = jnp.bfloat16, jnp.float32
VMEM = pl.BlockSpec(memory_space=pltpu.VMEM)
SMEM = pl.BlockSpec(memory_space=pltpu.SMEM)
ANY = pl.BlockSpec(memory_space=pl.ANY)


def kernel_call(body, out_shape, *operands, scratch=(), limit=16):
    several = isinstance(out_shape, (list, tuple))
    specs, arrays = [], []
    for operand in operands:
        array, place = operand if isinstance(operand, tuple) else (operand, None)
        specs.append({"smem": SMEM, "hbm": ANY}.get(place, VMEM))
        if place != "smem":
            array = pltpu.with_memory_space_constraint(array, pltpu.VMEM if place == "vmem" else pltpu.HBM)
        arrays.append(array)
    return pl.pallas_call(
        body,
        out_shape=out_shape,
        in_specs=specs,
        out_specs=[VMEM] * len(out_shape) if several else VMEM,
        scratch_shapes=scratch,
        compiler_params=pltpu.CompilerParams(vmem_limit_bytes=limit << 20),
    )(*arrays)


def fetched(pairs, sems):
    copies = [pltpu.make_async_copy(source, target, sems.at[k]) for k, (source, target) in enumerate(pairs)]
    for copy in copies:
        copy.start()
    return copies


def dot(a, b):
    return jnp.dot(a, b, preferred_element_type=F32)


def layer_norm(values, gain_vec, bias_vec):
    row_mean = jnp.mean(values, axis=-1, keepdims=True)
    spread = jnp.mean(jnp.square(values - row_mean), axis=-1, keepdims=True)
    return (values - row_mean) * lax.rsqrt(spread + NORM_EPSILON) * gain_vec + bias_vec


def softplus(x):
    u = jnp.exp(-jnp.abs(x))
    s = u / (2.0 + u)
    q = s * s
    series = 1.0 / 17.0
    for k in (15.0, 13.0, 11.0, 9.0, 7.0, 5.0, 3.0, 1.0):
        series = series * q + 1.0 / k
    return jnp.maximum(x, 0.0) + 2.0 * s * series


def expm1(z):
    series = 1.0 + z * (1.0 / 9.0)
    for k in (8.0, 7.0, 6.0, 5.0, 4.0, 3.0, 2.0):
        series = 1.0 + z * (1.0 / k) * series
    return jnp.where(jnp.abs(z) < 0.5, z * series, jnp.exp(z) - 1.0)


def shifted_rows(values, by, row, fill):
    if by < 8:
        return jnp.where(row >= by, pltpu.roll(values, by, 0), fill)
    head = jnp.full((by, values.shape[1]), fill, values.dtype)
    return jnp.concatenate([head, values[: values.shape[0] - by]], axis=0)


def chain_rows(decay, drive):
    row = lax.broadcasted_iota(jnp.int32, decay.shape, 0)
    by = 1
    while by < decay.shape[0]:
        drive = decay * shifted_rows(drive, by, row, 0.0) + drive
        decay = decay * shifted_rows(decay, by, row, 1.0)
        by *= 2
    return decay, drive


def local_kernel(rows, border, taps, small_maps, large_maps, decay_param, extra, decays, states, totals, padded, maps):
    length, half = rows.shape[1], rows.shape[2]
    tap_count = taps.shape[0]
    tap_weights = taps[...].astype(F32)
    rate = -8.0 * softplus(-decay_param[...])
    margin = border.shape[1]
    per_half = half // LANES
    products, ends = [], []
    for g, blocks in enumerate((small_maps, large_maps)):
        padded[0:margin] = border[g].astype(F32)
        padded[margin : margin + length] = rows[g].astype(F32)
        start = margin - (tap_count - 1)
        summed = tap_weights[0, g : g + 1] * padded[start : start + length]
        for k in range(1, tap_count):
            summed = summed + tap_weights[k, g : g + 1] * padded[start + k : start + k + length]
        conv_rows = summed.astype(BF16)
        maps[...] = jnp.zeros(maps.shape, BF16)
        head = blocks.shape[-1]
        for m in range(2):
            for h in range(blocks.shape[1]):
                maps[h * head : (h + 1) * head, m * half + h * head : m * half + (h + 1) * head] = blocks[m, h]
        gates = jax.nn.sigmoid(dot(conv_rows, maps[...]))
        log_decay = gates[:, :half] * rate[g : g + 1] + extra[g]
        drive = jnp.sqrt(-expm1(2.0 * log_decay)) * gates[:, half:] * conv_rows.astype(F32)
        decay = jnp.exp(log_decay)
        for c in range(per_half):
            at = slice(c * LANES, (c + 1) * LANES)
            run = g * per_half + c
            product, state = chain_rows(decay[:, at], drive[:, at])
            to = slice(run * LANES, (run + 1) * LANES)
            decays[:, to] = product
            states[:, to] = state
            products.append(product[length - 1 :])
            ends.append(state[length - 1 :])
    span = jnp.concatenate(products + ends, axis=0)
    for j in range(totals.shape[0]):
        totals[j] = span


def joined(first, second):
    return first[0] * second[0], second[0] * first[1] + second[1]


def before_mine(spans, mine):
    half = spans.shape[1] // 2
    ahead = (jnp.ones((half, LANES), F32), jnp.zeros((half, LANES), F32))
    for j in range(spans.shape[0] - 1):
        new = joined(ahead, (spans[j, :half], spans[j, half:]))
        passed = j < mine
        ahead = tuple(jnp.where(passed, n, old) for n, old in zip(new, ahead))
    return ahead


def project_kernel(mine, spans, decays, states, gate_rows, weight_far, out, weight, sems):
    (copy,) = fetched([(weight_far, weight)], sems)
    entering = before_mine(spans, mine[0])[1]
    width = gate_rows.shape[2]
    per_half = width // LANES
    branches = []
    for g in range(gate_rows.shape[0]):
        start = jnp.concatenate([entering[g * per_half + c : g * per_half + c + 1] for c in range(per_half)], axis=1)
        at = slice(g * width, (g + 1) * width)
        state = states[:, at] + decays[:, at] * start
        branches.append((jax.nn.gelu(gate_rows[g].astype(F32), approximate=True) * state).astype(BF16))
    copy.wait()
    acc = dot(branches[0], weight[0])
    for g in range(1, len(branches)):
        acc = acc + dot(branches[g], weight[g])
    out[...] = acc.astype(BF16).reshape(out.shape)


def route_kernel(ids, weights, select, merge):
    slot_count, rows = select.shape[0], ids.shape[1]
    slot = lax.broadcasted_iota(jnp.int32, (slot_count, rows), 0)
    names = jnp.zeros((slot_count, rows), F32)
    weight = jnp.zeros((slot_count, rows), F32)
    for k in range(ids.shape[0]):
        named = ids[k : k + 1] == slot // SLOTS
        names = jnp.where(named, 1.0, names)
        weight = jnp.where(named, weights[k : k + 1], weight)
    earlier = lax.broadcasted_iota(jnp.int32, (rows, rows), 0) < lax.broadcasted_iota(jnp.int32, (rows, rows), 1)
    rank = dot(names.astype(BF16), jnp.where(earlier, 1.0, 0.0).astype(BF16))
    taken = (names > 0.0) & (rank == (slot % SLOTS).astype(F32))
    select[...] = jnp.where(taken, 1.0, 0.0).astype(BF16)[:, : select.shape[1]]
    merge[...] = jnp.where(taken, weight, 0.0).T[: merge.shape[0]]


def mix_kernel(parts, stream, gain, bias, select, normed, outgoing):
    mixed = parts[0].astype(F32)
    for j in range(1, parts.shape[0]):
        mixed = mixed + parts[j].astype(F32)
    rows = layer_norm(RESIDUAL_SCALE * stream[...].astype(F32) + mixed, gain[...], bias[...]).astype(BF16)
    normed[...] = rows
    outgoing[...] = dot(select[...], rows).astype(BF16).reshape(outgoing.shape)


def shared_kernel(normed, gate_w, up_w, down_w, merge, gain, bias, base, *kept):
    for target, source in zip(kept, (merge, gain, bias)):
        target[...] = source[...]
    rows = normed[...]
    gated, lifted = dot(rows, gate_w[...]), dot(rows, up_w[...])
    hidden = (jax.nn.silu(gated) * lifted).astype(BF16)
    base[...] = RESIDUAL_SCALE * rows.astype(F32) + dot(hidden, down_w[...])


def expert_kernel(rows, g0, g1, g2, g3, u0, u1, u2, u3, d0, d1, d2, d3a, d3b, out, pairs, down, sems):
    width = g0.shape[1]
    moves = []
    for j, (gate_w, up_w) in enumerate(((g0, u0), (g1, u1), (g2, u2), (g3, u3))):
        moves += [(gate_w, pairs.at[j, :, 0:width]), (up_w, pairs.at[j, :, width : 2 * width])]
    at = 0
    for piece in (d0, d1, d2, d3a, d3b):
        moves.append((piece, down.at[at : at + piece.shape[0]]))
        at += piece.shape[0]
    copies = fetched(moves, sems)
    picked = rows[...].reshape(-1, rows.shape[-1])
    hidden = []
    for j in range(pairs.shape[0]):
        copies[2 * j].wait()
        copies[2 * j + 1].wait()
        pair = dot(picked, pairs[j])
        hidden.append((jax.nn.silu(pair[:, :width]) * pair[:, width:]).astype(BF16))
    for copy in copies[2 * pairs.shape[0] :]:
        copy.wait()
    acc = dot(jnp.concatenate(hidden, axis=1), down[...])
    out[...] = acc.astype(BF16).reshape(out.shape)


def merge_kernel(returned, base, merge, gain, bias, out):
    rest = merge[...]
    rows = returned[...].reshape(-1, returned.shape[-1])
    total = base[...]
    for _ in range(3):
        part = rest.astype(BF16)
        total = total + dot(part, rows)
        rest = rest - part.astype(F32)
    out[...] = layer_norm(total, gain[...], bias[...]).astype(BF16)


def turned(shard, by):
    count = lax.axis_size("tp")
    return lax.ppermute(shard, "tp", [(i, (i + by) % count) for i in range(count)])


def swapped(pieces, axis):
    return lax.all_to_all(pieces, axis, 0, 0, tiled=True)


def shards(
    stream,
    recurrence_input,
    output_gate_input,
    convolution_taps,
    first_group_gates,
    second_group_gates,
    channel_decay,
    position_log_extra,
    recurrence_output_weight,
    first_norm_gain,
    first_norm_bias,
    routed_expert_index,
    routed_expert_weight,
    routed_gate_weight,
    routed_up_weight,
    routed_down_weight,
    shared_gate_weight,
    shared_up_weight,
    shared_down_weight,
    second_norm_gain,
    second_norm_bias,
):
    length, groups, half = recurrence_input.shape
    width = stream.shape[1]
    tp_count, sp_count = lax.axis_size("tp"), lax.axis_size("sp")
    quarter = length // tp_count
    expert_count = routed_gate_weight.shape[0] * sp_count
    slot_count = expert_count * SLOTS
    channels = groups * half
    shape, kept = jax.ShapeDtypeStruct, pltpu.VMEM

    rows = jnp.transpose(recurrence_input, (1, 0, 2))
    margin = 8
    border = lax.ppermute(rows[:, length - margin :], "sp", [(i, i + 1) for i in range(sp_count - 1)])

    gate_w, up_w, down_w = routed_gate_weight[0], routed_up_weight[0], routed_down_weight[0]
    gate_left, up_right = turned(gate_w, 1), turned(up_w, -1)
    up_left, gate_right = turned(up_w, 1), turned(gate_w, -1)

    own_index = lax.axis_index("tp")
    own_ids = lax.dynamic_slice_in_dim(routed_expert_index.T, own_index * quarter, quarter, 1)
    own_weights = lax.dynamic_slice_in_dim(routed_expert_weight.T, own_index * quarter, quarter, 1)
    fill = ((0, 0), (0, LANES - quarter))
    select, merge = kernel_call(
        route_kernel,
        [kept((slot_count, quarter), BF16), shape((quarter, slot_count), F32)],
        (jnp.pad(own_ids, fill, constant_values=-1), "vmem"),
        (jnp.pad(own_weights, fill), "vmem"),
    )

    runs = channels // LANES
    decays, states, totals = kernel_call(
        local_kernel,
        [kept((length, channels), F32), kept((length, channels), F32), shape((sp_count, 2 * runs, LANES), F32)],
        (rows, "vmem"),
        (border, "vmem"),
        convolution_taps,
        first_group_gates,
        second_group_gates,
        channel_decay,
        (jnp.transpose(position_log_extra, (1, 0, 2)), "vmem"),
        scratch=(pltpu.VMEM((margin + length, half), F32), pltpu.VMEM((half, 2 * half), BF16)),
    )
    spans = swapped(totals, "sp")
    parts = kernel_call(
        project_kernel,
        shape((tp_count, quarter, width), BF16),
        (lax.axis_index("sp").reshape(1), "smem"),
        (spans, "vmem"),
        (decays, "vmem"),
        (states, "vmem"),
        (jnp.transpose(output_gate_input, (1, 0, 2)), "vmem"),
        (recurrence_output_weight, "hbm"),
        scratch=(pltpu.VMEM(recurrence_output_weight.shape, BF16), pltpu.SemaphoreType.DMA((1,))),
    )
    parts = swapped(parts, "tp")

    down_left, down_right = turned(down_w, 1), turned(down_w, -1)
    gate_far, up_far = turned(gate_left, 1), turned(up_right, -1)

    normed, outgoing = kernel_call(
        mix_kernel,
        [kept((quarter, width), BF16), shape((expert_count, SLOTS, width), BF16)],
        (parts, "vmem"),
        stream,
        first_norm_gain.reshape(1, width),
        first_norm_bias.reshape(1, width),
        (select, "vmem"),
    )
    arrived = swapped(outgoing, "sp")

    cut = down_w.shape[0] // 2
    down_far = turned(down_left[:cut], 1), turned(down_right[cut:], -1)

    last = (merge, second_norm_gain.reshape(1, width), second_norm_bias.reshape(1, width))
    base, *last = kernel_call(
        shared_kernel,
        [kept((quarter, width), F32), *(kept(x.shape, F32) for x in last)],
        (normed, "vmem"),
        shared_gate_weight,
        shared_up_weight,
        shared_down_weight,
        *last,
    )
    weights = (gate_w, gate_left, gate_right, gate_far, up_w, up_left, up_right, up_far, down_w, down_left, down_right, *down_far)
    leaving = kernel_call(
        expert_kernel,
        kept((expert_count, SLOTS, width), BF16),
        (arrived, "vmem"),
        *((w, "hbm") for w in weights),
        scratch=(
            pltpu.VMEM((tp_count, width, 2 * gate_w.shape[1]), BF16),
            pltpu.VMEM((tp_count * down_w.shape[0], width), BF16),
            pltpu.SemaphoreType.DMA((len(weights),)),
        ),
    )
    returned = swapped(leaving, "sp")
    return kernel_call(
        merge_kernel, shape((quarter, width), BF16), (returned, "vmem"), (base, "vmem"), *((x, "vmem") for x in last)
    )


def solution(mesh):
    in_specs = (
        P(("sp", "tp"), None),
        P("sp", None, "tp"),
        P("sp", None, "tp"),
        P(None, None, "tp"),
        P(None, "tp", None, None),
        P(None, "tp", None, None),
        P(None, "tp"),
        P("sp", None, "tp"),
        P(None, "tp", None),
        P(),
        P(),
        P("sp", None),
        P("sp", None),
        P("sp", None, "tp"),
        P("sp", None, "tp"),
        P("sp", "tp", None),
        P(),
        P(),
        P(),
        P(),
        P(),
    )

    return jax.shard_map(shards, mesh=mesh, in_specs=in_specs, out_specs=P(("sp", "tp"), None), check_vma=False)
```

time: 152 us -> 139 us (0.914)
  local copies, waits for them, and re-layouts: 16 us -> 3.61 us
  waiting for transfers between devices: 58 us -> 65.6 us
  Pallas kernels: 23.8 us -> 18 us
  starting transfers between devices: 53.7 us -> 51.5 us
    reshape x4 -> x0, local copies, waits for them, and re-layouts: 6.34 us -> none  [the longest x1 2.18 us: shards(): arrived = swapped(outgoing.reshape(expert_count, SLOTS, width), sp_axes)]
    pallas_call x8 -> x7, Pallas kernels: 23.8 us -> 18 us  [kernel_call(): pl.pallas_call(body, out_shape=out_shape, in_specs=specs, out_specs=[VMEM...]
    all_to_all x5 -> x4, starting transfers between devices: 41 us -> 35.6 us  [swapped(): return lax.all_to_all(pieces, axis, 0, 0, tiled=True)]
    all_to_all x5 -> x4, waiting for transfers between devices: 24.1 us -> 29.3 us  [swapped(): return lax.all_to_all(pieces, axis, 0, 0, tiled=True)]
    unnamed x33 -> x31, local copies, waits for them, and re-layouts: 8.26 us -> 3.42 us
    ppermute x10, starting transfers between devices: 8.22 us -> 11.4 us  [turned(): lax.ppermute(shard, 'tp', [(i, (i + by) % count) for i in range(count)])]
    ppermute x10, waiting for transfers between devices: 33.9 us -> 36.3 us  [turned(): lax.ppermute(shard, 'tp', [(i, (i + by) % count) for i in range(count)])]
  transfers between devices with their start and end apart: 16 -> 15, of which waited for: 9 -> 9; matrix products, arithmetic and copies ran while one was open for 5% -> 1% of each run, Pallas kernels for 6% -> 5%
where the time goes in v2:
time: 139 us
  waiting for transfers between devices  65.6 us (47%)
  starting transfers between devices  51.5 us (37%)
  Pallas kernels  18 us (13%)
  local copies, waits for them, and re-layouts  3.61 us (3%)
    ppermute x10, waiting for transfers between devices, turned(): lax.ppermute(shard, 'tp', [(i, (i + by) % count) for i in range(count)])  36.3 us
    all_to_all x4, starting transfers between devices, swapped(): return lax.all_to_all(pieces, axis, 0, 0, tiled=True)  35.6 us
    all_to_all x4, waiting for transfers between devices, swapped(): return lax.all_to_all(pieces, axis, 0, 0, tiled=True)  29.3 us
    pallas_call x7, Pallas kernels, kernel_call(): pl.pallas_call(body, out_shape=out_shape, in_specs=specs, out_specs=[VMEM...  18 us
    ppermute x10, starting transfers between devices, turned(): lax.ppermute(shard, 'tp', [(i, (i + by) % count) for i in range(count)])  11.4 us
    ppermute x1, starting transfers between devices, shards(): lax.ppermute(rows[:, length - margin:], 'sp', [(i, i + 1) for i in range(...  4.5 us
    unnamed x31, local copies, waits for them, and re-layouts  3.42 us
  transfers between devices with their start and end apart: 15, of which 9 were waited for; matrix products, arithmetic and copies ran while one was open for 1% of the time, Pallas kernels for 5%

profile of v2, /device:TPU:1, one launch (start us, length us, event | category | flops | bytes accessed | tf_op | source)
XLA Modules:
  0.0 138.9 jit_solution(16095585013125782777)
XLA Ops:
  0.0 0.0 copy-start
  0.0 0.0 copy-start.12
  0.0 1.0 copy.30
  1.0 4.5 %collective-permute-start = (bf16[2,8,256]{2,1,0:T(8,128)(2,1)S(1)}, bf16[2,8,256]{2,1,0:T(8,128)(2,1)S(1)}, u32[]{:S(2)}, u32[]{:S(2)}) collective-permute-start(bf16[2,8,256]{2,1,0:T(8,128)(2,1)S(1)} %slice.12), channel_id=1, source_target_pairs={{0,4},{4,8},{8,12},{12,16},{16,20},{20,24},{24,28},{28,32},{32,36}... | collective-permute-start | bytes 24584 | tf_op jit(solution)/shard_map/ppermute | solution.py:270
  5.5 1.0 copy.28
  6.5 0.0 collective-permute-done.border
  6.5 2.8 %shard_map.199 = (f32[128,512]{1,0:T(8,128)S(1)}, f32[128,512]{1,0:T(8,128)S(1)}, f32[64,8,128]{2,1,0:T(8,128)}) custom-call(bf16[2,128,256]{2,1,0:T(8,128)(2,1)S(1)} %bitcast.23, bf16[2,8,256]{2,1,0:T(8,128)(2,1)S(1)} %collective-permute-done.border, bf16[4,2,256]{2,1,0:T(2,128)(2,1)} %taps.1, bf16[2,4,64,64]{3,2,1,0:T(8,128)(2,1)} %small_maps.1, ...), custom_call_target="tpu_custom_call" | custom-call | tf_op jit(solution)/shard_map/pallas_call | solution.py:27
  9.3 13.3 %all-to-all-start = ((f32[64,8,128]{2,1,0:T(8,128)}), f32[64,8,128]{2,1,0:T(8,128)S(1)}, u32[]{:S(2)}, u32[]{:S(2)}) async-start(f32[64,8,128]{2,1,0:T(8,128)} %get-tuple-element.16), calls=%async_computation | async-start | bytes 524288 | tf_op jit(solution)/shard_map/all_to_all | solution.py:233
  22.6 0.0 copy-done.12
  22.7 13.0 %all-to-all-done.spans = f32[64,8,128]{2,1,0:T(8,128)S(1)} async-done(((f32[64,8,128]{2,1,0:T(8,128)}), f32[64,8,128]{2,1,0:T(8,128)S(1)}, u32[]{:S(2)}, u32[]{:S(2)}) %all-to-all-start) | async-done | bytes 262176 | tf_op jit(solution)/shard_map/all_to_all | solution.py:233
  35.7 0.0 copy-start.6
  35.7 0.0 copy-start.4
  35.7 0.0 copy-start.5
  35.7 0.0 copy-start.13
  35.7 3.0 %shard_map.200 = bf16[4,32,2048]{2,1,0:T(8,128)(2,1)} custom-call(s32[1]{0:T(128)} %bitcast.mine, f32[64,8,128]{2,1,0:T(8,128)S(1)} %all-to-all-done.spans, f32[128,512]{1,0:T(8,128)S(1)} %get-tuple-element.17.decays, f32[128,512]{1,0:T(8,128)S(1)} %get-tuple-element.18.states, bf16[2,128,256]{2,1,0:T(8,128)(2,1)S(1)} %bitcast.24, ...), custom_call_target="tpu_custom_call" | custom-call | tf_op jit(solution)/shard_map/pallas_call | solution.py:27
  38.7 4.2 %all-to-all-start.1 = ((bf16[4,32,2048]{2,1,0:T(8,128)(2,1)}), bf16[4,32,2048]{2,1,0:T(8,128)(2,1)S(1)}, u32[]{:S(2)}, u32[]{:S(2)}) async-start(bf16[4,32,2048]{2,1,0:T(8,128)(2,1)} %shard_map.200), calls=%async_computation.1 | async-start | bytes 1048576 | tf_op jit(solution)/shard_map/all_to_all | solution.py:233
  42.9 0.0 copy-done.6
  42.9 2.7 %collective-permute-start.8 = (bf16[128,2048]{1,0:T(8,128)(2,1)S(1)}, bf16[128,2048]{1,0:T(8,128)(2,1)S(1)}, u32[]{:S(2)}, u32[]{:S(2)}) collective-permute-start(bf16[128,2048]{1,0:T(8,128)(2,1)S(1)} %bitcast.32), channel_id=1, source_target_pairs={{0,3},{1,0},{2,1},{3,2},{4,7},{5,4},{6,5},{7,6},{8,11},{9,8},{10,9... | collective-permute-start | bytes 1572872 | tf_op jit(solution)/shard_map/ppermute | solution.py:229
  45.6 0.0 copy-done.4
  45.6 0.0 collective-permute-start.1
  45.6 0.0 copy-done.5
  45.6 2.7 %collective-permute-start.5 = (bf16[2048,128]{1,0:T(8,128)(2,1)S(1)}, bf16[2048,128]{1,0:T(8,128)(2,1)}, u32[]{:S(2)}, u32[]{:S(2)}) collective-permute-start(bf16[2048,128]{1,0:T(8,128)(2,1)S(1)} %bitcast.29), channel_id=1, source_target_pairs={{0,3},{1,0},{2,1},{3,2},{4,7},{5,4},{6,5},{7,6},{8,11},{9,8},{10,9... | collective-permute-start | bytes 1572872 | tf_op jit(solution)/shard_map/ppermute | solution.py:229
  48.2 0.0 copy-done
  48.2 0.1 dynamic-slice_bitcast_fusion.1
  48.3 0.0 copy-done.13
  48.3 0.1 dynamic-slice_bitcast_fusion
  48.4 0.2 shard_map.201
  48.6 0.0 copy-start.1
  48.6 0.6 copy-done.1
  49.2 2.7 %all-to-all-done.1.parts = bf16[4,32,2048]{2,1,0:T(8,128)(2,1)S(1)} async-done(((bf16[4,32,2048]{2,1,0:T(8,128)(2,1)}), bf16[4,32,2048]{2,1,0:T(8,128)(2,1)S(1)}, u32[]{:S(2)}, u32[]{:S(2)}) %all-to-all-start.1) | async-done | bytes 524320 | tf_op jit(solution)/shard_map/all_to_all | solution.py:233
  51.9 2.3 %shard_map.202 = (bf16[32,2048]{1,0:T(8,128)(2,1)S(1)}, bf16[64,2,2048]{2,1,0:T(2,128)(2,1)}) custom-call(bf16[4,32,2048]{2,1,0:T(8,128)(2,1)S(1)} %all-to-all-done.1.parts, bf16[32,2048]{1,0:T(8,128)(2,1)} %stream.1, f32[1,2048]{1,0:T(1,128)} %bitcast.34, f32[1,2048]{1,0:T(1,128)} %bitcast.35, bf16[128,32]{1,0:T(8,128)(2,1)S(1)} %get-tuple-element.19.select), custom_call_target="tpu_custom_call" | custom-call | tf_op jit(solution)/shard_map/pallas_call | solution.py:27
  54.2 6.9 %all-to-all-start.2 = ((bf16[64,2,2048]{2,1,0:T(2,128)(2,1)}), bf16[64,2,2048]{2,1,0:T(2,128)(2,1)S(1)}, u32[]{:S(2)}, u32[]{:S(2)}) async-start(bf16[64,2,2048]{2,1,0:T(2,128)(2,1)} %get-tuple-element.20), calls=%async_computation.2 | async-start | bytes 1048576 | tf_op jit(solution)/shard_map/all_to_all | solution.py:233
  61.1 0.4 collective-permute-start.7
  61.5 2.4 %collective-permute-start.2 = (bf16[2048,128]{1,0:T(8,128)(2,1)S(1)}, bf16[2048,128]{1,0:T(8,128)(2,1)S(1)}, u32[]{:S(2)}, u32[]{:S(2)}) collective-permute-start(bf16[2048,128]{1,0:T(8,128)(2,1)S(1)} %bitcast.27), channel_id=1, source_target_pairs={{0,3},{1,0},{2,1},{3,2},{4,7},{5,4},{6,5},{7,6},{8,11},{9,8},{10,9... | collective-permute-start | bytes 1572872 | tf_op jit(solution)/shard_map/ppermute | solution.py:229
  63.9 0.0 collective-permute-done.8.d2
  63.9 0.0 copy-start.2
  63.9 0.0 collective-permute-start.4
  63.9 0.0 collective-permute-done.1.g1
  63.9 0.1 collective-permute-start.3
  64.0 9.0 %collective-permute-done.5.u2 = bf16[2048,128]{1,0:T(8,128)(2,1)} collective-permute-done((bf16[2048,128]{1,0:T(8,128)(2,1)S(1)}, bf16[2048,128]{1,0:T(8,128)(2,1)}, u32[]{:S(2)}, u32[]{:S(2)}) %collective-permute-start.5) | collective-permute-done | bytes 524320 | tf_op jit(solution)/shard_map/ppermute | solution.py:229
  73.0 1.7 %collective-permute-start.6 = (bf16[2048,128]{1,0:T(8,128)(2,1)}, bf16[2048,128]{1,0:T(8,128)(2,1)}, u32[]{:S(2)}, u32[]{:S(2)}) collective-permute-start(bf16[2048,128]{1,0:T(8,128)(2,1)} %collective-permute-done.5.u2), channel_id=1, source_target_pairs={{0,3},{1,0},{2,1},{3,2},{4,7},{5,4},{6,5},{7,6},{8,11},{9,8},{10,9... | collective-permute-start | bytes 1572872 | tf_op jit(solution)/shard_map/ppermute | solution.py:229
  74.7 0.8 collective-permute-done.7.d1
  75.4 0.4 collective-permute-start.10
  75.8 8.3 %collective-permute-done.2.g2 = bf16[2048,128]{1,0:T(8,128)(2,1)S(1)} collective-permute-done((bf16[2048,128]{1,0:T(8,128)(2,1)S(1)}, bf16[2048,128]{1,0:T(8,128)(2,1)S(1)}, u32[]{:S(2)}, u32[]{:S(2)}) %collective-permute-start.2) | collective-permute-done | bytes 524320 | tf_op jit(solution)/shard_map/ppermute | solution.py:229
  84.1 1.2 collective-permute-start.9
  85.3 1.4 collective-permute-done.4.u1
  86.7 14.3 %collective-permute-done.10.d3b = bf16[64,2048]{1,0:T(8,128)(2,1)S(1)} collective-permute-done((bf16[64,2048]{1,0:T(8,128)(2,1)S(1)}, bf16[64,2048]{1,0:T(8,128)(2,1)S(1)}, u32[]{:S(2)}, u32[]{:S(2)}) %collective-permute-start.10) | collective-permute-done | bytes 262176 | tf_op jit(solution)/shard_map/ppermute | solution.py:229
  101.0 2.5 %collective-permute-done.9.d3a = bf16[64,2048]{1,0:T(8,128)(2,1)S(1)} collective-permute-done((bf16[64,2048]{1,0:T(8,128)(2,1)S(1)}, bf16[64,2048]{1,0:T(8,128)(2,1)S(1)}, u32[]{:S(2)}, u32[]{:S(2)}) %collective-permute-start.9) | collective-permute-done | bytes 262176 | tf_op jit(solution)/shard_map/ppermute | solution.py:229
  103.5 0.0 collective-permute-done.3.g3
  103.5 0.0 copy-done.7
  103.5 0.0 copy-done.8
  103.5 0.0 copy-start.9
  103.5 0.8 copy-done.9
  104.4 0.0 collective-permute-done.6.u3
  104.4 0.0 all-to-all-done.2.rows
  104.4 0.0 copy-done.2
  104.4 0.0 copy-done.3
  104.4 0.0 copy-done.10
  104.4 0.0 copy-done.11
  104.4 4.3 %shard_map.203 = bf16[64,2,2048]{2,1,0:T(2,128)(2,1)} custom-call(bf16[64,2,2048]{2,1,0:T(2,128)(2,1)S(1)} %all-to-all-done.2.rows, bf16[2048,128]{1,0:T(8,128)(2,1)} %bitcast.25, bf16[2048,128]{1,0:T(8,128)(2,1)} %collective-permute-done.1.g1, bf16[2048,128]{1,0:T(8,128)(2,1)} %copy-done.7, bf16[2048,128]{1,0:T(8,128)(2,1)} %copy-done.9, ...), custom_call_target="tpu_custom_call" | custom-call | tf_op jit(solution)/shard_map/pallas_call | solution.py:27
  108.7 11.2 %all-to-all-start.3 = ((bf16[64,2,2048]{2,1,0:T(2,128)(2,1)}), bf16[64,2,2048]{2,1,0:T(2,128)(2,1)S(1)}, u32[]{:S(2)}, u32[]{:S(2)}) async-start(bf16[64,2,2048]{2,1,0:T(2,128)(2,1)} %shard_map.203), calls=%async_computation.3 | async-start | bytes 1048576 | tf_op jit(solution)/shard_map/all_to_all | solution.py:233
  120.0 4.1 %shard_map.204 = (f32[32,2048]{1,0:T(8,128)S(1)}, f32[32,128]{1,0:T(8,128)S(1)}, f32[1,2048]{1,0:T(1,128)S(1)}, f32[1,2048]{1,0:T(1,128)S(1)}) custom-call(bf16[32,2048]{1,0:T(8,128)(2,1)S(1)} %get-tuple-element.21.normed, bf16[2048,512]{1,0:T(8,128)(2,1)} %gate_w.1, bf16[2048,512]{1,0:T(8,128)(2,1)} %up_w.1, bf16[512,2048]{1,0:T(8,128)(2,1)} %down_w.1, ...), custom_call_target="tpu_custom_call" | custom-call | tf_op jit(solution)/shard_map/pallas_call | solution.py:27
  124.1 13.5 %all-to-all-done.3.returned = bf16[64,2,2048]{2,1,0:T(2,128)(2,1)S(1)} async-done(((bf16[64,2,2048]{2,1,0:T(2,128)(2,1)}), bf16[64,2,2048]{2,1,0:T(2,128)(2,1)S(1)}, u32[]{:S(2)}, u32[]{:S(2)}) %all-to-all-start.3) | async-done | bytes 524320 | tf_op jit(solution)/shard_map/all_to_all | solution.py:233
  137.7 1.2 shard_map.205
  (11 shorter events, 0.1 us)
Async XLA Ops:
  0.0 48.2 %copy-start = (s32[128,4]{0,1:T(4,128)S(1)}, s32[128,4]{0,1:T(4,128)}, u32[]{:S(2)}) copy-start(s32[128,4]{0,1:T(4,128)} %param.32) | copy-start | bytes 6148
  0.0 22.6 %copy-start.12 = (bf16[128,2,256]{2,1,0:T(2,128)(2,1)S(1)}, bf16[128,2,256]{2,1,0:T(2,128)(2,1)}, u32[]{:S(2)}) copy-start(bf16[128,2,256]{2,1,0:T(2,128)(2,1)} %param.23) | copy-start | bytes 393220
  1.0 5.5 %collective-permute-start = (bf16[2,8,256]{2,1,0:T(8,128)(2,1)S(1)}, bf16[2,8,256]{2,1,0:T(8,128)(2,1)S(1)}, u32[]{:S(2)}, u32[]{:S(2)}) collective-permute-start(bf16[2,8,256]{2,1,0:T(8,128)(2,1)S(1)} %slice.12), channel_id=1, source_target_pairs={{0,4},{4,8},{8,12},{12,16},{16,20},{20,24},{24,28},{28,32},{32,36}... | collective-permute-start | bytes 24584 | tf_op jit(solution)/shard_map/ppermute | solution.py:270
  9.3 26.4 %all-to-all-start = ((f32[64,8,128]{2,1,0:T(8,128)}), f32[64,8,128]{2,1,0:T(8,128)S(1)}, u32[]{:S(2)}, u32[]{:S(2)}) async-start(f32[64,8,128]{2,1,0:T(8,128)} %get-tuple-element.16), calls=%async_computation | async-start | bytes 524288 | tf_op jit(solution)/shard_map/all_to_all | solution.py:233
  35.7 7.2 %copy-start.6 = (bf16[1,128,2048]{2,1,0:T(8,128)(2,1)S(1)}, bf16[1,128,2048]{2,1,0:T(8,128)(2,1)}, u32[]{:S(2)}) copy-start(bf16[1,128,2048]{2,1,0:T(8,128)(2,1)} %param.36) | copy-start | bytes 1572868
  35.7 9.9 %copy-start.4 = (bf16[1,2048,128]{2,1,0:T(8,128)(2,1)S(1)}, bf16[1,2048,128]{2,1,0:T(8,128)(2,1)}, u32[]{:S(2)}) copy-start(bf16[1,2048,128]{2,1,0:T(8,128)(2,1)} %param.34) | copy-start | bytes 1572868
  35.7 9.9 %copy-start.5 = (bf16[1,2048,128]{2,1,0:T(8,128)(2,1)S(1)}, bf16[1,2048,128]{2,1,0:T(8,128)(2,1)}, u32[]{:S(2)}) copy-start(bf16[1,2048,128]{2,1,0:T(8,128)(2,1)} %param.35) | copy-start | bytes 1572868
  35.7 12.6 %copy-start.13 = (f32[128,4]{0,1:T(4,128)S(1)}, f32[128,4]{0,1:T(4,128)}, u32[]{:S(2)}) copy-start(f32[128,4]{0,1:T(4,128)} %param.33) | copy-start | bytes 6148
  38.7 13.2 %all-to-all-start.1 = ((bf16[4,32,2048]{2,1,0:T(8,128)(2,1)}), bf16[4,32,2048]{2,1,0:T(8,128)(2,1)S(1)}, u32[]{:S(2)}, u32[]{:S(2)}) async-start(bf16[4,32,2048]{2,1,0:T(8,128)(2,1)} %shard_map.200), calls=%async_computation.1 | async-start | bytes 1048576 | tf_op jit(solution)/shard_map/all_to_all | solution.py:233
  42.9 21.0 %collective-permute-start.8 = (bf16[128,2048]{1,0:T(8,128)(2,1)S(1)}, bf16[128,2048]{1,0:T(8,128)(2,1)S(1)}, u32[]{:S(2)}, u32[]{:S(2)}) collective-permute-start(bf16[128,2048]{1,0:T(8,128)(2,1)S(1)} %bitcast.32), channel_id=1, source_target_pairs={{0,3},{1,0},{2,1},{3,2},{4,7},{5,4},{6,5},{7,6},{8,11},{9,8},{10,9... | collective-permute-start | bytes 1572872 | tf_op jit(solution)/shard_map/ppermute | solution.py:229
  45.6 18.3 %collective-permute-start.1 = (bf16[2048,128]{1,0:T(8,128)(2,1)S(1)}, bf16[2048,128]{1,0:T(8,128)(2,1)}, u32[]{:S(2)}, u32[]{:S(2)}) collective-permute-start(bf16[2048,128]{1,0:T(8,128)(2,1)S(1)} %bitcast.26), channel_id=1, source_target_pairs={{0,1},{1,2},{2,3},{3,0},{4,5},{5,6},{6,7},{7,4},{8,9},{9,10},{10,1... | collective-permute-start | bytes 1572872 | tf_op jit(solution)/shard_map/ppermute | solution.py:229
  45.6 27.4 %collective-permute-start.5 = (bf16[2048,128]{1,0:T(8,128)(2,1)S(1)}, bf16[2048,128]{1,0:T(8,128)(2,1)}, u32[]{:S(2)}, u32[]{:S(2)}) collective-permute-start(bf16[2048,128]{1,0:T(8,128)(2,1)S(1)} %bitcast.29), channel_id=1, source_target_pairs={{0,3},{1,0},{2,1},{3,2},{4,7},{5,4},{6,5},{7,6},{8,11},{9,8},{10,9... | collective-permute-start | bytes 1572872 | tf_op jit(solution)/shard_map/ppermute | solution.py:229
  48.6 0.6 copy-start.1
  54.2 50.2 %all-to-all-start.2 = ((bf16[64,2,2048]{2,1,0:T(2,128)(2,1)}), bf16[64,2,2048]{2,1,0:T(2,128)(2,1)S(1)}, u32[]{:S(2)}, u32[]{:S(2)}) async-start(bf16[64,2,2048]{2,1,0:T(2,128)(2,1)} %get-tuple-element.20), calls=%async_computation.2 | async-start | bytes 1048576 | tf_op jit(solution)/shard_map/all_to_all | solution.py:233
  61.1 14.3 %collective-permute-start.7 = (bf16[128,2048]{1,0:T(8,128)(2,1)S(1)}, bf16[128,2048]{1,0:T(8,128)(2,1)S(1)}, u32[]{:S(2)}, u32[]{:S(2)}) collective-permute-start(bf16[128,2048]{1,0:T(8,128)(2,1)S(1)} %bitcast.33), channel_id=1, source_target_pairs={{0,1},{1,2},{2,3},{3,0},{4,5},{5,6},{6,7},{7,4},{8,9},{9,10},{10,1... | collective-permute-start | bytes 1572872 | tf_op jit(solution)/shard_map/ppermute | solution.py:229
  61.5 22.6 %collective-permute-start.2 = (bf16[2048,128]{1,0:T(8,128)(2,1)S(1)}, bf16[2048,128]{1,0:T(8,128)(2,1)S(1)}, u32[]{:S(2)}, u32[]{:S(2)}) collective-permute-start(bf16[2048,128]{1,0:T(8,128)(2,1)S(1)} %bitcast.27), channel_id=1, source_target_pairs={{0,3},{1,0},{2,1},{3,2},{4,7},{5,4},{6,5},{7,6},{8,11},{9,8},{10,9... | collective-permute-start | bytes 1572872 | tf_op jit(solution)/shard_map/ppermute | solution.py:229
  63.9 40.5 %copy-start.2 = (bf16[128,2048]{1,0:T(8,128)(2,1)}, bf16[128,2048]{1,0:T(8,128)(2,1)S(1)}, u32[]{:S(2)}) copy-start(bf16[128,2048]{1,0:T(8,128)(2,1)S(1)} %collective-permute-done.8.d2) | copy-start | bytes 1572868
  63.9 22.8 %collective-permute-start.4 = (bf16[2048,128]{1,0:T(8,128)(2,1)S(1)}, bf16[2048,128]{1,0:T(8,128)(2,1)S(1)}, u32[]{:S(2)}, u32[]{:S(2)}) collective-permute-start(bf16[2048,128]{1,0:T(8,128)(2,1)S(1)} %bitcast.30), channel_id=1, source_target_pairs={{0,1},{1,2},{2,3},{3,0},{4,5},{5,6},{6,7},{7,4},{8,9},{9,10},{10,1... | collective-permute-start | bytes 1572872 | tf_op jit(solution)/shard_map/ppermute | solution.py:229
  63.9 39.6 %collective-permute-start.3 = (bf16[2048,128]{1,0:T(8,128)(2,1)}, bf16[2048,128]{1,0:T(8,128)(2,1)S(1)}, u32[]{:S(2)}, u32[]{:S(2)}) collective-permute-start(bf16[2048,128]{1,0:T(8,128)(2,1)} %collective-permute-done.1.g1), channel_id=1, source_target_pairs={{0,1},{1,2},{2,3},{3,0},{4,5},{5,6},{6,7},{7,4},{8,9},{9,10},{10,1... | collective-permute-start | bytes 1572872 | tf_op jit(solution)/shard_map/ppermute | solution.py:229
  73.0 31.4 %collective-permute-start.6 = (bf16[2048,128]{1,0:T(8,128)(2,1)}, bf16[2048,128]{1,0:T(8,128)(2,1)}, u32[]{:S(2)}, u32[]{:S(2)}) collective-permute-start(bf16[2048,128]{1,0:T(8,128)(2,1)} %collective-permute-done.5.u2), channel_id=1, source_target_pairs={{0,3},{1,0},{2,1},{3,2},{4,7},{5,4},{6,5},{7,6},{8,11},{9,8},{10,9... | collective-permute-start | bytes 1572872 | tf_op jit(solution)/shard_map/ppermute | solution.py:229
  75.4 28.9 %copy-start.3 = (bf16[128,2048]{1,0:T(8,128)(2,1)}, bf16[128,2048]{1,0:T(8,128)(2,1)S(1)}, u32[]{:S(2)}) copy-start(bf16[128,2048]{1,0:T(8,128)(2,1)S(1)} %collective-permute-done.7.d1) | copy-start | bytes 1572868
  75.4 25.5 %collective-permute-start.10 = (bf16[64,2048]{1,0:T(8,128)(2,1)S(1)}, bf16[64,2048]{1,0:T(8,128)(2,1)S(1)}, u32[]{:S(2)}, u32[]{:S(2)}) collective-permute-start(bf16[64,2048]{1,0:T(8,128)(2,1)S(1)} %slice.14), channel_id=1, source_target_pairs={{0,3},{1,0},{2,1},{3,2},{4,7},{5,4},{6,5},{7,6},{8,11},{9,8},{10,9... | collective-permute-start | bytes 786440 | tf_op jit(solution)/shard_map/ppermute | solution.py:229
  84.1 19.4 %copy-start.7 = (bf16[2048,128]{1,0:T(8,128)(2,1)}, bf16[2048,128]{1,0:T(8,128)(2,1)S(1)}, u32[]{:S(2)}) copy-start(bf16[2048,128]{1,0:T(8,128)(2,1)S(1)} %collective-permute-done.2.g2) | copy-start | bytes 1572868
  84.1 19.4 %collective-permute-start.9 = (bf16[64,2048]{1,0:T(8,128)(2,1)S(1)}, bf16[64,2048]{1,0:T(8,128)(2,1)S(1)}, u32[]{:S(2)}, u32[]{:S(2)}) collective-permute-start(bf16[64,2048]{1,0:T(8,128)(2,1)S(1)} %slice.13), channel_id=1, source_target_pairs={{0,1},{1,2},{2,3},{3,0},{4,5},{5,6},{6,7},{7,4},{8,9},{9,10},{10,1... | collective-permute-start | bytes 786440 | tf_op jit(solution)/shard_map/ppermute | solution.py:229
  86.7 16.9 %copy-start.8 = (bf16[2048,128]{1,0:T(8,128)(2,1)}, bf16[2048,128]{1,0:T(8,128)(2,1)S(1)}, u32[]{:S(2)}) copy-start(bf16[2048,128]{1,0:T(8,128)(2,1)S(1)} %collective-permute-done.4.u1) | copy-start | bytes 1572868
  101.0 3.4 %copy-start.10 = (bf16[64,2048]{1,0:T(8,128)(2,1)}, bf16[64,2048]{1,0:T(8,128)(2,1)S(1)}, u32[]{:S(2)}) copy-start(bf16[64,2048]{1,0:T(8,128)(2,1)S(1)} %collective-permute-done.10.d3b) | copy-start | bytes 786436
  103.5 0.9 copy-start.11
  103.5 0.8 copy-start.9
  108.7 28.9 %all-to-all-start.3 = ((bf16[64,2,2048]{2,1,0:T(2,128)(2,1)}), bf16[64,2,2048]{2,1,0:T(2,128)(2,1)S(1)}, u32[]{:S(2)}, u32[]{:S(2)}) async-start(bf16[64,2,2048]{2,1,0:T(2,128)(2,1)} %shard_map.203), calls=%async_computation.3 | async-start | bytes 1048576 | tf_op jit(solution)/shard_map/all_to_all | solution.py:233

commit v3 on v2

--- a/solution.py
+++ b/solution.py
@@ -85,78 +85,100 @@
     return decay, drive
 
 
+def flat(array):
+    length, groups, half = array.shape
+    return array.reshape(length, groups, half // LANES, LANES).transpose(0, 2, 1, 3).reshape(-1, LANES)
+
+
 def local_kernel(rows, border, taps, small_maps, large_maps, decay_param, extra, decays, states, totals, padded, maps):
-    length, half = rows.shape[1], rows.shape[2]
+    groups, half = decay_param.shape
+    per_half = half // LANES
+    step = groups * per_half
+    length = rows.shape[0] // step
     tap_count = taps.shape[0]
     tap_weights = taps[...].astype(F32)
     rate = -8.0 * softplus(-decay_param[...])
-    margin = border.shape[1]
-    per_half = half // LANES
-    products, ends = [], []
+    margin = border.shape[0]
+    padded[0:margin] = border[...].astype(F32)
+    padded[margin:] = rows[...].astype(F32)
+    logs, ends = [], []
     for g, blocks in enumerate((small_maps, large_maps)):
-        padded[0:margin] = border[g].astype(F32)
-        padded[margin : margin + length] = rows[g].astype(F32)
-        start = margin - (tap_count - 1)
-        summed = tap_weights[0, g : g + 1] * padded[start : start + length]
-        for k in range(1, tap_count):
-            summed = summed + tap_weights[k, g : g + 1] * padded[start + k : start + k + length]
-        conv_rows = summed.astype(BF16)
+        conv_runs = []
+        for c in range(per_half):
+            at = slice(c * LANES, (c + 1) * LANES)
+            summed = None
+            for k in range(tap_count):
+                start = margin - (tap_count - 1 - k) * step + c * groups + g
+                term = tap_weights[k, g : g + 1, at] * padded[pl.ds(start, length, stride=step), :]
+                summed = term if summed is None else summed + term
+            conv_runs.append(summed.astype(BF16))
+        conv_rows = jnp.concatenate(conv_runs, axis=1)
         maps[...] = jnp.zeros(maps.shape, BF16)
         head = blocks.shape[-1]
         for m in range(2):
             for h in range(blocks.shape[1]):
                 maps[h * head : (h + 1) * head, m * half + h * head : m * half + (h + 1) * head] = blocks[m, h]
         gates = jax.nn.sigmoid(dot(conv_rows, maps[...]))
-        log_decay = gates[:, :half] * rate[g : g + 1] + extra[g]
-        drive = jnp.sqrt(-expm1(2.0 * log_decay)) * gates[:, half:] * conv_rows.astype(F32)
-        decay = jnp.exp(log_decay)
         for c in range(per_half):
             at = slice(c * LANES, (c + 1) * LANES)
-            run = g * per_half + c
-            product, state = chain_rows(decay[:, at], drive[:, at])
-            to = slice(run * LANES, (run + 1) * LANES)
+            log_decay = gates[:, at] * rate[g : g + 1, at] + extra[pl.ds(c * groups + g, length, stride=step), :]
+            gate = gates[:, half + c * LANES : half + (c + 1) * LANES]
+            drive = jnp.sqrt(-expm1(2.0 * log_decay)) * gate * conv_runs[c].astype(F32)
+            product, state = chain_rows(jnp.exp(log_decay), drive)
+            to = slice((g * per_half + c) * LANES, (g * per_half + c + 1) * LANES)
             decays[:, to] = product
             states[:, to] = state
-            products.append(product[length - 1 :])
+            logs.append(jnp.sum(log_decay, axis=0, keepdims=True))
             ends.append(state[length - 1 :])
-    span = jnp.concatenate(products + ends, axis=0)
+    span = jnp.concatenate(logs + ends, axis=0).astype(BF16)
     for j in range(totals.shape[0]):
         totals[j] = span
 
 
-def joined(first, second):
-    return first[0] * second[0], second[0] * first[1] + second[1]
-
-
-def before_mine(spans, mine):
+def entering_state(spans, mine):
     half = spans.shape[1] // 2
-    ahead = (jnp.ones((half, LANES), F32), jnp.zeros((half, LANES), F32))
-    for j in range(spans.shape[0] - 1):
-        new = joined(ahead, (spans[j, :half], spans[j, half:]))
-        passed = j < mine
-        ahead = tuple(jnp.where(passed, n, old) for n, old in zip(new, ahead))
-    return ahead
-
-
-def project_kernel(mine, spans, decays, states, gate_rows, weight_far, out, weight, sems):
+    span = lax.broadcasted_iota(jnp.int32, (spans.shape[0], half, LANES), 0)
+    logs = spans[:, :half].astype(F32)
+    decays = jnp.where(span < mine, jnp.exp(logs), 1.0)
+    ends = jnp.where(span < mine, spans[:, half:].astype(F32), 0.0)
+    state = ends[0]
+    for j in range(1, spans.shape[0] - 1):
+        state = decays[j] * state + ends[j]
+    return state
+
+
+def project_kernel(mine, spans, decays, states, gated, weight_far, out, weight, sems):
     (copy,) = fetched([(weight_far, weight)], sems)
-    entering = before_mine(spans, mine[0])[1]
-    width = gate_rows.shape[2]
-    per_half = width // LANES
+    entering = entering_state(spans, mine[0])
+    runs = entering.shape[0]
     branches = []
-    for g in range(gate_rows.shape[0]):
-        start = jnp.concatenate([entering[g * per_half + c : g * per_half + c + 1] for c in range(per_half)], axis=1)
-        at = slice(g * width, (g + 1) * width)
-        state = states[:, at] + decays[:, at] * start
-        branches.append((jax.nn.gelu(gate_rows[g].astype(F32), approximate=True) * state).astype(BF16))
+    for run in range(runs):
+        at = slice(run * LANES, (run + 1) * LANES)
+        state = states[:, at] + decays[:, at] * entering[run : run + 1]
+        branches.append((gated[:, at] * state).astype(BF16))
     copy.wait()
-    acc = dot(branches[0], weight[0])
-    for g in range(1, len(branches)):
-        acc = acc + dot(branches[g], weight[g])
+    acc, per_half = None, runs // weight.shape[0]
+    for g in range(weight.shape[0]):
+        part = dot(jnp.concatenate(branches[g * per_half : (g + 1) * per_half], axis=1), weight[g])
+        acc = part if acc is None else acc + part
     out[...] = acc.astype(BF16).reshape(out.shape)
 
 
-def route_kernel(ids, weights, select, merge):
+def side_kernel(ids, weights, gate_rows, stream, gain, bias, select, merge, gated, scaled, gain_kept, bias_kept, wide):
+    route(ids, weights, select, merge)
+    wide[...] = gate_rows[...].astype(F32)
+    runs = gated.shape[1] // LANES
+    groups = 2
+    for run in range(runs):
+        g, c = divmod(run, runs // groups)
+        values = wide[pl.ds(c * groups + g, gated.shape[0], stride=runs), :]
+        gated[:, run * LANES : (run + 1) * LANES] = jax.nn.gelu(values, approximate=True)
+    scaled[...] = RESIDUAL_SCALE * stream[...].astype(F32)
+    gain_kept[...] = gain[...]
+    bias_kept[...] = bias[...]
+
+
+def route(ids, weights, select, merge):
     slot_count, rows = select.shape[0], ids.shape[1]
     slot = lax.broadcasted_iota(jnp.int32, (slot_count, rows), 0)
     names = jnp.zeros((slot_count, rows), F32)
@@ -172,11 +194,11 @@
     merge[...] = jnp.where(taken, weight, 0.0).T[: merge.shape[0]]
 
 
-def mix_kernel(parts, stream, gain, bias, select, normed, outgoing):
+def mix_kernel(parts, scaled, gain, bias, select, normed, outgoing):
     mixed = parts[0].astype(F32)
     for j in range(1, parts.shape[0]):
         mixed = mixed + parts[j].astype(F32)
-    rows = layer_norm(RESIDUAL_SCALE * stream[...].astype(F32) + mixed, gain[...], bias[...]).astype(BF16)
+    rows = layer_norm(scaled[...] + mixed, gain[...], bias[...]).astype(BF16)
     normed[...] = rows
     outgoing[...] = dot(select[...], rows).astype(BF16).reshape(outgoing.shape)
 
@@ -190,10 +212,11 @@
     base[...] = RESIDUAL_SCALE * rows.astype(F32) + dot(hidden, down_w[...])
 
 
-def expert_kernel(rows, g0, g1, g2, g3, u0, u1, u2, u3, d0, d1, d2, d3a, d3b, out, pairs, down, sems):
-    width = g0.shape[1]
+def expert_kernel(rows, gate_own, up_own, left, right, gate_far, up_far, d0, d1, d2, d3a, d3b, out, pairs, down, sems):
+    depth, width = gate_own.shape
+    near = [(side.at[0:depth], side.at[depth : 2 * depth]) for side in (left, right)]
     moves = []
-    for j, (gate_w, up_w) in enumerate(((g0, u0), (g1, u1), (g2, u2), (g3, u3))):
+    for j, (gate_w, up_w) in enumerate([(gate_own, up_own), *near, (gate_far, up_far)]):
         moves += [(gate_w, pairs.at[j, :, 0:width]), (up_w, pairs.at[j, :, width : 2 * width])]
     at = 0
     for piece in (d0, d1, d2, d3a, d3b):
@@ -265,39 +288,52 @@
     channels = groups * half
     shape, kept = jax.ShapeDtypeStruct, pltpu.VMEM
 
-    rows = jnp.transpose(recurrence_input, (1, 0, 2))
-    margin = 8
-    border = lax.ppermute(rows[:, length - margin :], "sp", [(i, i + 1) for i in range(sp_count - 1)])
+    rows = flat(recurrence_input)
+    margin = 16
+    border = lax.ppermute(rows[rows.shape[0] - margin :], "sp", [(i, i + 1) for i in range(sp_count - 1)])
 
     gate_w, up_w, down_w = routed_gate_weight[0], routed_up_weight[0], routed_down_weight[0]
-    gate_left, up_right = turned(gate_w, 1), turned(up_w, -1)
-    up_left, gate_right = turned(up_w, 1), turned(gate_w, -1)
-
-    own_index = lax.axis_index("tp")
-    own_ids = lax.dynamic_slice_in_dim(routed_expert_index.T, own_index * quarter, quarter, 1)
-    own_weights = lax.dynamic_slice_in_dim(routed_expert_weight.T, own_index * quarter, quarter, 1)
-    fill = ((0, 0), (0, LANES - quarter))
-    select, merge = kernel_call(
-        route_kernel,
-        [kept((slot_count, quarter), BF16), shape((quarter, slot_count), F32)],
-        (jnp.pad(own_ids, fill, constant_values=-1), "vmem"),
-        (jnp.pad(own_weights, fill), "vmem"),
-    )
+    pair_w = jnp.concatenate([gate_w, up_w], axis=0)
+    pair_left, pair_right = turned(pair_w, 1), turned(pair_w, -1)
+    down_left, down_right = turned(down_w, 1), turned(down_w, -1)
 
     runs = channels // LANES
     decays, states, totals = kernel_call(
         local_kernel,
-        [kept((length, channels), F32), kept((length, channels), F32), shape((sp_count, 2 * runs, LANES), F32)],
-        (rows, "vmem"),
+        [kept((length, channels), F32), kept((length, channels), F32), shape((sp_count, 2 * runs, LANES), BF16)],
+        rows,
         (border, "vmem"),
         convolution_taps,
         first_group_gates,
         second_group_gates,
         channel_decay,
-        (jnp.transpose(position_log_extra, (1, 0, 2)), "vmem"),
-        scratch=(pltpu.VMEM((margin + length, half), F32), pltpu.VMEM((half, 2 * half), BF16)),
+        flat(position_log_extra),
+        scratch=(pltpu.VMEM((margin + rows.shape[0], LANES), F32), pltpu.VMEM((half, 2 * half), BF16)),
     )
     spans = swapped(totals, "sp")
+
+    own_index = lax.axis_index("tp")
+    own_ids = lax.dynamic_slice_in_dim(routed_expert_index.T, own_index * quarter, quarter, 1)
+    own_weights = lax.dynamic_slice_in_dim(routed_expert_weight.T, own_index * quarter, quarter, 1)
+    fill = ((0, 0), (0, LANES - quarter))
+    select, merge, gated, *norm_parts = kernel_call(
+        side_kernel,
+        [
+            kept((slot_count, quarter), BF16),
+            shape((quarter, slot_count), F32),
+            kept((length, channels), F32),
+            kept((quarter, width), F32),
+            kept((1, width), F32),
+            kept((1, width), F32),
+        ],
+        (jnp.pad(own_ids, fill, constant_values=-1), "vmem"),
+        (jnp.pad(own_weights, fill), "vmem"),
+        flat(output_gate_input),
+        stream,
+        first_norm_gain.reshape(1, width),
+        first_norm_bias.reshape(1, width),
+        scratch=(pltpu.VMEM(rows.shape, F32),),
+    )
     parts = kernel_call(
         project_kernel,
         shape((tp_count, quarter, width), BF16),
@@ -305,22 +341,20 @@
         (spans, "vmem"),
         (decays, "vmem"),
         (states, "vmem"),
-        (jnp.transpose(output_gate_input, (1, 0, 2)), "vmem"),
+        (gated, "vmem"),
         (recurrence_output_weight, "hbm"),
         scratch=(pltpu.VMEM(recurrence_output_weight.shape, BF16), pltpu.SemaphoreType.DMA((1,))),
     )
     parts = swapped(parts, "tp")
 
-    down_left, down_right = turned(down_w, 1), turned(down_w, -1)
-    gate_far, up_far = turned(gate_left, 1), turned(up_right, -1)
+    depth = gate_w.shape[0]
+    gate_far, up_far = turned(pair_left[:depth], 1), turned(pair_right[depth:], -1)
 
     normed, outgoing = kernel_call(
         mix_kernel,
         [kept((quarter, width), BF16), shape((expert_count, SLOTS, width), BF16)],
         (parts, "vmem"),
-        stream,
-        first_norm_gain.reshape(1, width),
-        first_norm_bias.reshape(1, width),
+        *((x, "vmem") for x in norm_parts),
         (select, "vmem"),
     )
     arrived = swapped(outgoing, "sp")
@@ -338,7 +372,7 @@
         shared_down_weight,
         *last,
     )
-    weights = (gate_w, gate_left, gate_right, gate_far, up_w, up_left, up_right, up_far, down_w, down_left, down_right, *down_far)
+    weights = (gate_w, up_w, pair_left, pair_right, gate_far, up_far, down_w, down_left, down_right, *down_far)
     leaving = kernel_call(
         expert_kernel,
         kept((expert_count, SLOTS, width), BF16),
@@ -347,7 +381,7 @@
         scratch=(
             pltpu.VMEM((tp_count, width, 2 * gate_w.shape[1]), BF16),
             pltpu.VMEM((tp_count * down_w.shape[0], width), BF16),
-            pltpu.SemaphoreType.DMA((len(weights),)),
+            pltpu.SemaphoreType.DMA((len(weights) + 2,)),
         ),
     )
     returned = swapped(leaving, "sp")

time: 139 us -> 138 us (level)
  waiting for transfers between devices: 65.6 us -> 41 us
  blocking collectives: 0 us -> 21.6 us
  other arithmetic: 0 us -> 2.23 us
    all_to_all x0 -> x1, blocking collectives: none -> 21.6 us  [swapped(): return lax.all_to_all(pieces, axis, 0, 0, tiled=True)]
    ppermute x10 -> x8, waiting for transfers between devices: 36.3 us -> 22.7 us  [turned(): lax.ppermute(shard, 'tp', [(i, (i + by) % count) for i in range(count)])]
    all_to_all x4 -> x3, waiting for transfers between devices: 29.3 us -> 17.6 us  [swapped(): return lax.all_to_all(pieces, axis, 0, 0, tiled=True)]
    concatenate x0 -> x1, other arithmetic: none -> 2.23 us  [shards(): pair_w = jnp.concatenate([gate_w, up_w], axis=0)]
    unnamed x31 -> x20, local copies, waits for them, and re-layouts: 3.42 us -> 2.14 us
    all_to_all x4 -> x3, starting transfers between devices: 35.6 us -> 36 us  [swapped(): return lax.all_to_all(pieces, axis, 0, 0, tiled=True)]
    ppermute x10 -> x8, starting transfers between devices: 11.4 us -> 11.3 us  [turned(): lax.ppermute(shard, 'tp', [(i, (i + by) % count) for i in range(count)])]
  transfers between devices with their start and end apart: 15 -> 12, of which waited for: 9 -> 5; matrix products, arithmetic and copies ran while one was open for 1% -> 2% of each run, Pallas kernels for 5% -> 6%
where the time goes in v3:
time: 138 us; the launch traced here: 137 us
  starting transfers between devices  51.7 us (37%)
  waiting for transfers between devices  41 us (30%)
  blocking collectives  21.6 us (16%)
  Pallas kernels  17.3 us (13%)
  local copies, waits for them, and re-layouts  3.12 us (2%)
  other arithmetic  2.23 us (2%)
    all_to_all x3, starting transfers between devices, swapped(): return lax.all_to_all(pieces, axis, 0, 0, tiled=True)  36 us
    ppermute x8, waiting for transfers between devices, turned(): lax.ppermute(shard, 'tp', [(i, (i + by) % count) for i in range(count)])  22.7 us
    all_to_all x1, blocking collectives, swapped(): return lax.all_to_all(pieces, axis, 0, 0, tiled=True)  21.6 us
    all_to_all x3, waiting for transfers between devices, swapped(): return lax.all_to_all(pieces, axis, 0, 0, tiled=True)  17.6 us
    pallas_call x7, Pallas kernels, kernel_call(): pl.pallas_call(body, out_shape=out_shape, in_specs=specs, out_specs=[VMEM...  17.3 us
    ppermute x8, starting transfers between devices, turned(): lax.ppermute(shard, 'tp', [(i, (i + by) % count) for i in range(count)])  11.3 us
    ppermute x1, starting transfers between devices, shards(): lax.ppermute(rows[rows.shape[0] - margin:], 'sp', [(i, i + 1) for i in ra...  4.49 us
  transfers between devices with their start and end apart: 12, of which 5 were waited for; matrix products, arithmetic and copies ran while one was open for 2% of the time, Pallas kernels for 6%

profile of v3, /device:TPU:1, one launch (start us, length us, event | category | flops | bytes accessed | tf_op | source)
XLA Modules:
  0.0 137.2 jit_solution(16099609981526993542)
XLA Ops:
  0.0 0.0 copy-start
  0.0 0.0 copy-start.9
  0.0 0.7 slice.24
  0.7 4.5 %collective-permute-start = (bf16[16,128]{1,0:T(8,128)(2,1)S(1)}, bf16[16,128]{1,0:T(8,128)(2,1)S(1)}, u32[]{:S(2)}, u32[]{:S(2)}) collective-permute-start(bf16[16,128]{1,0:T(8,128)(2,1)S(1)} %bitcast.43), channel_id=1, source_target_pairs={{0,4},{4,8},{8,12},{12,16},{16,20},{20,24},{24,28},{28,32},{32,36}... | collective-permute-start | bytes 12296 | tf_op jit(solution)/shard_map/ppermute | solution.py:293
  5.2 0.7 collective-permute-done.border
  6.0 3.0 %shard_map.199 = (f32[128,512]{1,0:T(8,128)S(1)}, f32[128,512]{1,0:T(8,128)S(1)}, bf16[64,8,128]{2,1,0:T(8,128)(2,1)}) custom-call(bf16[512,128]{1,0:T(8,128)(2,1)} %bitcast.37, bf16[16,128]{1,0:T(8,128)(2,1)S(1)} %collective-permute-done.border, bf16[4,2,256]{2,1,0:T(2,128)(2,1)} %taps.1, bf16[2,4,64,64]{3,2,1,0:T(8,128)(2,1)} %small_maps.1, ...), custom_call_target="tpu_custom_call" | custom-call | tf_op jit(solution)/shard_map/pallas_call | solution.py:27
  8.9 13.5 %all-to-all-start = ((bf16[64,8,128]{2,1,0:T(8,128)(2,1)}), bf16[64,8,128]{2,1,0:T(8,128)(2,1)S(1)}, u32[]{:S(2)}, u32[]{:S(2)}) async-start(bf16[64,8,128]{2,1,0:T(8,128)(2,1)} %get-tuple-element.20), calls=%async_computation | async-start | bytes 262144 | tf_op jit(solution)/shard_map/all_to_all | solution.py:256
  22.5 2.2 %pad_maximum_fusion = bf16[4096,128]{1,0:T(8,128)(2,1)} fusion(bf16[2048,128]{1,0:T(8,128)(2,1)} %bitcast.30, bf16[2048,128]{1,0:T(8,128)(2,1)} %bitcast.28), kind=kLoop, calls=%fused_computation | loop fusion | flops 2097152 | bytes 2097152 | tf_op jit(solution)/shard_map/concatenate | solution.py:296
  24.7 1.3 collective-permute-start.1
  26.0 1.4 %collective-permute-start.2 = (bf16[4096,128]{1,0:T(8,128)(2,1)}, bf16[4096,128]{1,0:T(8,128)(2,1)S(1)}, u32[]{:S(2)}, u32[]{:S(2)}) collective-permute-start(bf16[4096,128]{1,0:T(8,128)(2,1)} %pad_maximum_fusion), channel_id=1, source_target_pairs={{0,3},{1,0},{2,1},{3,2},{4,7},{5,4},{6,5},{7,6},{8,11},{9,8},{10,9... | collective-permute-start | bytes 3145736 | tf_op jit(solution)/shard_map/ppermute | solution.py:252
  27.4 0.0 copy-done
  27.4 0.1 dynamic-slice_bitcast_fusion.1
  27.5 0.0 copy-done.9
  27.5 0.1 dynamic-slice_bitcast_fusion
  27.6 1.3 shard_map.200
  28.9 0.0 copy-start.1
  28.9 0.6 copy-done.1
  29.5 4.1 %all-to-all-done.spans = bf16[64,8,128]{2,1,0:T(8,128)(2,1)S(1)} async-done(((bf16[64,8,128]{2,1,0:T(8,128)(2,1)}), bf16[64,8,128]{2,1,0:T(8,128)(2,1)S(1)}, u32[]{:S(2)}, u32[]{:S(2)}) %all-to-all-start) | async-done | bytes 131104 | tf_op jit(solution)/shard_map/all_to_all | solution.py:256
  33.5 2.1 %shard_map.201 = bf16[4,32,2048]{2,1,0:T(8,128)(2,1)S(1)} custom-call(s32[1]{0:T(128)} %bitcast.mine, bf16[64,8,128]{2,1,0:T(8,128)(2,1)S(1)} %all-to-all-done.spans, f32[128,512]{1,0:T(8,128)S(1)} %get-tuple-element.21.decays, f32[128,512]{1,0:T(8,128)S(1)} %get-tuple-element.22.states, f32[128,512]{1,0:T(8,128)S(1)} %get-tuple-element.23.gated, ...), custom_call_target="tpu_custom_call" | custom-call | tf_op jit(solution)/shard_map/pallas_call | solution.py:27
  35.6 21.6 %all_to_all.20.parts = bf16[4,32,2048]{2,1,0:T(8,128)(2,1)S(1)} all-to-all(bf16[4,32,2048]{2,1,0:T(8,128)(2,1)S(1)} %shard_map.201), channel_id=1, replica_groups=mesh['sp'=64,'tp'=4] {'tp'}, dimensions={0} | all-to-all | bytes 1048576 | tf_op jit(solution)/shard_map/all_to_all | solution.py:256
  57.2 1.4 shard_map.202
  58.6 11.2 %all-to-all-start.2 = ((bf16[64,2,2048]{2,1,0:T(2,128)(2,1)}), bf16[64,2,2048]{2,1,0:T(2,128)(2,1)S(1)}, u32[]{:S(2)}, u32[]{:S(2)}) async-start(bf16[64,2,2048]{2,1,0:T(2,128)(2,1)} %get-tuple-element.28), calls=%async_computation.2 | async-start | bytes 1048576 | tf_op jit(solution)/shard_map/all_to_all | solution.py:256
  69.8 0.9 collective-permute-start.5
  70.7 1.8 %collective-permute-start.6 = (bf16[128,2048]{1,0:T(8,128)(2,1)}, bf16[128,2048]{1,0:T(8,128)(2,1)S(1)}, u32[]{:S(2)}, u32[]{:S(2)}) collective-permute-start(bf16[128,2048]{1,0:T(8,128)(2,1)} %bitcast.33), channel_id=1, source_target_pairs={{0,3},{1,0},{2,1},{3,2},{4,7},{5,4},{6,5},{7,6},{8,11},{9,8},{10,9... | collective-permute-start | bytes 1572872 | tf_op jit(solution)/shard_map/ppermute | solution.py:252
  72.6 0.0 collective-permute-done.1.left
  72.6 0.0 copy-start.2
  72.6 0.1 collective-permute-start.3
  72.7 0.0 collective-permute-done.2.right
  72.7 0.0 copy-start.3
  72.8 2.7 %collective-permute-start.4 = (bf16[2048,128]{1,0:T(8,128)(2,1)S(1)}, bf16[2048,128]{1,0:T(8,128)(2,1)}, u32[]{:S(2)}, u32[]{:S(2)}) collective-permute-start(bf16[2048,128]{1,0:T(8,128)(2,1)S(1)} %slice.26), channel_id=1, source_target_pairs={{0,3},{1,0},{2,1},{3,2},{4,7},{5,4},{6,5},{7,6},{8,11},{9,8},{10,9... | collective-permute-start | bytes 1572872 | tf_op jit(solution)/shard_map/ppermute | solution.py:252
  75.5 8.9 %collective-permute-done.5.d1 = bf16[128,2048]{1,0:T(8,128)(2,1)S(1)} collective-permute-done((bf16[128,2048]{1,0:T(8,128)(2,1)}, bf16[128,2048]{1,0:T(8,128)(2,1)S(1)}, u32[]{:S(2)}, u32[]{:S(2)}) %collective-permute-start.5) | collective-permute-done | bytes 524320 | tf_op jit(solution)/shard_map/ppermute | solution.py:252
  84.3 0.0 copy-start.4
  84.4 0.1 collective-permute-start.7
  84.4 0.0 collective-permute-done.6.d2
  84.5 0.0 copy-start.5
  84.5 2.9 %collective-permute-start.8 = (bf16[64,2048]{1,0:T(8,128)(2,1)S(1)}, bf16[64,2048]{1,0:T(8,128)(2,1)S(1)}, u32[]{:S(2)}, u32[]{:S(2)}) collective-permute-start(bf16[64,2048]{1,0:T(8,128)(2,1)S(1)} %slice.28), channel_id=1, source_target_pairs={{0,3},{1,0},{2,1},{3,2},{4,7},{5,4},{6,5},{7,6},{8,11},{9,8},{10,9... | collective-permute-start | bytes 786440 | tf_op jit(solution)/shard_map/ppermute | solution.py:252
  87.4 13.8 %collective-permute-done.7.d3a = bf16[64,2048]{1,0:T(8,128)(2,1)S(1)} collective-permute-done((bf16[64,2048]{1,0:T(8,128)(2,1)S(1)}, bf16[64,2048]{1,0:T(8,128)(2,1)S(1)}, u32[]{:S(2)}, u32[]{:S(2)}) %collective-permute-start.7) | collective-permute-done | bytes 262176 | tf_op jit(solution)/shard_map/ppermute | solution.py:252
  101.2 0.0 copy-start.7
  101.2 0.0 collective-permute-done.8.d3b
  101.2 0.0 copy-start.8
  101.2 0.0 collective-permute-done.3.gate_far
  101.2 0.0 copy-done.4
  101.2 0.0 copy-done.5
  101.2 0.7 copy-done.8
  101.9 0.0 copy-start.6
  101.9 0.0 collective-permute-done.4.up_far
  101.9 0.0 all-to-all-done.2.rows
  102.0 0.0 copy-done.2
  102.0 0.0 copy-done.3
  102.0 0.0 copy-done.7
  102.0 0.8 copy-done.6
  102.7 4.3 %shard_map.203 = bf16[64,2,2048]{2,1,0:T(2,128)(2,1)} custom-call(bf16[64,2,2048]{2,1,0:T(2,128)(2,1)S(1)} %all-to-all-done.2.rows, bf16[2048,128]{1,0:T(8,128)(2,1)} %bitcast.29, bf16[2048,128]{1,0:T(8,128)(2,1)} %bitcast.31, bf16[4096,128]{1,0:T(8,128)(2,1)} %copy-done.2, bf16[4096,128]{1,0:T(8,128)(2,1)} %copy-done.3, bf16[2048,128]{1,0:T(8,128)(2,1)} %copy-done.6, ...), custom_call_target="tpu_custom_call" | custom-call | tf_op jit(solution)/shard_map/pallas_call | solution.py:27
  107.1 11.2 %all-to-all-start.3 = ((bf16[64,2,2048]{2,1,0:T(2,128)(2,1)}), bf16[64,2,2048]{2,1,0:T(2,128)(2,1)S(1)}, u32[]{:S(2)}, u32[]{:S(2)}) async-start(bf16[64,2,2048]{2,1,0:T(2,128)(2,1)} %shard_map.203), calls=%async_computation.3 | async-start | bytes 1048576 | tf_op jit(solution)/shard_map/all_to_all | solution.py:256
  118.3 4.1 %shard_map.204 = (f32[32,2048]{1,0:T(8,128)S(1)}, f32[32,128]{1,0:T(8,128)S(1)}, f32[1,2048]{1,0:T(1,128)S(1)}, f32[1,2048]{1,0:T(1,128)S(1)}) custom-call(bf16[32,2048]{1,0:T(8,128)(2,1)S(1)} %get-tuple-element.29.normed, bf16[2048,512]{1,0:T(8,128)(2,1)} %gate_w.1, bf16[2048,512]{1,0:T(8,128)(2,1)} %up_w.1, bf16[512,2048]{1,0:T(8,128)(2,1)} %down_w.1, ...), custom_call_target="tpu_custom_call" | custom-call | tf_op jit(solution)/shard_map/pallas_call | solution.py:27
  122.5 13.5 %all-to-all-done.3.returned = bf16[64,2,2048]{2,1,0:T(2,128)(2,1)S(1)} async-done(((bf16[64,2,2048]{2,1,0:T(2,128)(2,1)}), bf16[64,2,2048]{2,1,0:T(2,128)(2,1)S(1)}, u32[]{:S(2)}, u32[]{:S(2)}) %all-to-all-start.3) | async-done | bytes 524320 | tf_op jit(solution)/shard_map/all_to_all | solution.py:256
  136.0 1.2 shard_map.205
  (6 shorter events, 0.1 us)
Async XLA Ops:
  0.0 27.4 %copy-start = (s32[128,4]{0,1:T(4,128)S(1)}, s32[128,4]{0,1:T(4,128)}, u32[]{:S(2)}) copy-start(s32[128,4]{0,1:T(4,128)} %param.32) | copy-start | bytes 6148
  0.0 27.5 %copy-start.9 = (f32[128,4]{0,1:T(4,128)S(1)}, f32[128,4]{0,1:T(4,128)}, u32[]{:S(2)}) copy-start(f32[128,4]{0,1:T(4,128)} %param.33) | copy-start | bytes 6148
  0.7 5.2 %collective-permute-start = (bf16[16,128]{1,0:T(8,128)(2,1)S(1)}, bf16[16,128]{1,0:T(8,128)(2,1)S(1)}, u32[]{:S(2)}, u32[]{:S(2)}) collective-permute-start(bf16[16,128]{1,0:T(8,128)(2,1)S(1)} %bitcast.43), channel_id=1, source_target_pairs={{0,4},{4,8},{8,12},{12,16},{16,20},{20,24},{24,28},{28,32},{32,36}... | collective-permute-start | bytes 12296 | tf_op jit(solution)/shard_map/ppermute | solution.py:293
  8.9 24.6 %all-to-all-start = ((bf16[64,8,128]{2,1,0:T(8,128)(2,1)}), bf16[64,8,128]{2,1,0:T(8,128)(2,1)S(1)}, u32[]{:S(2)}, u32[]{:S(2)}) async-start(bf16[64,8,128]{2,1,0:T(8,128)(2,1)} %get-tuple-element.20), calls=%async_computation | async-start | bytes 262144 | tf_op jit(solution)/shard_map/all_to_all | solution.py:256
  24.7 47.9 %collective-permute-start.1 = (bf16[4096,128]{1,0:T(8,128)(2,1)}, bf16[4096,128]{1,0:T(8,128)(2,1)S(1)}, u32[]{:S(2)}, u32[]{:S(2)}) collective-permute-start(bf16[4096,128]{1,0:T(8,128)(2,1)} %pad_maximum_fusion), channel_id=1, source_target_pairs={{0,1},{1,2},{2,3},{3,0},{4,5},{5,6},{6,7},{7,4},{8,9},{9,10},{10,1... | collective-permute-start | bytes 3145736 | tf_op jit(solution)/shard_map/ppermute | solution.py:252
  26.0 46.7 %collective-permute-start.2 = (bf16[4096,128]{1,0:T(8,128)(2,1)}, bf16[4096,128]{1,0:T(8,128)(2,1)S(1)}, u32[]{:S(2)}, u32[]{:S(2)}) collective-permute-start(bf16[4096,128]{1,0:T(8,128)(2,1)} %pad_maximum_fusion), channel_id=1, source_target_pairs={{0,3},{1,0},{2,1},{3,2},{4,7},{5,4},{6,5},{7,6},{8,11},{9,8},{10,9... | collective-permute-start | bytes 3145736 | tf_op jit(solution)/shard_map/ppermute | solution.py:252
  28.9 0.6 copy-start.1
  58.6 43.4 %all-to-all-start.2 = ((bf16[64,2,2048]{2,1,0:T(2,128)(2,1)}), bf16[64,2,2048]{2,1,0:T(2,128)(2,1)S(1)}, u32[]{:S(2)}, u32[]{:S(2)}) async-start(bf16[64,2,2048]{2,1,0:T(2,128)(2,1)} %get-tuple-element.28), calls=%async_computation.2 | async-start | bytes 1048576 | tf_op jit(solution)/shard_map/all_to_all | solution.py:256
  69.8 14.5 %collective-permute-start.5 = (bf16[128,2048]{1,0:T(8,128)(2,1)}, bf16[128,2048]{1,0:T(8,128)(2,1)S(1)}, u32[]{:S(2)}, u32[]{:S(2)}) collective-permute-start(bf16[128,2048]{1,0:T(8,128)(2,1)} %bitcast.32), channel_id=1, source_target_pairs={{0,1},{1,2},{2,3},{3,0},{4,5},{5,6},{6,7},{7,4},{8,9},{9,10},{10,1... | collective-permute-start | bytes 1572872 | tf_op jit(solution)/shard_map/ppermute | solution.py:252
  70.7 13.7 %collective-permute-start.6 = (bf16[128,2048]{1,0:T(8,128)(2,1)}, bf16[128,2048]{1,0:T(8,128)(2,1)S(1)}, u32[]{:S(2)}, u32[]{:S(2)}) collective-permute-start(bf16[128,2048]{1,0:T(8,128)(2,1)} %bitcast.33), channel_id=1, source_target_pairs={{0,3},{1,0},{2,1},{3,2},{4,7},{5,4},{6,5},{7,6},{8,11},{9,8},{10,9... | collective-permute-start | bytes 1572872 | tf_op jit(solution)/shard_map/ppermute | solution.py:252
  72.6 29.4 %copy-start.2 = (bf16[4096,128]{1,0:T(8,128)(2,1)}, bf16[4096,128]{1,0:T(8,128)(2,1)S(1)}, u32[]{:S(2)}) copy-start(bf16[4096,128]{1,0:T(8,128)(2,1)S(1)} %collective-permute-done.1.left) | copy-start | bytes 3145732
  72.6 28.6 %collective-permute-start.3 = (bf16[2048,128]{1,0:T(8,128)(2,1)S(1)}, bf16[2048,128]{1,0:T(8,128)(2,1)S(1)}, u32[]{:S(2)}, u32[]{:S(2)}) collective-permute-start(bf16[2048,128]{1,0:T(8,128)(2,1)S(1)} %slice.25), channel_id=1, source_target_pairs={{0,1},{1,2},{2,3},{3,0},{4,5},{5,6},{6,7},{7,4},{8,9},{9,10},{10,1... | collective-permute-start | bytes 1572872 | tf_op jit(solution)/shard_map/ppermute | solution.py:252
  72.7 29.3 %copy-start.3 = (bf16[4096,128]{1,0:T(8,128)(2,1)}, bf16[4096,128]{1,0:T(8,128)(2,1)S(1)}, u32[]{:S(2)}) copy-start(bf16[4096,128]{1,0:T(8,128)(2,1)S(1)} %collective-permute-done.2.right) | copy-start | bytes 3145732
  72.8 29.2 %collective-permute-start.4 = (bf16[2048,128]{1,0:T(8,128)(2,1)S(1)}, bf16[2048,128]{1,0:T(8,128)(2,1)}, u32[]{:S(2)}, u32[]{:S(2)}) collective-permute-start(bf16[2048,128]{1,0:T(8,128)(2,1)S(1)} %slice.26), channel_id=1, source_target_pairs={{0,3},{1,0},{2,1},{3,2},{4,7},{5,4},{6,5},{7,6},{8,11},{9,8},{10,9... | collective-permute-start | bytes 1572872 | tf_op jit(solution)/shard_map/ppermute | solution.py:252
  84.3 16.9 %copy-start.4 = (bf16[128,2048]{1,0:T(8,128)(2,1)}, bf16[128,2048]{1,0:T(8,128)(2,1)S(1)}, u32[]{:S(2)}) copy-start(bf16[128,2048]{1,0:T(8,128)(2,1)S(1)} %collective-permute-done.5.d1) | copy-start | bytes 1572868
  84.4 16.8 %collective-permute-start.7 = (bf16[64,2048]{1,0:T(8,128)(2,1)S(1)}, bf16[64,2048]{1,0:T(8,128)(2,1)S(1)}, u32[]{:S(2)}, u32[]{:S(2)}) collective-permute-start(bf16[64,2048]{1,0:T(8,128)(2,1)S(1)} %slice.27), channel_id=1, source_target_pairs={{0,1},{1,2},{2,3},{3,0},{4,5},{5,6},{6,7},{7,4},{8,9},{9,10},{10,1... | collective-permute-start | bytes 786440 | tf_op jit(solution)/shard_map/ppermute | solution.py:252
  84.5 16.8 %copy-start.5 = (bf16[128,2048]{1,0:T(8,128)(2,1)}, bf16[128,2048]{1,0:T(8,128)(2,1)S(1)}, u32[]{:S(2)}) copy-start(bf16[128,2048]{1,0:T(8,128)(2,1)S(1)} %collective-permute-done.6.d2) | copy-start | bytes 1572868
  84.5 16.7 %collective-permute-start.8 = (bf16[64,2048]{1,0:T(8,128)(2,1)S(1)}, bf16[64,2048]{1,0:T(8,128)(2,1)S(1)}, u32[]{:S(2)}, u32[]{:S(2)}) collective-permute-start(bf16[64,2048]{1,0:T(8,128)(2,1)S(1)} %slice.28), channel_id=1, source_target_pairs={{0,3},{1,0},{2,1},{3,2},{4,7},{5,4},{6,5},{7,6},{8,11},{9,8},{10,9... | collective-permute-start | bytes 786440 | tf_op jit(solution)/shard_map/ppermute | solution.py:252
  101.2 0.8 copy-start.7
  101.2 0.8 copy-start.8
  101.9 0.8 copy-start.6
  107.1 28.9 %all-to-all-start.3 = ((bf16[64,2,2048]{2,1,0:T(2,128)(2,1)}), bf16[64,2,2048]{2,1,0:T(2,128)(2,1)S(1)}, u32[]{:S(2)}, u32[]{:S(2)}) async-start(bf16[64,2,2048]{2,1,0:T(2,128)(2,1)} %shard_map.203), calls=%async_computation.3 | async-start | bytes 1048576 | tf_op jit(solution)/shard_map/all_to_all | solution.py:256

commit v4 on v3

--- a/solution.py
+++ b/solution.py
@@ -135,28 +135,24 @@
         totals[j] = span
 
 
-def entering_state(spans, mine):
+def entering_state(spans, ahead):
     half = spans.shape[1] // 2
-    span = lax.broadcasted_iota(jnp.int32, (spans.shape[0], half, LANES), 0)
-    logs = spans[:, :half].astype(F32)
-    decays = jnp.where(span < mine, jnp.exp(logs), 1.0)
-    ends = jnp.where(span < mine, spans[:, half:].astype(F32), 0.0)
+    passed = (ahead[...] > 0.0)[:, None, :]
+    decays = jnp.where(passed, jnp.exp(spans[:, :half].astype(F32)), 1.0)
+    ends = jnp.where(passed, spans[:, half:].astype(F32), 0.0)
     state = ends[0]
     for j in range(1, spans.shape[0] - 1):
         state = decays[j] * state + ends[j]
     return state
 
 
-def project_kernel(mine, spans, decays, states, gated, weight_far, out, weight, sems):
-    (copy,) = fetched([(weight_far, weight)], sems)
-    entering = entering_state(spans, mine[0])
+def project_kernel(spans, ahead, decays, states, weight, out):
+    entering = entering_state(spans, ahead)
     runs = entering.shape[0]
     branches = []
     for run in range(runs):
         at = slice(run * LANES, (run + 1) * LANES)
-        state = states[:, at] + decays[:, at] * entering[run : run + 1]
-        branches.append((gated[:, at] * state).astype(BF16))
-    copy.wait()
+        branches.append((states[:, at] + decays[:, at] * entering[run : run + 1]).astype(BF16))
     acc, per_half = None, runs // weight.shape[0]
     for g in range(weight.shape[0]):
         part = dot(jnp.concatenate(branches[g * per_half : (g + 1) * per_half], axis=1), weight[g])
@@ -164,18 +160,24 @@
     out[...] = acc.astype(BF16).reshape(out.shape)
 
 
-def side_kernel(ids, weights, gate_rows, stream, gain, bias, select, merge, gated, scaled, gain_kept, bias_kept, wide):
+def side_kernel(mine, ids, weights, decays, states, gate_rows, stream, gain, bias, projection, *rest):
+    select, merge, gated_decays, gated_states, stream_kept, gain_kept, bias_kept, projection_kept, ahead, wide, sems = rest
+    (copy,) = fetched([(projection, projection_kept)], sems)
+    ahead[...] = jnp.where(lax.broadcasted_iota(jnp.int32, ahead.shape, 0) < mine[0], 1.0, 0.0)
     route(ids, weights, select, merge)
     wide[...] = gate_rows[...].astype(F32)
-    runs = gated.shape[1] // LANES
+    length, runs = decays.shape[0], decays.shape[1] // LANES
     groups = 2
     for run in range(runs):
         g, c = divmod(run, runs // groups)
-        values = wide[pl.ds(c * groups + g, gated.shape[0], stride=runs), :]
-        gated[:, run * LANES : (run + 1) * LANES] = jax.nn.gelu(values, approximate=True)
-    scaled[...] = RESIDUAL_SCALE * stream[...].astype(F32)
+        values = jax.nn.gelu(wide[pl.ds(c * groups + g, length, stride=runs), :], approximate=True)
+        at = slice(run * LANES, (run + 1) * LANES)
+        gated_decays[:, at] = values * decays[:, at]
+        gated_states[:, at] = values * states[:, at]
+    stream_kept[...] = stream[...]
     gain_kept[...] = gain[...]
     bias_kept[...] = bias[...]
+    copy.wait()
 
 
 def route(ids, weights, select, merge):
@@ -194,43 +196,56 @@
     merge[...] = jnp.where(taken, weight, 0.0).T[: merge.shape[0]]
 
 
-def mix_kernel(parts, scaled, gain, bias, select, normed, outgoing):
+def mix_kernel(parts, stream, gain, bias, select, normed, outgoing):
     mixed = parts[0].astype(F32)
     for j in range(1, parts.shape[0]):
         mixed = mixed + parts[j].astype(F32)
-    rows = layer_norm(scaled[...] + mixed, gain[...], bias[...]).astype(BF16)
+    rows = layer_norm(RESIDUAL_SCALE * stream[...].astype(F32) + mixed, gain[...], bias[...]).astype(BF16)
     normed[...] = rows
     outgoing[...] = dot(select[...], rows).astype(BF16).reshape(outgoing.shape)
 
 
-def shared_kernel(normed, gate_w, up_w, down_w, merge, gain, bias, base, *kept):
+def pair_moves(pairs, weights):
+    moves = []
+    for j, (gate_w, up_w) in enumerate(weights):
+        width = gate_w.shape[1]
+        moves += [(gate_w, pairs.at[j, :, 0:width]), (up_w, pairs.at[j, :, width : 2 * width])]
+    return moves
+
+
+def shared_kernel(normed, gate_w, up_w, down_w, merge, gain, bias, g0, u0, g1, u1, base, *rest):
+    *kept, near, sems = rest
+    copies = fetched(pair_moves(near, ((g0, u0), (g1, u1))), sems)
     for target, source in zip(kept, (merge, gain, bias)):
         target[...] = source[...]
     rows = normed[...]
     gated, lifted = dot(rows, gate_w[...]), dot(rows, up_w[...])
     hidden = (jax.nn.silu(gated) * lifted).astype(BF16)
     base[...] = RESIDUAL_SCALE * rows.astype(F32) + dot(hidden, down_w[...])
-
-
-def expert_kernel(rows, gate_own, up_own, left, right, gate_far, up_far, d0, d1, d2, d3a, d3b, out, pairs, down, sems):
-    depth, width = gate_own.shape
-    near = [(side.at[0:depth], side.at[depth : 2 * depth]) for side in (left, right)]
-    moves = []
-    for j, (gate_w, up_w) in enumerate([(gate_own, up_own), *near, (gate_far, up_far)]):
-        moves += [(gate_w, pairs.at[j, :, 0:width]), (up_w, pairs.at[j, :, width : 2 * width])]
+    for copy in copies:
+        copy.wait()
+
+
+def expert_kernel(rows, near, g2, u2, g3, u3, d0, d1, d2, d3a, d3b, out, far, down, sems):
+    moves = pair_moves(far, ((g2, u2), (g3, u3)))
     at = 0
     for piece in (d0, d1, d2, d3a, d3b):
         moves.append((piece, down.at[at : at + piece.shape[0]]))
         at += piece.shape[0]
     copies = fetched(moves, sems)
     picked = rows[...].reshape(-1, rows.shape[-1])
-    hidden = []
-    for j in range(pairs.shape[0]):
+
+    def hidden_of(both):
+        pair = dot(picked, both)
+        width = pair.shape[1] // 2
+        return (jax.nn.silu(pair[:, :width]) * pair[:, width:]).astype(BF16)
+
+    hidden = [hidden_of(near[j]) for j in range(near.shape[0])]
+    for j in range(far.shape[0]):
         copies[2 * j].wait()
         copies[2 * j + 1].wait()
-        pair = dot(picked, pairs[j])
-        hidden.append((jax.nn.silu(pair[:, :width]) * pair[:, width:]).astype(BF16))
-    for copy in copies[2 * pairs.shape[0] :]:
+        hidden.append(hidden_of(far[j]))
+    for copy in copies[2 * far.shape[0] :]:
         copy.wait()
     acc = dot(jnp.concatenate(hidden, axis=1), down[...])
     out[...] = acc.astype(BF16).reshape(out.shape)
@@ -293,8 +308,8 @@
     border = lax.ppermute(rows[rows.shape[0] - margin :], "sp", [(i, i + 1) for i in range(sp_count - 1)])
 
     gate_w, up_w, down_w = routed_gate_weight[0], routed_up_weight[0], routed_down_weight[0]
-    pair_w = jnp.concatenate([gate_w, up_w], axis=0)
-    pair_left, pair_right = turned(pair_w, 1), turned(pair_w, -1)
+    gate_left, up_right = turned(gate_w, 1), turned(up_w, -1)
+    up_left, gate_right = turned(up_w, 1), turned(gate_w, -1)
     down_left, down_right = turned(down_w, 1), turned(down_w, -1)
 
     runs = channels // LANES
@@ -316,39 +331,39 @@
     own_ids = lax.dynamic_slice_in_dim(routed_expert_index.T, own_index * quarter, quarter, 1)
     own_weights = lax.dynamic_slice_in_dim(routed_expert_weight.T, own_index * quarter, quarter, 1)
     fill = ((0, 0), (0, LANES - quarter))
-    select, merge, gated, *norm_parts = kernel_call(
+    select, merge, decays, states, *norm_parts, projection, ahead = kernel_call(
         side_kernel,
         [
             kept((slot_count, quarter), BF16),
             shape((quarter, slot_count), F32),
             kept((length, channels), F32),
-            kept((quarter, width), F32),
+            kept((length, channels), F32),
+            kept((quarter, width), BF16),
             kept((1, width), F32),
             kept((1, width), F32),
+            kept(recurrence_output_weight.shape, BF16),
+            kept((sp_count, LANES), F32),
         ],
+        (lax.axis_index("sp").reshape(1), "smem"),
         (jnp.pad(own_ids, fill, constant_values=-1), "vmem"),
         (jnp.pad(own_weights, fill), "vmem"),
+        (decays, "vmem"),
+        (states, "vmem"),
         flat(output_gate_input),
         stream,
         first_norm_gain.reshape(1, width),
         first_norm_bias.reshape(1, width),
-        scratch=(pltpu.VMEM(rows.shape, F32),),
+        (recurrence_output_weight, "hbm"),
+        scratch=(pltpu.VMEM(rows.shape, F32), pltpu.SemaphoreType.DMA((1,))),
     )
     parts = kernel_call(
         project_kernel,
         shape((tp_count, quarter, width), BF16),
-        (lax.axis_index("sp").reshape(1), "smem"),
-        (spans, "vmem"),
-        (decays, "vmem"),
-        (states, "vmem"),
-        (gated, "vmem"),
-        (recurrence_output_weight, "hbm"),
-        scratch=(pltpu.VMEM(recurrence_output_weight.shape, BF16), pltpu.SemaphoreType.DMA((1,))),
+        *((x, "vmem") for x in (spans, ahead, decays, states, projection)),
     )
     parts = swapped(parts, "tp")
 
-    depth = gate_w.shape[0]
-    gate_far, up_far = turned(pair_left[:depth], 1), turned(pair_right[depth:], -1)
+    gate_far, up_far = turned(gate_left, 1), turned(up_right, -1)
 
     normed, outgoing = kernel_call(
         mix_kernel,
@@ -363,25 +378,34 @@
     down_far = turned(down_left[:cut], 1), turned(down_right[cut:], -1)
 
     last = (merge, second_norm_gain.reshape(1, width), second_norm_bias.reshape(1, width))
-    base, *last = kernel_call(
+    near_weights = (gate_w, up_w, gate_left, up_left)
+    unit = gate_w.shape[1]
+    base, *last, near = kernel_call(
         shared_kernel,
-        [kept((quarter, width), F32), *(kept(x.shape, F32) for x in last)],
+        [
+            kept((quarter, width), F32),
+            *(kept(x.shape, F32) for x in last),
+            kept((len(near_weights) // 2, width, 2 * unit), BF16),
+        ],
         (normed, "vmem"),
         shared_gate_weight,
         shared_up_weight,
         shared_down_weight,
         *last,
-    )
-    weights = (gate_w, up_w, pair_left, pair_right, gate_far, up_far, down_w, down_left, down_right, *down_far)
+        *((w, "hbm") for w in near_weights),
+        scratch=(pltpu.SemaphoreType.DMA((len(near_weights),)),),
+    )
+    weights = (gate_right, up_right, gate_far, up_far, down_w, down_left, down_right, *down_far)
     leaving = kernel_call(
         expert_kernel,
         kept((expert_count, SLOTS, width), BF16),
         (arrived, "vmem"),
+        (near, "vmem"),
         *((w, "hbm") for w in weights),
         scratch=(
-            pltpu.VMEM((tp_count, width, 2 * gate_w.shape[1]), BF16),
-            pltpu.VMEM((tp_count * down_w.shape[0], width), BF16),
-            pltpu.SemaphoreType.DMA((len(weights) + 2,)),
+            pltpu.VMEM((2, width, 2 * unit), BF16),
+            pltpu.VMEM((tp_count * unit, width), BF16),
+            pltpu.SemaphoreType.DMA((len(weights),)),
         ),
     )
     returned = swapped(leaving, "sp")

time: 138 us -> 134 us (0.971)
  starting transfers between devices: 51.7 us -> 37.9 us
  blocking collectives: 21.6 us -> 28.9 us
  waiting for transfers between devices: 41 us -> 44.6 us
  other arithmetic: 2.23 us -> 0 us
    all_to_all x3, starting transfers between devices: 36 us -> 24.6 us  [swapped(): return lax.all_to_all(pieces, axis, 0, 0, tiled=True)]
    ppermute x8 -> x10, waiting for transfers between devices: 22.7 us -> 32.3 us  [turned(): lax.ppermute(shard, 'tp', [(i, (i + by) % count) for i in range(count)])]
    all_to_all x1, blocking collectives: 21.6 us -> 28.9 us  [swapped(): return lax.all_to_all(pieces, axis, 0, 0, tiled=True)]
    all_to_all x3, waiting for transfers between devices: 17.6 us -> 11.6 us  [swapped(): return lax.all_to_all(pieces, axis, 0, 0, tiled=True)]
    ppermute x8 -> x10, starting transfers between devices: 11.3 us -> 8.82 us  [turned(): lax.ppermute(shard, 'tp', [(i, (i + by) % count) for i in range(count)])]
    concatenate x1 -> x0, other arithmetic: 2.23 us -> none  [shards(): pair_w = jnp.concatenate([gate_w, up_w], axis=0)]
    unnamed x20 -> x22, local copies, waits for them, and re-layouts: 2.14 us -> 2.9 us
  transfers between devices with their start and end apart: 12 -> 14, of which waited for: 5 -> 8; matrix products, arithmetic and copies ran while one was open for 2% -> 1% of each run, Pallas kernels for 6% -> 6%
where the time goes in v4:
time: 134 us; the launch traced here: 133 us
  waiting for transfers between devices  44.6 us (33%)
  starting transfers between devices  37.9 us (28%)
  blocking collectives  28.9 us (22%)
  Pallas kernels  17.1 us (13%)
  local copies, waits for them, and re-layouts  4.49 us (3%)
    ppermute x10, waiting for transfers between devices, turned(): lax.ppermute(shard, 'tp', [(i, (i + by) % count) for i in range(count)])  32.3 us
    all_to_all x1, blocking collectives, swapped(): return lax.all_to_all(pieces, axis, 0, 0, tiled=True)  28.9 us
    all_to_all x3, starting transfers between devices, swapped(): return lax.all_to_all(pieces, axis, 0, 0, tiled=True)  24.6 us
    pallas_call x7, Pallas kernels, kernel_call(): pl.pallas_call(body, out_shape=out_shape, in_specs=specs, out_specs=[VMEM...  17.1 us
    all_to_all x3, waiting for transfers between devices, swapped(): return lax.all_to_all(pieces, axis, 0, 0, tiled=True)  11.6 us
    ppermute x10, starting transfers between devices, turned(): lax.ppermute(shard, 'tp', [(i, (i + by) % count) for i in range(count)])  8.82 us
    ppermute x1, starting transfers between devices, shards(): lax.ppermute(rows[rows.shape[0] - margin:], 'sp', [(i, i + 1) for i in ra...  4.49 us
    unnamed x22, local copies, waits for them, and re-layouts  2.9 us
  transfers between devices with their start and end apart: 14, of which 8 were waited for; matrix products, arithmetic and copies ran while one was open for 1% of the time, Pallas kernels for 6%

profile of v4, /device:TPU:1, one launch (start us, length us, event | category | flops | bytes accessed | tf_op | source)
XLA Modules:
  0.0 133.2 jit_solution(7397692045949561638)
XLA Ops:
  0.0 0.0 copy-start
  0.0 0.7 slice.16
  0.7 4.5 %collective-permute-start = (bf16[16,128]{1,0:T(8,128)(2,1)S(1)}, bf16[16,128]{1,0:T(8,128)(2,1)S(1)}, u32[]{:S(2)}, u32[]{:S(2)}) collective-permute-start(bf16[16,128]{1,0:T(8,128)(2,1)S(1)} %bitcast.45), channel_id=1, source_target_pairs={{0,4},{4,8},{8,12},{12,16},{16,20},{20,24},{24,28},{28,32},{32,36}... | collective-permute-start | bytes 12296 | tf_op jit(solution)/shard_map/ppermute | solution.py:308
  5.2 0.7 collective-permute-done.border
  5.9 3.0 %shard_map.199 = (f32[128,512]{1,0:T(8,128)S(1)}, f32[128,512]{1,0:T(8,128)S(1)}, bf16[64,8,128]{2,1,0:T(8,128)(2,1)}) custom-call(bf16[512,128]{1,0:T(8,128)(2,1)} %bitcast.39, bf16[16,128]{1,0:T(8,128)(2,1)S(1)} %collective-permute-done.border, bf16[4,2,256]{2,1,0:T(2,128)(2,1)} %taps.1, bf16[2,4,64,64]{3,2,1,0:T(8,128)(2,1)} %small_maps.1, ...), custom_call_target="tpu_custom_call" | custom-call | tf_op jit(solution)/shard_map/pallas_call | solution.py:27
  8.9 13.5 %all-to-all-start = ((bf16[64,8,128]{2,1,0:T(8,128)(2,1)}), bf16[64,8,128]{2,1,0:T(8,128)(2,1)S(1)}, u32[]{:S(2)}, u32[]{:S(2)}) async-start(bf16[64,8,128]{2,1,0:T(8,128)(2,1)} %get-tuple-element.24), calls=%async_computation | async-start | bytes 262144 | tf_op jit(solution)/shard_map/all_to_all | solution.py:271
  22.4 0.0 copy-done
  22.4 0.1 dynamic-slice_bitcast_fusion.1
  22.5 0.8 dynamic-slice_bitcast_fusion
  23.3 2.7 %shard_map.200 = (bf16[128,32]{1,0:T(8,128)(2,1)S(1)}, f32[32,128]{1,0:T(8,128)S(1)}, f32[128,512]{1,0:T(8,128)S(1)}, f32[128,512]{1,0:T(8,128)S(1)}, bf16[32,20...) custom-call(s32[1]{0:T(128)} %bitcast.8.mine, ...), custom_call_target="tpu_custom_call" | custom-call | tf_op jit(solution)/shard_map/pallas_call | solution.py:27
  26.0 0.0 copy-start.1
  26.0 0.6 copy-done.1
  26.6 6.9 %all-to-all-done.spans = bf16[64,8,128]{2,1,0:T(8,128)(2,1)S(1)} async-done(((bf16[64,8,128]{2,1,0:T(8,128)(2,1)}), bf16[64,8,128]{2,1,0:T(8,128)(2,1)S(1)}, u32[]{:S(2)}, u32[]{:S(2)}) %all-to-all-start) | async-done | bytes 131104 | tf_op jit(solution)/shard_map/all_to_all | solution.py:271
  33.5 0.0 copy-start.4
  33.5 1.4 %shard_map.201 = bf16[4,32,2048]{2,1,0:T(8,128)(2,1)} custom-call(bf16[64,8,128]{2,1,0:T(8,128)(2,1)S(1)} %all-to-all-done.spans, f32[64,128]{1,0:T(8,128)S(1)} %get-tuple-element.27.ahead, f32[128,512]{1,0:T(8,128)S(1)} %get-tuple-element.28.decays, f32[128,512]{1,0:T(8,128)S(1)} %get-tuple-element.29.states, bf16[2,256,2048]{2,1,0:T(8,128)(2,1)S(1)} %get-tuple-element.30.weight), custom_call_target="tpu_custom_call" | custom-call | tf_op jit(solution)/shard_map/pallas_call | solution.py:27
  34.9 0.0 copy-start.7
  34.9 4.3 %all-to-all-start.1 = ((bf16[4,32,2048]{2,1,0:T(8,128)(2,1)}), bf16[4,32,2048]{2,1,0:T(8,128)(2,1)S(1)}, u32[]{:S(2)}, u32[]{:S(2)}) async-start(bf16[4,32,2048]{2,1,0:T(8,128)(2,1)} %shard_map.201), calls=%async_computation.1 | async-start | bytes 1048576 | tf_op jit(solution)/shard_map/all_to_all | solution.py:271
  39.2 1.5 %collective-permute-start.1 = (bf16[2048,128]{1,0:T(8,128)(2,1)}, bf16[2048,128]{1,0:T(8,128)(2,1)}, u32[]{:S(2)}, u32[]{:S(2)}) collective-permute-start(bf16[2048,128]{1,0:T(8,128)(2,1)} %bitcast.34), channel_id=1, source_target_pairs={{0,1},{1,2},{2,3},{3,0},{4,5},{5,6},{6,7},{7,4},{8,9},{9,10},{10,1... | collective-permute-start | bytes 1572872 | tf_op jit(solution)/shard_map/ppermute | solution.py:267
  40.7 0.0 copy-done.4
  40.7 1.2 collective-permute-start.8
  41.9 1.4 %collective-permute-start.4 = (bf16[2048,128]{1,0:T(8,128)(2,1)}, bf16[2048,128]{1,0:T(8,128)(2,1)}, u32[]{:S(2)}, u32[]{:S(2)}) collective-permute-start(bf16[2048,128]{1,0:T(8,128)(2,1)} %bitcast.31), channel_id=1, source_target_pairs={{0,3},{1,0},{2,1},{3,2},{4,7},{5,4},{6,5},{7,6},{8,11},{9,8},{10,9... | collective-permute-start | bytes 1572872 | tf_op jit(solution)/shard_map/ppermute | solution.py:267
  43.4 4.7 %all-to-all-done.1.parts = bf16[4,32,2048]{2,1,0:T(8,128)(2,1)S(1)} async-done(((bf16[4,32,2048]{2,1,0:T(8,128)(2,1)}), bf16[4,32,2048]{2,1,0:T(8,128)(2,1)S(1)}, u32[]{:S(2)}, u32[]{:S(2)}) %all-to-all-start.1) | async-done | bytes 524320 | tf_op jit(solution)/shard_map/all_to_all | solution.py:271
  48.1 1.4 %shard_map.202 = (bf16[32,2048]{1,0:T(8,128)(2,1)S(1)}, bf16[64,2,2048]{2,1,0:T(2,128)(2,1)}) custom-call(bf16[4,32,2048]{2,1,0:T(8,128)(2,1)S(1)} %all-to-all-done.1.parts, bf16[32,2048]{1,0:T(8,128)(2,1)S(1)} %get-tuple-element.31.stream, f32[1,2048]{1,0:T(1,128)S(1)} %get-tuple-element.32.gain, f32[1,2048]{1,0:T(1,128)S(1)} %get-tuple-element.33.bias, ...), custom_call_target="tpu_custom_call" | custom-call | tf_op jit(solution)/shard_map/pallas_call | solution.py:27
  49.5 6.7 %all-to-all-start.2 = ((bf16[64,2,2048]{2,1,0:T(2,128)(2,1)}), bf16[64,2,2048]{2,1,0:T(2,128)(2,1)S(1)}, u32[]{:S(2)}, u32[]{:S(2)}) async-start(bf16[64,2,2048]{2,1,0:T(2,128)(2,1)} %get-tuple-element.35), calls=%async_computation.2 | async-start | bytes 1048576 | tf_op jit(solution)/shard_map/all_to_all | solution.py:271
  56.3 0.4 collective-permute-start.7
  56.6 0.0 copy-done.7
  56.6 0.1 collective-permute-start.2
  56.7 2.5 %collective-permute-done.1.g1 = bf16[2048,128]{1,0:T(8,128)(2,1)} collective-permute-done((bf16[2048,128]{1,0:T(8,128)(2,1)}, bf16[2048,128]{1,0:T(8,128)(2,1)}, u32[]{:S(2)}, u32[]{:S(2)}) %collective-permute-start.1) | collective-permute-done | bytes 524320 | tf_op jit(solution)/shard_map/ppermute | solution.py:267
  59.2 0.6 collective-permute-start.3
  59.8 0.0 collective-permute-done.8.d2
  59.8 0.0 copy-start.2
  59.8 0.9 collective-permute-start.5
  60.7 8.6 %collective-permute-done.4.u2 = bf16[2048,128]{1,0:T(8,128)(2,1)} collective-permute-done((bf16[2048,128]{1,0:T(8,128)(2,1)}, bf16[2048,128]{1,0:T(8,128)(2,1)}, u32[]{:S(2)}, u32[]{:S(2)}) %collective-permute-start.4) | collective-permute-done | bytes 524320 | tf_op jit(solution)/shard_map/ppermute | solution.py:267
  69.2 1.8 %collective-permute-start.6 = (bf16[2048,128]{1,0:T(8,128)(2,1)}, bf16[2048,128]{1,0:T(8,128)(2,1)}, u32[]{:S(2)}, u32[]{:S(2)}) collective-permute-start(bf16[2048,128]{1,0:T(8,128)(2,1)} %collective-permute-done.4.u2), channel_id=1, source_target_pairs={{0,3},{1,0},{2,1},{3,2},{4,7},{5,4},{6,5},{7,6},{8,11},{9,8},{10,9... | collective-permute-start | bytes 1572872 | tf_op jit(solution)/shard_map/ppermute | solution.py:267
  71.0 0.0 collective-permute-done.7.d1
  71.0 0.0 copy-start.3
  71.0 1.0 collective-permute-start.10
  72.0 9.7 %collective-permute-done.2.u1 = bf16[2048,128]{1,0:T(8,128)(2,1)S(1)} collective-permute-done((bf16[2048,128]{1,0:T(8,128)(2,1)S(1)}, bf16[2048,128]{1,0:T(8,128)(2,1)S(1)}, u32[]{:S(2)}, u32[]{:S(2)}) %collective-permute-start.2) | collective-permute-done | bytes 524320 | tf_op jit(solution)/shard_map/ppermute | solution.py:267
  81.7 0.0 copy-start.8
  81.7 0.0 collective-permute-start.9
  81.7 0.0 copy-done.2
  81.7 0.0 copy-done.3
  81.7 0.8 copy-done.8
  82.5 4.4 %shard_map.203 = (f32[32,2048]{1,0:T(8,128)S(1)}, f32[32,128]{1,0:T(8,128)S(1)}, f32[1,2048]{1,0:T(1,128)S(1)}, f32[1,2048]{1,0:T(1,128)S(1)}, bf16[2,2048,256]{2,1,0:T(8,128)(2,1)S(1)}) custom-call(bf16[32,2048]{1,0:T(8,128)(2,1)S(1)} %get-tuple-element.36.normed, bf16[2048,512]{1,0:T(8,128)(2,1)} %gate_w.1, bf16[2048,512]{1,0:T(8,128)(2,1)} %up_w.1, ...), custom_call_target="tpu_custom_call" | custom-call | tf_op jit(solution)/shard_map/pallas_call | solution.py:27
  87.0 0.0 collective-permute-done.3.g2
  87.0 0.0 copy-start.5
  87.0 10.2 %collective-permute-done.10.d3b = bf16[64,2048]{1,0:T(8,128)(2,1)S(1)} collective-permute-done((bf16[64,2048]{1,0:T(8,128)(2,1)S(1)}, bf16[64,2048]{1,0:T(8,128)(2,1)S(1)}, u32[]{:S(2)}, u32[]{:S(2)}) %collective-permute-start.10) | collective-permute-done | bytes 262176 | tf_op jit(solution)/shard_map/ppermute | solution.py:267
  97.2 0.0 copy-start.9
  97.2 1.3 %collective-permute-done.9.d3a = bf16[64,2048]{1,0:T(8,128)(2,1)S(1)} collective-permute-done((bf16[64,2048]{1,0:T(8,128)(2,1)S(1)}, bf16[64,2048]{1,0:T(8,128)(2,1)S(1)}, u32[]{:S(2)}, u32[]{:S(2)}) %collective-permute-start.9) | collective-permute-done | bytes 262176 | tf_op jit(solution)/shard_map/ppermute | solution.py:267
  98.5 0.0 copy-start.10
  98.5 0.0 collective-permute-done.5.g3
  98.5 0.0 copy-done.5
  98.6 0.7 copy-done.10
  99.2 0.0 copy-start.6
  99.2 0.8 copy-done.6
  100.0 0.0 collective-permute-done.6.u3
  100.0 0.0 all-to-all-done.2.rows
  100.1 0.0 copy-done.9
  100.1 3.0 %shard_map.204 = bf16[64,2,2048]{2,1,0:T(2,128)(2,1)S(1)} custom-call(bf16[64,2,2048]{2,1,0:T(2,128)(2,1)S(1)} %all-to-all-done.2.rows, bf16[2,2048,256]{2,1,0:T(8,128)(2,1)S(1)} %get-tuple-element.38.near, bf16[2048,128]{1,0:T(8,128)(2,1)} %copy-done.5, bf16[2048,128]{1,0:T(8,128)(2,1)} %collective-permute-done.4.u2, bf16[2048,128]{1,0:T(8,128)(2,1)} %copy-done.6, ...), custom_call_target="tpu_custom_call" | custom-call | tf_op jit(solution)/shard_map/pallas_call | solution.py:27
  103.0 28.9 %all_to_all.20.returned = bf16[64,2,2048]{2,1,0:T(2,128)(2,1)S(1)} all-to-all(bf16[64,2,2048]{2,1,0:T(2,128)(2,1)S(1)} %shard_map.204), channel_id=1, replica_groups=mesh['sp'=64,'tp'=4] {'sp'}, dimensions={0} | all-to-all | bytes 1048576 | tf_op jit(solution)/shard_map/all_to_all | solution.py:271
  132.0 1.2 shard_map.205
  (4 shorter events, 0.1 us)
Async XLA Ops:
  0.0 22.4 %copy-start = (s32[128,4]{0,1:T(4,128)S(1)}, s32[128,4]{0,1:T(4,128)}, u32[]{:S(2)}) copy-start(s32[128,4]{0,1:T(4,128)} %param.32) | copy-start | bytes 6148
  0.7 5.2 %collective-permute-start = (bf16[16,128]{1,0:T(8,128)(2,1)S(1)}, bf16[16,128]{1,0:T(8,128)(2,1)S(1)}, u32[]{:S(2)}, u32[]{:S(2)}) collective-permute-start(bf16[16,128]{1,0:T(8,128)(2,1)S(1)} %bitcast.45), channel_id=1, source_target_pairs={{0,4},{4,8},{8,12},{12,16},{16,20},{20,24},{24,28},{28,32},{32,36}... | collective-permute-start | bytes 12296 | tf_op jit(solution)/shard_map/ppermute | solution.py:308
  8.9 24.6 %all-to-all-start = ((bf16[64,8,128]{2,1,0:T(8,128)(2,1)}), bf16[64,8,128]{2,1,0:T(8,128)(2,1)S(1)}, u32[]{:S(2)}, u32[]{:S(2)}) async-start(bf16[64,8,128]{2,1,0:T(8,128)(2,1)} %get-tuple-element.24), calls=%async_computation | async-start | bytes 262144 | tf_op jit(solution)/shard_map/all_to_all | solution.py:271
  26.0 0.6 copy-start.1
  33.5 7.2 %copy-start.4 = (bf16[1,128,2048]{2,1,0:T(8,128)(2,1)S(1)}, bf16[1,128,2048]{2,1,0:T(8,128)(2,1)}, u32[]{:S(2)}) copy-start(bf16[1,128,2048]{2,1,0:T(8,128)(2,1)} %param.36) | copy-start | bytes 1572868
  34.9 21.7 %copy-start.7 = (bf16[1,2048,128]{2,1,0:T(8,128)(2,1)S(1)}, bf16[1,2048,128]{2,1,0:T(8,128)(2,1)}, u32[]{:S(2)}) copy-start(bf16[1,2048,128]{2,1,0:T(8,128)(2,1)} %param.35) | copy-start | bytes 1572868
  34.9 13.2 %all-to-all-start.1 = ((bf16[4,32,2048]{2,1,0:T(8,128)(2,1)}), bf16[4,32,2048]{2,1,0:T(8,128)(2,1)S(1)}, u32[]{:S(2)}, u32[]{:S(2)}) async-start(bf16[4,32,2048]{2,1,0:T(8,128)(2,1)} %shard_map.201), calls=%async_computation.1 | async-start | bytes 1048576 | tf_op jit(solution)/shard_map/all_to_all | solution.py:271
  39.2 19.9 %collective-permute-start.1 = (bf16[2048,128]{1,0:T(8,128)(2,1)}, bf16[2048,128]{1,0:T(8,128)(2,1)}, u32[]{:S(2)}, u32[]{:S(2)}) collective-permute-start(bf16[2048,128]{1,0:T(8,128)(2,1)} %bitcast.34), channel_id=1, source_target_pairs={{0,1},{1,2},{2,3},{3,0},{4,5},{5,6},{6,7},{7,4},{8,9},{9,10},{10,1... | collective-permute-start | bytes 1572872 | tf_op jit(solution)/shard_map/ppermute | solution.py:267
  40.7 19.1 %collective-permute-start.8 = (bf16[128,2048]{1,0:T(8,128)(2,1)S(1)}, bf16[128,2048]{1,0:T(8,128)(2,1)S(1)}, u32[]{:S(2)}, u32[]{:S(2)}) collective-permute-start(bf16[128,2048]{1,0:T(8,128)(2,1)S(1)} %bitcast.29), channel_id=1, source_target_pairs={{0,3},{1,0},{2,1},{3,2},{4,7},{5,4},{6,5},{7,6},{8,11},{9,8},{10,9... | collective-permute-start | bytes 1572872 | tf_op jit(solution)/shard_map/ppermute | solution.py:267
  41.9 27.3 %collective-permute-start.4 = (bf16[2048,128]{1,0:T(8,128)(2,1)}, bf16[2048,128]{1,0:T(8,128)(2,1)}, u32[]{:S(2)}, u32[]{:S(2)}) collective-permute-start(bf16[2048,128]{1,0:T(8,128)(2,1)} %bitcast.31), channel_id=1, source_target_pairs={{0,3},{1,0},{2,1},{3,2},{4,7},{5,4},{6,5},{7,6},{8,11},{9,8},{10,9... | collective-permute-start | bytes 1572872 | tf_op jit(solution)/shard_map/ppermute | solution.py:267
  49.5 50.6 %all-to-all-start.2 = ((bf16[64,2,2048]{2,1,0:T(2,128)(2,1)}), bf16[64,2,2048]{2,1,0:T(2,128)(2,1)S(1)}, u32[]{:S(2)}, u32[]{:S(2)}) async-start(bf16[64,2,2048]{2,1,0:T(2,128)(2,1)} %get-tuple-element.35), calls=%async_computation.2 | async-start | bytes 1048576 | tf_op jit(solution)/shard_map/all_to_all | solution.py:271
  56.3 14.8 %collective-permute-start.7 = (bf16[128,2048]{1,0:T(8,128)(2,1)S(1)}, bf16[128,2048]{1,0:T(8,128)(2,1)S(1)}, u32[]{:S(2)}, u32[]{:S(2)}) collective-permute-start(bf16[128,2048]{1,0:T(8,128)(2,1)S(1)} %bitcast.30), channel_id=1, source_target_pairs={{0,1},{1,2},{2,3},{3,0},{4,5},{5,6},{6,7},{7,4},{8,9},{9,10},{10,1... | collective-permute-start | bytes 1572872 | tf_op jit(solution)/shard_map/ppermute | solution.py:267
  56.6 25.1 %collective-permute-start.2 = (bf16[2048,128]{1,0:T(8,128)(2,1)S(1)}, bf16[2048,128]{1,0:T(8,128)(2,1)S(1)}, u32[]{:S(2)}, u32[]{:S(2)}) collective-permute-start(bf16[2048,128]{1,0:T(8,128)(2,1)S(1)} %bitcast.33), channel_id=1, source_target_pairs={{0,1},{1,2},{2,3},{3,0},{4,5},{5,6},{6,7},{7,4},{8,9},{9,10},{10,1... | collective-permute-start | bytes 1572872 | tf_op jit(solution)/shard_map/ppermute | solution.py:267
  59.2 27.8 %collective-permute-start.3 = (bf16[2048,128]{1,0:T(8,128)(2,1)}, bf16[2048,128]{1,0:T(8,128)(2,1)S(1)}, u32[]{:S(2)}, u32[]{:S(2)}) collective-permute-start(bf16[2048,128]{1,0:T(8,128)(2,1)} %bitcast.35), channel_id=1, source_target_pairs={{0,3},{1,0},{2,1},{3,2},{4,7},{5,4},{6,5},{7,6},{8,11},{9,8},{10,9... | collective-permute-start | bytes 1572872 | tf_op jit(solution)/shard_map/ppermute | solution.py:267
  59.8 21.9 %copy-start.2 = (bf16[128,2048]{1,0:T(8,128)(2,1)}, bf16[128,2048]{1,0:T(8,128)(2,1)S(1)}, u32[]{:S(2)}) copy-start(bf16[128,2048]{1,0:T(8,128)(2,1)S(1)} %collective-permute-done.8.d2) | copy-start | bytes 1572868
  59.8 38.8 %collective-permute-start.5 = (bf16[2048,128]{1,0:T(8,128)(2,1)}, bf16[2048,128]{1,0:T(8,128)(2,1)S(1)}, u32[]{:S(2)}, u32[]{:S(2)}) collective-permute-start(bf16[2048,128]{1,0:T(8,128)(2,1)} %collective-permute-done.1.g1), channel_id=1, source_target_pairs={{0,1},{1,2},{2,3},{3,0},{4,5},{5,6},{6,7},{7,4},{8,9},{9,10},{10,1... | collective-permute-start | bytes 1572872 | tf_op jit(solution)/shard_map/ppermute | solution.py:267
  69.2 30.8 %collective-permute-start.6 = (bf16[2048,128]{1,0:T(8,128)(2,1)}, bf16[2048,128]{1,0:T(8,128)(2,1)}, u32[]{:S(2)}, u32[]{:S(2)}) collective-permute-start(bf16[2048,128]{1,0:T(8,128)(2,1)} %collective-permute-done.4.u2), channel_id=1, source_target_pairs={{0,3},{1,0},{2,1},{3,2},{4,7},{5,4},{6,5},{7,6},{8,11},{9,8},{10,9... | collective-permute-start | bytes 1572872 | tf_op jit(solution)/shard_map/ppermute | solution.py:267
  71.0 10.7 %copy-start.3 = (bf16[128,2048]{1,0:T(8,128)(2,1)}, bf16[128,2048]{1,0:T(8,128)(2,1)S(1)}, u32[]{:S(2)}) copy-start(bf16[128,2048]{1,0:T(8,128)(2,1)S(1)} %collective-permute-done.7.d1) | copy-start | bytes 1572868
  71.0 26.2 %collective-permute-start.10 = (bf16[64,2048]{1,0:T(8,128)(2,1)S(1)}, bf16[64,2048]{1,0:T(8,128)(2,1)S(1)}, u32[]{:S(2)}, u32[]{:S(2)}) collective-permute-start(bf16[64,2048]{1,0:T(8,128)(2,1)S(1)} %slice.18), channel_id=1, source_target_pairs={{0,3},{1,0},{2,1},{3,2},{4,7},{5,4},{6,5},{7,6},{8,11},{9,8},{10,9... | collective-permute-start | bytes 786440 | tf_op jit(solution)/shard_map/ppermute | solution.py:267
  81.7 0.8 copy-start.8
  81.7 16.9 %collective-permute-start.9 = (bf16[64,2048]{1,0:T(8,128)(2,1)S(1)}, bf16[64,2048]{1,0:T(8,128)(2,1)S(1)}, u32[]{:S(2)}, u32[]{:S(2)}) collective-permute-start(bf16[64,2048]{1,0:T(8,128)(2,1)S(1)} %slice.17), channel_id=1, source_target_pairs={{0,1},{1,2},{2,3},{3,0},{4,5},{5,6},{6,7},{7,4},{8,9},{9,10},{10,1... | collective-permute-start | bytes 786440 | tf_op jit(solution)/shard_map/ppermute | solution.py:267
  87.0 11.6 %copy-start.5 = (bf16[2048,128]{1,0:T(8,128)(2,1)}, bf16[2048,128]{1,0:T(8,128)(2,1)S(1)}, u32[]{:S(2)}) copy-start(bf16[2048,128]{1,0:T(8,128)(2,1)S(1)} %collective-permute-done.3.g2) | copy-start | bytes 1572868
  97.2 2.9 %copy-start.9 = (bf16[64,2048]{1,0:T(8,128)(2,1)}, bf16[64,2048]{1,0:T(8,128)(2,1)S(1)}, u32[]{:S(2)}) copy-start(bf16[64,2048]{1,0:T(8,128)(2,1)S(1)} %collective-permute-done.10.d3b) | copy-start | bytes 786436
  98.5 0.7 copy-start.10
  99.2 0.8 copy-start.6

commit v5 on v4

--- a/solution.py
+++ b/solution.py
@@ -160,11 +160,11 @@
     out[...] = acc.astype(BF16).reshape(out.shape)
 
 
-def side_kernel(mine, ids, weights, decays, states, gate_rows, stream, gain, bias, projection, *rest):
+def side_kernel(mine, part, ids, weights, decays, states, gate_rows, stream, gain, bias, projection, *rest):
     select, merge, gated_decays, gated_states, stream_kept, gain_kept, bias_kept, projection_kept, ahead, wide, sems = rest
     (copy,) = fetched([(projection, projection_kept)], sems)
     ahead[...] = jnp.where(lax.broadcasted_iota(jnp.int32, ahead.shape, 0) < mine[0], 1.0, 0.0)
-    route(ids, weights, select, merge)
+    route(ids, weights, select, merge, part[0])
     wide[...] = gate_rows[...].astype(F32)
     length, runs = decays.shape[0], decays.shape[1] // LANES
     groups = 2
@@ -180,8 +180,13 @@
     copy.wait()
 
 
-def route(ids, weights, select, merge):
+def route(ids, weights, select, merge, part):
     slot_count, rows = select.shape[0], ids.shape[1]
+    kept_rows = select.shape[1]
+    turn = (rows - part * kept_rows) % rows
+    own = lax.broadcasted_iota(jnp.int32, ids.shape, 1) < kept_rows
+    ids = jnp.where(own, pltpu.roll(ids[...], turn, 1), -1)
+    weights = pltpu.roll(weights[...], turn, 1)
     slot = lax.broadcasted_iota(jnp.int32, (slot_count, rows), 0)
     names = jnp.zeros((slot_count, rows), F32)
     weight = jnp.zeros((slot_count, rows), F32)
@@ -226,29 +231,31 @@
         copy.wait()
 
 
-def expert_kernel(rows, near, g2, u2, g3, u3, d0, d1, d2, d3a, d3b, out, far, down, sems):
+def expert_kernel(rows, near, g2, u2, g3, u3, d0, d1, d2, acc, last, far, down, sems):
     moves = pair_moves(far, ((g2, u2), (g3, u3)))
-    at = 0
-    for piece in (d0, d1, d2, d3a, d3b):
-        moves.append((piece, down.at[at : at + piece.shape[0]]))
-        at += piece.shape[0]
+    unit = d0.shape[0]
+    moves += [(piece, down.at[j * unit : (j + 1) * unit]) for j, piece in enumerate((d0, d1, d2))]
     copies = fetched(moves, sems)
     picked = rows[...].reshape(-1, rows.shape[-1])
 
     def hidden_of(both):
         pair = dot(picked, both)
-        width = pair.shape[1] // 2
-        return (jax.nn.silu(pair[:, :width]) * pair[:, width:]).astype(BF16)
+        return (jax.nn.silu(pair[:, :unit]) * pair[:, unit:]).astype(BF16)
 
     hidden = [hidden_of(near[j]) for j in range(near.shape[0])]
     for j in range(far.shape[0]):
         copies[2 * j].wait()
         copies[2 * j + 1].wait()
         hidden.append(hidden_of(far[j]))
+    last[...] = hidden.pop()
     for copy in copies[2 * far.shape[0] :]:
         copy.wait()
-    acc = dot(jnp.concatenate(hidden, axis=1), down[...])
-    out[...] = acc.astype(BF16).reshape(out.shape)
+    acc[...] = dot(jnp.concatenate(hidden, axis=1), down[...])
+
+
+def last_kernel(acc, hidden, d3a, d3b, out):
+    total = acc[...] + dot(hidden[...], jnp.concatenate([d3a[...], d3b[...]], axis=0))
+    out[...] = total.astype(BF16).reshape(out.shape)
 
 
 def merge_kernel(returned, base, merge, gain, bias, out):
@@ -327,15 +334,11 @@
     )
     spans = swapped(totals, "sp")
 
-    own_index = lax.axis_index("tp")
-    own_ids = lax.dynamic_slice_in_dim(routed_expert_index.T, own_index * quarter, quarter, 1)
-    own_weights = lax.dynamic_slice_in_dim(routed_expert_weight.T, own_index * quarter, quarter, 1)
-    fill = ((0, 0), (0, LANES - quarter))
     select, merge, decays, states, *norm_parts, projection, ahead = kernel_call(
         side_kernel,
         [
             kept((slot_count, quarter), BF16),
-            shape((quarter, slot_count), F32),
+            kept((quarter, slot_count), F32),
             kept((length, channels), F32),
             kept((length, channels), F32),
             kept((quarter, width), BF16),
@@ -345,8 +348,9 @@
             kept((sp_count, LANES), F32),
         ],
         (lax.axis_index("sp").reshape(1), "smem"),
-        (jnp.pad(own_ids, fill, constant_values=-1), "vmem"),
-        (jnp.pad(own_weights, fill), "vmem"),
+        (lax.axis_index("tp").reshape(1), "smem"),
+        routed_expert_index.T,
+        routed_expert_weight.T,
         (decays, "vmem"),
         (states, "vmem"),
         flat(output_gate_input),
@@ -391,22 +395,26 @@
         shared_gate_weight,
         shared_up_weight,
         shared_down_weight,
-        *last,
+        (last[0], "vmem"),
+        *last[1:],
         *((w, "hbm") for w in near_weights),
         scratch=(pltpu.SemaphoreType.DMA((len(near_weights),)),),
     )
-    weights = (gate_right, up_right, gate_far, up_far, down_w, down_left, down_right, *down_far)
-    leaving = kernel_call(
+    weights = (gate_right, up_right, gate_far, up_far, down_w, down_left, down_right)
+    acc, hidden = kernel_call(
         expert_kernel,
-        kept((expert_count, SLOTS, width), BF16),
+        [kept((slot_count, width), F32), kept((slot_count, unit), BF16)],
         (arrived, "vmem"),
         (near, "vmem"),
         *((w, "hbm") for w in weights),
         scratch=(
             pltpu.VMEM((2, width, 2 * unit), BF16),
-            pltpu.VMEM((tp_count * unit, width), BF16),
+            pltpu.VMEM((3 * unit, width), BF16),
             pltpu.SemaphoreType.DMA((len(weights),)),
         ),
+    )
+    leaving = kernel_call(
+        last_kernel, kept((expert_count, SLOTS, width), BF16), (acc, "vmem"), (hidden, "vmem"), *down_far
     )
     returned = swapped(leaving, "sp")
     return kernel_call(

time: 134 us -> 131 us (0.978)
  waiting for transfers between devices: 44.6 us -> 42 us
  local copies, waits for them, and re-layouts: 4.49 us -> 3.02 us
    ppermute x10, waiting for transfers between devices: 32.3 us -> 28.2 us  [turned(): lax.ppermute(shard, 'tp', [(i, (i + by) % count) for i in range(count)])]
    all_to_all x3, waiting for transfers between devices: 11.6 us -> 13.1 us  [swapped(): return lax.all_to_all(pieces, axis, 0, 0, tiled=True)]
    unnamed x22 -> x10, local copies, waits for them, and re-layouts: 2.9 us -> 1.6 us
    pallas_call x7 -> x8, Pallas kernels: 17.1 us -> 18.3 us  [kernel_call(): pl.pallas_call(body, out_shape=out_shape, in_specs=specs, out_specs=[VMEM...]
  transfers between devices with their start and end apart: 14 -> 14, of which waited for: 8 -> 9; matrix products, arithmetic and copies ran while one was open for 1% -> 1% of each run, Pallas kernels for 6% -> 9%
where the time goes in v5:
time: 131 us; the launch traced here: 130 us
  waiting for transfers between devices  42 us (32%)
  starting transfers between devices  37.7 us (29%)
  blocking collectives  28.9 us (22%)
  Pallas kernels  18.3 us (14%)
  local copies, waits for them, and re-layouts  3.02 us (2%)
    all_to_all x1, blocking collectives, swapped(): return lax.all_to_all(pieces, axis, 0, 0, tiled=True)  28.9 us
    ppermute x10, waiting for transfers between devices, turned(): lax.ppermute(shard, 'tp', [(i, (i + by) % count) for i in range(count)])  28.2 us
    all_to_all x3, starting transfers between devices, swapped(): return lax.all_to_all(pieces, axis, 0, 0, tiled=True)  24.4 us
    pallas_call x8, Pallas kernels, kernel_call(): pl.pallas_call(body, out_shape=out_shape, in_specs=specs, out_specs=[VMEM...  18.3 us
    all_to_all x3, waiting for transfers between devices, swapped(): return lax.all_to_all(pieces, axis, 0, 0, tiled=True)  13.1 us
    ppermute x10, starting transfers between devices, turned(): lax.ppermute(shard, 'tp', [(i, (i + by) % count) for i in range(count)])  8.82 us
    ppermute x1, starting transfers between devices, shards(): lax.ppermute(rows[rows.shape[0] - margin:], 'sp', [(i, i + 1) for i in ra...  4.49 us
  transfers between devices with their start and end apart: 14, of which 9 were waited for; matrix products, arithmetic and copies ran while one was open for 1% of the time, Pallas kernels for 9%

profile of v5, /device:TPU:1, one launch (start us, length us, event | category | flops | bytes accessed | tf_op | source)
XLA Modules:
  0.0 130.2 jit_solution(6406902574600655815)
XLA Ops:
  0.0 0.7 slice.16
  0.7 4.5 %collective-permute-start = (bf16[16,128]{1,0:T(8,128)(2,1)S(1)}, bf16[16,128]{1,0:T(8,128)(2,1)S(1)}, u32[]{:S(2)}, u32[]{:S(2)}) collective-permute-start(bf16[16,128]{1,0:T(8,128)(2,1)S(1)} %bitcast.35), channel_id=1, source_target_pairs={{0,4},{4,8},{8,12},{12,16},{16,20},{20,24},{24,28},{28,32},{32,36}... | collective-permute-start | bytes 12296 | tf_op jit(solution)/shard_map/ppermute | solution.py:315
  5.2 0.7 collective-permute-done.border
  5.9 3.0 %shard_map.199 = (f32[128,512]{1,0:T(8,128)S(1)}, f32[128,512]{1,0:T(8,128)S(1)}, bf16[64,8,128]{2,1,0:T(8,128)(2,1)}) custom-call(bf16[512,128]{1,0:T(8,128)(2,1)} %bitcast.29, bf16[16,128]{1,0:T(8,128)(2,1)S(1)} %collective-permute-done.border, bf16[4,2,256]{2,1,0:T(2,128)(2,1)} %taps.1, bf16[2,4,64,64]{3,2,1,0:T(8,128)(2,1)} %small_maps.1, ...), custom_call_target="tpu_custom_call" | custom-call | tf_op jit(solution)/shard_map/pallas_call | solution.py:27
  8.9 13.5 %all-to-all-start = ((bf16[64,8,128]{2,1,0:T(8,128)(2,1)}), bf16[64,8,128]{2,1,0:T(8,128)(2,1)S(1)}, u32[]{:S(2)}, u32[]{:S(2)}) async-start(bf16[64,8,128]{2,1,0:T(8,128)(2,1)} %get-tuple-element.26), calls=%async_computation | async-start | bytes 262144 | tf_op jit(solution)/shard_map/all_to_all | solution.py:278
  22.4 2.8 %shard_map.200 = (bf16[128,32]{1,0:T(8,128)(2,1)S(1)}, f32[32,128]{1,0:T(8,128)S(1)}, f32[128,512]{1,0:T(8,128)S(1)}, f32[128,512]{1,0:T(8,128)S(1)}, bf16[32,20...) custom-call(s32[1]{0:T(128)} %bitcast.8.mine, ...), custom_call_target="tpu_custom_call" | custom-call | tf_op jit(solution)/shard_map/pallas_call | solution.py:27
  25.2 8.3 %all-to-all-done.spans = bf16[64,8,128]{2,1,0:T(8,128)(2,1)S(1)} async-done(((bf16[64,8,128]{2,1,0:T(8,128)(2,1)}), bf16[64,8,128]{2,1,0:T(8,128)(2,1)S(1)}, u32[]{:S(2)}, u32[]{:S(2)}) %all-to-all-start) | async-done | bytes 131104 | tf_op jit(solution)/shard_map/all_to_all | solution.py:278
  33.5 1.4 %shard_map.201 = bf16[4,32,2048]{2,1,0:T(8,128)(2,1)} custom-call(bf16[64,8,128]{2,1,0:T(8,128)(2,1)S(1)} %all-to-all-done.spans, f32[64,128]{1,0:T(8,128)S(1)} %get-tuple-element.29.ahead, f32[128,512]{1,0:T(8,128)S(1)} %get-tuple-element.30.decays, f32[128,512]{1,0:T(8,128)S(1)} %get-tuple-element.31.states, bf16[2,256,2048]{2,1,0:T(8,128)(2,1)S(1)} %get-tuple-element.32.weight), custom_call_target="tpu_custom_call" | custom-call | tf_op jit(solution)/shard_map/pallas_call | solution.py:27
  34.9 4.2 %all-to-all-start.1 = ((bf16[4,32,2048]{2,1,0:T(8,128)(2,1)}), bf16[4,32,2048]{2,1,0:T(8,128)(2,1)S(1)}, u32[]{:S(2)}, u32[]{:S(2)}) async-start(bf16[4,32,2048]{2,1,0:T(8,128)(2,1)} %shard_map.201), calls=%async_computation.1 | async-start | bytes 1048576 | tf_op jit(solution)/shard_map/all_to_all | solution.py:278
  39.1 1.5 %collective-permute-start.1 = (bf16[2048,128]{1,0:T(8,128)(2,1)}, bf16[2048,128]{1,0:T(8,128)(2,1)}, u32[]{:S(2)}, u32[]{:S(2)}) collective-permute-start(bf16[2048,128]{1,0:T(8,128)(2,1)} %bitcast.19.g0), channel_id=1, source_target_pairs={{0,1},{1,2},{2,3},{3,0},{4,5},{5,6},{6,7},{7,4},{8,9},{9,10},{10,1... | collective-permute-start | bytes 1572872 | tf_op jit(solution)/shard_map/ppermute | solution.py:274
  40.6 1.2 collective-permute-start.4
  41.8 1.4 %collective-permute-start.8 = (bf16[128,2048]{1,0:T(8,128)(2,1)}, bf16[128,2048]{1,0:T(8,128)(2,1)S(1)}, u32[]{:S(2)}, u32[]{:S(2)}) collective-permute-start(bf16[128,2048]{1,0:T(8,128)(2,1)} %bitcast.21.d0), channel_id=1, source_target_pairs={{0,3},{1,0},{2,1},{3,2},{4,7},{5,4},{6,5},{7,6},{8,11},{9,8},{10,9... | collective-permute-start | bytes 1572872 | tf_op jit(solution)/shard_map/ppermute | solution.py:274
  43.3 4.8 %all-to-all-done.1.parts = bf16[4,32,2048]{2,1,0:T(8,128)(2,1)S(1)} async-done(((bf16[4,32,2048]{2,1,0:T(8,128)(2,1)}), bf16[4,32,2048]{2,1,0:T(8,128)(2,1)S(1)}, u32[]{:S(2)}, u32[]{:S(2)}) %all-to-all-start.1) | async-done | bytes 524320 | tf_op jit(solution)/shard_map/all_to_all | solution.py:278
  48.0 1.4 %shard_map.202 = (bf16[32,2048]{1,0:T(8,128)(2,1)S(1)}, bf16[64,2,2048]{2,1,0:T(2,128)(2,1)}) custom-call(bf16[4,32,2048]{2,1,0:T(8,128)(2,1)S(1)} %all-to-all-done.1.parts, bf16[32,2048]{1,0:T(8,128)(2,1)S(1)} %get-tuple-element.33.stream, f32[1,2048]{1,0:T(1,128)S(1)} %get-tuple-element.34.gain, f32[1,2048]{1,0:T(1,128)S(1)} %get-tuple-element.35.bias, ...), custom_call_target="tpu_custom_call" | custom-call | tf_op jit(solution)/shard_map/pallas_call | solution.py:27
  49.4 6.7 %all-to-all-start.2 = ((bf16[64,2,2048]{2,1,0:T(2,128)(2,1)}), bf16[64,2,2048]{2,1,0:T(2,128)(2,1)S(1)}, u32[]{:S(2)}, u32[]{:S(2)}) async-start(bf16[64,2,2048]{2,1,0:T(2,128)(2,1)} %get-tuple-element.37), calls=%async_computation.2 | async-start | bytes 1048576 | tf_op jit(solution)/shard_map/all_to_all | solution.py:278
  56.1 0.4 collective-permute-start.7
  56.5 0.1 collective-permute-start.2
  56.6 2.5 %collective-permute-done.1.g1 = bf16[2048,128]{1,0:T(8,128)(2,1)} collective-permute-done((bf16[2048,128]{1,0:T(8,128)(2,1)}, bf16[2048,128]{1,0:T(8,128)(2,1)}, u32[]{:S(2)}, u32[]{:S(2)}) %collective-permute-start.1) | collective-permute-done | bytes 524320 | tf_op jit(solution)/shard_map/ppermute | solution.py:274
  59.1 0.6 collective-permute-start.3
  59.6 0.0 collective-permute-done.4.u2
  59.6 0.9 collective-permute-start.5
  60.5 8.4 %collective-permute-done.8.d2 = bf16[128,2048]{1,0:T(8,128)(2,1)S(1)} collective-permute-done((bf16[128,2048]{1,0:T(8,128)(2,1)}, bf16[128,2048]{1,0:T(8,128)(2,1)S(1)}, u32[]{:S(2)}, u32[]{:S(2)}) %collective-permute-start.8) | collective-permute-done | bytes 524320 | tf_op jit(solution)/shard_map/ppermute | solution.py:274
  69.0 0.0 copy-start
  69.0 1.7 %collective-permute-start.6 = (bf16[2048,128]{1,0:T(8,128)(2,1)}, bf16[2048,128]{1,0:T(8,128)(2,1)}, u32[]{:S(2)}, u32[]{:S(2)}) collective-permute-start(bf16[2048,128]{1,0:T(8,128)(2,1)} %collective-permute-done.4.u2), channel_id=1, source_target_pairs={{0,3},{1,0},{2,1},{3,2},{4,7},{5,4},{6,5},{7,6},{8,11},{9,8},{10,9... | collective-permute-start | bytes 1572872 | tf_op jit(solution)/shard_map/ppermute | solution.py:274
  70.7 0.0 collective-permute-done.7.d1
  70.7 0.0 copy-start.1
  70.7 1.1 collective-permute-start.10
  71.8 0.7 slice.17
  72.5 9.3 %collective-permute-done.2.u1 = bf16[2048,128]{1,0:T(8,128)(2,1)S(1)} collective-permute-done((bf16[2048,128]{1,0:T(8,128)(2,1)}, bf16[2048,128]{1,0:T(8,128)(2,1)S(1)}, u32[]{:S(2)}, u32[]{:S(2)}) %collective-permute-start.2) | collective-permute-done | bytes 524320 | tf_op jit(solution)/shard_map/ppermute | solution.py:274
  81.8 0.0 copy-start.4
  81.8 0.0 collective-permute-start.9
  81.8 0.0 copy-done
  81.8 0.0 copy-done.1
  81.8 0.8 copy-done.4
  82.6 4.4 %shard_map.203 = (f32[32,2048]{1,0:T(8,128)S(1)}, f32[32,128]{1,0:T(8,128)S(1)}, f32[1,2048]{1,0:T(1,128)S(1)}, f32[1,2048]{1,0:T(1,128)S(1)}, bf16[2,2048,256]{2,1,0:T(8,128)(2,1)S(1)}) custom-call(bf16[32,2048]{1,0:T(8,128)(2,1)S(1)} %get-tuple-element.38.normed, bf16[2048,512]{1,0:T(8,128)(2,1)} %gate_w.1, bf16[2048,512]{1,0:T(8,128)(2,1)} %up_w.1, ...), custom_call_target="tpu_custom_call" | custom-call | tf_op jit(solution)/shard_map/pallas_call | solution.py:27
  87.0 0.0 collective-permute-done.3.g2
  87.0 0.0 copy-start.2
  87.0 6.0 %collective-permute-done.5.g3 = bf16[2048,128]{1,0:T(8,128)(2,1)S(1)} collective-permute-done((bf16[2048,128]{1,0:T(8,128)(2,1)}, bf16[2048,128]{1,0:T(8,128)(2,1)S(1)}, u32[]{:S(2)}, u32[]{:S(2)}) %collective-permute-start.5) | collective-permute-done | bytes 524320 | tf_op jit(solution)/shard_map/ppermute | solution.py:274
  93.0 0.0 copy-done.2
  93.0 0.0 copy-start.3
  93.0 0.8 copy-done.3
  93.8 0.0 collective-permute-done.6.u3
  93.8 0.0 all-to-all-done.2.rows
  93.8 2.9 %shard_map.204 = (f32[128,2048]{1,0:T(8,128)S(1)}, bf16[128,128]{1,0:T(8,128)(2,1)S(1)}) custom-call(bf16[64,2,2048]{2,1,0:T(2,128)(2,1)S(1)} %all-to-all-done.2.rows, bf16[2,2048,256]{2,1,0:T(8,128)(2,1)S(1)} %get-tuple-element.40.near, bf16[2048,128]{1,0:T(8,128)(2,1)} %copy-done.2, bf16[2048,128]{1,0:T(8,128)(2,1)} %collective-permute-done.4.u2, ...), custom_call_target="tpu_custom_call" | custom-call | tf_op jit(solution)/shard_map/pallas_call | solution.py:27
  96.7 0.5 collective-permute-done.10.d3b
  97.2 1.5 %collective-permute-done.9.d3a = bf16[64,2048]{1,0:T(8,128)(2,1)} collective-permute-done((bf16[64,2048]{1,0:T(8,128)(2,1)}, bf16[64,2048]{1,0:T(8,128)(2,1)}, u32[]{:S(2)}, u32[]{:S(2)}) %collective-permute-start.9) | collective-permute-done | bytes 262176 | tf_op jit(solution)/shard_map/ppermute | solution.py:274
  98.7 1.3 %shard_map.205 = bf16[64,2,2048]{2,1,0:T(2,128)(2,1)S(1)} custom-call(f32[128,2048]{1,0:T(8,128)S(1)} %get-tuple-element.41.acc, bf16[128,128]{1,0:T(8,128)(2,1)S(1)} %get-tuple-element.42.hidden, bf16[64,2048]{1,0:T(8,128)(2,1)} %collective-permute-done.9.d3a, bf16[64,2048]{1,0:T(8,128)(2,1)} %collective-permute-done.10.d3b), custom_call_target="tpu_custom_call" | custom-call | tf_op jit(solution)/shard_map/pallas_call | solution.py:27
  100.0 28.9 %all_to_all.20.returned = bf16[64,2,2048]{2,1,0:T(2,128)(2,1)S(1)} all-to-all(bf16[64,2,2048]{2,1,0:T(2,128)(2,1)S(1)} %shard_map.205), channel_id=1, replica_groups=mesh['sp'=64,'tp'=4] {'sp'}, dimensions={0} | all-to-all | bytes 1048576 | tf_op jit(solution)/shard_map/all_to_all | solution.py:278
  129.0 1.2 shard_map.206
  (1 shorter events, 0.0 us)
Async XLA Ops:
  0.7 5.2 %collective-permute-start = (bf16[16,128]{1,0:T(8,128)(2,1)S(1)}, bf16[16,128]{1,0:T(8,128)(2,1)S(1)}, u32[]{:S(2)}, u32[]{:S(2)}) collective-permute-start(bf16[16,128]{1,0:T(8,128)(2,1)S(1)} %bitcast.35), channel_id=1, source_target_pairs={{0,4},{4,8},{8,12},{12,16},{16,20},{20,24},{24,28},{28,32},{32,36}... | collective-permute-start | bytes 12296 | tf_op jit(solution)/shard_map/ppermute | solution.py:315
  8.9 24.6 %all-to-all-start = ((bf16[64,8,128]{2,1,0:T(8,128)(2,1)}), bf16[64,8,128]{2,1,0:T(8,128)(2,1)S(1)}, u32[]{:S(2)}, u32[]{:S(2)}) async-start(bf16[64,8,128]{2,1,0:T(8,128)(2,1)} %get-tuple-element.26), calls=%async_computation | async-start | bytes 262144 | tf_op jit(solution)/shard_map/all_to_all | solution.py:278
  34.9 13.1 %all-to-all-start.1 = ((bf16[4,32,2048]{2,1,0:T(8,128)(2,1)}), bf16[4,32,2048]{2,1,0:T(8,128)(2,1)S(1)}, u32[]{:S(2)}, u32[]{:S(2)}) async-start(bf16[4,32,2048]{2,1,0:T(8,128)(2,1)} %shard_map.201), calls=%async_computation.1 | async-start | bytes 1048576 | tf_op jit(solution)/shard_map/all_to_all | solution.py:278
  39.1 19.9 %collective-permute-start.1 = (bf16[2048,128]{1,0:T(8,128)(2,1)}, bf16[2048,128]{1,0:T(8,128)(2,1)}, u32[]{:S(2)}, u32[]{:S(2)}) collective-permute-start(bf16[2048,128]{1,0:T(8,128)(2,1)} %bitcast.19.g0), channel_id=1, source_target_pairs={{0,1},{1,2},{2,3},{3,0},{4,5},{5,6},{6,7},{7,4},{8,9},{9,10},{10,1... | collective-permute-start | bytes 1572872 | tf_op jit(solution)/shard_map/ppermute | solution.py:274
  40.6 19.1 %collective-permute-start.4 = (bf16[2048,128]{1,0:T(8,128)(2,1)}, bf16[2048,128]{1,0:T(8,128)(2,1)}, u32[]{:S(2)}, u32[]{:S(2)}) collective-permute-start(bf16[2048,128]{1,0:T(8,128)(2,1)} %bitcast.20.u0), channel_id=1, source_target_pairs={{0,3},{1,0},{2,1},{3,2},{4,7},{5,4},{6,5},{7,6},{8,11},{9,8},{10,9... | collective-permute-start | bytes 1572872 | tf_op jit(solution)/shard_map/ppermute | solution.py:274
  41.8 27.2 %collective-permute-start.8 = (bf16[128,2048]{1,0:T(8,128)(2,1)}, bf16[128,2048]{1,0:T(8,128)(2,1)S(1)}, u32[]{:S(2)}, u32[]{:S(2)}) collective-permute-start(bf16[128,2048]{1,0:T(8,128)(2,1)} %bitcast.21.d0), channel_id=1, source_target_pairs={{0,3},{1,0},{2,1},{3,2},{4,7},{5,4},{6,5},{7,6},{8,11},{9,8},{10,9... | collective-permute-start | bytes 1572872 | tf_op jit(solution)/shard_map/ppermute | solution.py:274
  49.4 44.4 %all-to-all-start.2 = ((bf16[64,2,2048]{2,1,0:T(2,128)(2,1)}), bf16[64,2,2048]{2,1,0:T(2,128)(2,1)S(1)}, u32[]{:S(2)}, u32[]{:S(2)}) async-start(bf16[64,2,2048]{2,1,0:T(2,128)(2,1)} %get-tuple-element.37), calls=%async_computation.2 | async-start | bytes 1048576 | tf_op jit(solution)/shard_map/all_to_all | solution.py:278
  56.1 14.6 %collective-permute-start.7 = (bf16[128,2048]{1,0:T(8,128)(2,1)}, bf16[128,2048]{1,0:T(8,128)(2,1)S(1)}, u32[]{:S(2)}, u32[]{:S(2)}) collective-permute-start(bf16[128,2048]{1,0:T(8,128)(2,1)} %bitcast.21.d0), channel_id=1, source_target_pairs={{0,1},{1,2},{2,3},{3,0},{4,5},{5,6},{6,7},{7,4},{8,9},{9,10},{10,1... | collective-permute-start | bytes 1572872 | tf_op jit(solution)/shard_map/ppermute | solution.py:274
  56.5 25.3 %collective-permute-start.2 = (bf16[2048,128]{1,0:T(8,128)(2,1)}, bf16[2048,128]{1,0:T(8,128)(2,1)S(1)}, u32[]{:S(2)}, u32[]{:S(2)}) collective-permute-start(bf16[2048,128]{1,0:T(8,128)(2,1)} %bitcast.20.u0), channel_id=1, source_target_pairs={{0,1},{1,2},{2,3},{3,0},{4,5},{5,6},{6,7},{7,4},{8,9},{9,10},{10,1... | collective-permute-start | bytes 1572872 | tf_op jit(solution)/shard_map/ppermute | solution.py:274
  59.1 27.9 %collective-permute-start.3 = (bf16[2048,128]{1,0:T(8,128)(2,1)}, bf16[2048,128]{1,0:T(8,128)(2,1)S(1)}, u32[]{:S(2)}, u32[]{:S(2)}) collective-permute-start(bf16[2048,128]{1,0:T(8,128)(2,1)} %bitcast.19.g0), channel_id=1, source_target_pairs={{0,3},{1,0},{2,1},{3,2},{4,7},{5,4},{6,5},{7,6},{8,11},{9,8},{10,9... | collective-permute-start | bytes 1572872 | tf_op jit(solution)/shard_map/ppermute | solution.py:274
  59.6 33.3 %collective-permute-start.5 = (bf16[2048,128]{1,0:T(8,128)(2,1)}, bf16[2048,128]{1,0:T(8,128)(2,1)S(1)}, u32[]{:S(2)}, u32[]{:S(2)}) collective-permute-start(bf16[2048,128]{1,0:T(8,128)(2,1)} %collective-permute-done.1.g1), channel_id=1, source_target_pairs={{0,1},{1,2},{2,3},{3,0},{4,5},{5,6},{6,7},{7,4},{8,9},{9,10},{10,1... | collective-permute-start | bytes 1572872 | tf_op jit(solution)/shard_map/ppermute | solution.py:274
  69.0 12.8 %copy-start = (bf16[128,2048]{1,0:T(8,128)(2,1)}, bf16[128,2048]{1,0:T(8,128)(2,1)S(1)}, u32[]{:S(2)}) copy-start(bf16[128,2048]{1,0:T(8,128)(2,1)S(1)} %collective-permute-done.8.d2) | copy-start | bytes 1572868
  69.0 24.8 %collective-permute-start.6 = (bf16[2048,128]{1,0:T(8,128)(2,1)}, bf16[2048,128]{1,0:T(8,128)(2,1)}, u32[]{:S(2)}, u32[]{:S(2)}) collective-permute-start(bf16[2048,128]{1,0:T(8,128)(2,1)} %collective-permute-done.4.u2), channel_id=1, source_target_pairs={{0,3},{1,0},{2,1},{3,2},{4,7},{5,4},{6,5},{7,6},{8,11},{9,8},{10,9... | collective-permute-start | bytes 1572872 | tf_op jit(solution)/shard_map/ppermute | solution.py:274
  70.7 11.1 %copy-start.1 = (bf16[128,2048]{1,0:T(8,128)(2,1)}, bf16[128,2048]{1,0:T(8,128)(2,1)S(1)}, u32[]{:S(2)}) copy-start(bf16[128,2048]{1,0:T(8,128)(2,1)S(1)} %collective-permute-done.7.d1) | copy-start | bytes 1572868
  70.7 26.5 %collective-permute-start.10 = (bf16[64,2048]{1,0:T(8,128)(2,1)S(1)}, bf16[64,2048]{1,0:T(8,128)(2,1)}, u32[]{:S(2)}, u32[]{:S(2)}) collective-permute-start(bf16[64,2048]{1,0:T(8,128)(2,1)S(1)} %slice.18), channel_id=1, source_target_pairs={{0,3},{1,0},{2,1},{3,2},{4,7},{5,4},{6,5},{7,6},{8,11},{9,8},{10,9... | collective-permute-start | bytes 786440 | tf_op jit(solution)/shard_map/ppermute | solution.py:274
  81.8 0.8 copy-start.4
  81.8 17.0 %collective-permute-start.9 = (bf16[64,2048]{1,0:T(8,128)(2,1)}, bf16[64,2048]{1,0:T(8,128)(2,1)}, u32[]{:S(2)}, u32[]{:S(2)}) collective-permute-start(bf16[64,2048]{1,0:T(8,128)(2,1)} %slice.17), channel_id=1, source_target_pairs={{0,1},{1,2},{2,3},{3,0},{4,5},{5,6},{6,7},{7,4},{8,9},{9,10},{10,1... | collective-permute-start | bytes 786440 | tf_op jit(solution)/shard_map/ppermute | solution.py:274
  87.0 6.0 %copy-start.2 = (bf16[2048,128]{1,0:T(8,128)(2,1)}, bf16[2048,128]{1,0:T(8,128)(2,1)S(1)}, u32[]{:S(2)}) copy-start(bf16[2048,128]{1,0:T(8,128)(2,1)S(1)} %collective-permute-done.3.g2) | copy-start | bytes 1572868
  93.0 0.8 copy-start.3
